TPU v7x, 256 devices: a whole 4x4x8 slice. The times are simulated.
256 devices in a mesh: sp: 64 (over z, y, core), tp: 4 (over x).
Axes of the slice: x: 4, y: 4, z: 8, core: 2. Of those that a mesh axis runs over, the one named last changes fastest.
Arguments:
- residual: bfloat16 [16384, 2048], P(('sp', 'tp')), may hold values from -6 to 6
- output_gate_projected: bfloat16 [16384, 4096], P('sp', 'tp'), may hold values from -6 to 6
- value_projected_input: bfloat16 [16384, 4096], P('sp', 'tp'), may hold values from -6 to 6
- state_projected_input: bfloat16 [16384, 2048], P('sp', 'tp'), may hold values from -6 to 6
- readout_projected_input: bfloat16 [16384, 2048], P('sp', 'tp'), may hold values from -6 to 6
- step_preactivation: float32 [16384, 64], P('sp', 'tp'), may hold values from -5 to 5
- position_decay_extra: float32 [16384, 64], P('sp', 'tp')
- value_conv_kernel: bfloat16 [4, 4096], P(None, 'tp'), may hold values from -0.29882812 to 0.29882812
- state_conv_kernel: bfloat16 [4, 2048], P(None, 'tp'), may hold values from -0.8984375 to 0.8984375
- readout_conv_kernel: bfloat16 [4, 2048], P(None, 'tp'), may hold values from -0.8984375 to 0.8984375
- head_log_decay_rates: float32 [64], P('tp')
- head_direct_weight: float32 [64], P('tp'), may hold values from 0.5 to 4
- head_norm_gain: float32 [4096], P('tp'), may hold values from 0.1 to 1.9
- mixer_output_weight: bfloat16 [4096, 2048], P('tp'), may hold values from -0.09375 to 0.09375
- expert_norm_gain: float32 [2048], replicated, may hold values from 0.1 to 1.9
- routed_expert_index: int32 [16384, 4], P(('sp', 'tp')), may hold values from 0 to 63, all different within a row; in each aligned block of 64 rows (0 to 63, 64 to 127, ...) at most 8 rows name the same one
- routed_expert_weight: float32 [16384, 4], P(('sp', 'tp')), may hold values from 0.2 to 1
- routed_gate_weight: bfloat16 [64, 2048, 256], P('sp'), may hold values from -0.125 to 0.125
- routed_up_weight: bfloat16 [64, 2048, 256], P('sp'), may hold values from -0.125 to 0.125
- routed_down_weight: bfloat16 [64, 256, 2048], P('sp'), may hold values from -0.375 to 0.375
- common_gate_weight: bfloat16 [2048, 512], P(None, 'tp'), may hold values from -0.125 to 0.125
- common_up_weight: bfloat16 [2048, 512], P(None, 'tp'), may hold values from -0.125 to 0.125
- common_down_weight: bfloat16 [2048, 512], P(None, 'tp'), may hold values from -0.25 to 0.25
Outputs:
- layer_out: bfloat16 [16384, 2048], P(('sp', 'tp'))
Inputs may be any that keep to these rules, and one draw needn't show every extreme that they name: `routed_expert_index`: among the 64 rows of one device, no expert is named by more than 8 rows.
All inputs are finite; a program needn't handle non-finite values.
Results may differ from a plain program's by a relative error of at most 0.02.
Values may be sent and summed in bfloat16 or wider, within the bound.
A program may use at most 128 MiB of HBM per device.

v0:
```python
import jax
import jax.numpy as jnp
from jax import lax
from jax.sharding import Mesh
from jax.sharding import PartitionSpec as P

D = 2048
HEAD_DIM = 64
STATE = 128
CONV = 4
BLOCK_POSITIONS = 128
SP = ("sp_0", "sp_1", "sp_2")
SP_TP = ("sp_0", "sp_1", "sp_2", "tp")


EPSILON = 1e-06


def shifted(value, axis, steps):
    count = lax.axis_size(axis)
    first, last = (max(0, -steps), min(count, count - steps))
    return lax.ppermute(value, axis, [(source, source + steps) for source in range(first, last)])


def filled_with(array, identity):
    return jax.tree.map(
        lambda part, zero: jnp.zeros_like(part) + jnp.asarray(zero, part.dtype), array, identity
    )


def carried_in(array, axes, combine, identity):
    before = start = filled_with(array, identity)
    total = array
    for axis in reversed(axes):
        size, index = (lax.axis_size(axis), lax.axis_index(axis))
        pieces = jax.tree.map(
            lambda part, kind: lax.all_gather(part.astype(kind), axis),
            total,
            (jnp.bfloat16, jnp.bfloat16),
        )
        inside, total = (start, start)
        for k in range(size):
            passed = k < index
            total = combine(
                total, jax.tree.map(lambda part, own: part[k].astype(own.dtype), pieces, array)
            )
            inside = jax.tree.map(lambda new, old: jnp.where(passed, new, old), total, inside)
        before = combine(inside, before)
    return before


def cut_along(array, dim, size):
    lengths = array.shape
    blocks = array.reshape(*lengths[:dim], size, lengths[dim] // size, *lengths[dim + 1 :])
    return jnp.moveaxis(blocks, dim, 0)


def sum_at_owner(array, axis, dim):
    size = lax.axis_size(axis)
    blocks = lax.all_to_all(cut_along(array, dim, size), axis, 0, 0, tiled=True)
    return jnp.sum(blocks.astype(jnp.float32), axis=0)


def sent_together(arrays, axis, dim, along):
    widths = [a.shape[along] for a in arrays]
    both = jnp.concatenate(arrays, axis=along)
    filled = lax.all_gather(both, axis, axis=dim, tiled=True)
    return tuple(jnp.split(filled, [sum(widths[:k]) for k in range(1, len(widths))], axis=along))


def short_conv(inputs, rim_rows, weights):
    length = inputs.shape[0]
    extended = jnp.concatenate([rim_rows, inputs], axis=0)
    totals = jnp.zeros(inputs.shape, jnp.float32)
    for tap_index in range(CONV):
        totals = totals + extended[tap_index : tap_index + length].astype(jnp.float32) * weights[
            tap_index
        ].astype(jnp.float32)
    return jax.nn.silu(totals)


def shared_part(rows, gate_piece, up_piece, down_piece):
    gate_part = jnp.dot(rows, gate_piece, preferred_element_type=jnp.float32)
    lifted = jnp.dot(rows, up_piece, preferred_element_type=jnp.float32)
    hidden = (jax.nn.silu(gate_part) * lifted).astype(jnp.bfloat16)
    return jnp.einsum("rc,dc->rd", hidden, down_piece, preferred_element_type=jnp.float32)


def join_states(earlier, later):
    return (earlier[0] * later[0], later[0][..., None, None] * earlier[1] + later[1])


def shards(
    residual,
    output_gate_projected,
    value_projected_input,
    state_projected_input,
    readout_projected_input,
    step_preactivation,
    position_decay_extra,
    value_conv_kernel,
    state_conv_kernel,
    readout_conv_kernel,
    head_log_decay_rates,
    head_direct_weight,
    head_norm_gain,
    mixer_output_weight,
    expert_norm_gain,
    routed_expert_index,
    routed_expert_weight,
    routed_gate_weight,
    routed_up_weight,
    routed_down_weight,
    common_gate_weight,
    common_up_weight,
    common_down_weight,
):
    head_count = step_preactivation.shape[1]
    groups = state_projected_input.shape[1] // STATE
    heads_per_group = head_count // groups
    length = value_projected_input.shape[0]
    block_list = length // BLOCK_POSITIONS
    conv_tails = (
        value_projected_input[length - CONV + 1 :],
        state_projected_input[length - CONV + 1 :],
        readout_projected_input[length - CONV + 1 :],
    )
    value_rim, input_rim, readout_rim = shifted(
        (conv_tails[0], conv_tails[1], conv_tails[2]), SP, 1
    )
    values = short_conv(value_projected_input, value_rim, value_conv_kernel).reshape(
        block_list, BLOCK_POSITIONS, groups, heads_per_group, HEAD_DIM
    )
    state_in = short_conv(state_projected_input, input_rim, state_conv_kernel).reshape(
        block_list, BLOCK_POSITIONS, groups, STATE
    )
    readout = short_conv(readout_projected_input, readout_rim, readout_conv_kernel).reshape(
        block_list, BLOCK_POSITIONS, groups, STATE
    )
    head_step_lengths = jax.nn.softplus(step_preactivation)
    decay_logarithm = (
        head_step_lengths * (-jnp.exp(head_log_decay_rates))[None, :] + position_decay_extra
    ).reshape(block_list, BLOCK_POSITIONS, groups, heads_per_group)
    head_step_lengths = head_step_lengths.reshape(
        block_list, BLOCK_POSITIONS, groups, heads_per_group
    )
    causal = jnp.arange(BLOCK_POSITIONS)[:, None] >= jnp.arange(BLOCK_POSITIONS)[None, :]
    cumulative = jnp.cumsum(decay_logarithm, axis=1)
    weighted_output = values * head_step_lengths[..., None]
    by_head = jnp.transpose(cumulative, (0, 2, 3, 1))
    span_logs = by_head[..., :, None] - by_head[..., None, :]
    decay_factors = jnp.exp(jnp.where(causal, span_logs, -jnp.inf))
    attention_scores = jnp.einsum("ctgn,csgn->cgts", readout, state_in)
    within_block_output = jnp.einsum(
        "cgrts,csgrp->ctgrp", attention_scores[:, :, None] * decay_factors, weighted_output
    )
    to_end = jnp.exp(cumulative[:, -1:] - cumulative)
    fresh_state = jnp.einsum("csgn,csgrp->cgrpn", state_in, weighted_output * to_end[..., None])
    block_decay = jnp.exp(cumulative[:, -1])

    def block_chain(carried, block_item):
        state_now, factor = carried
        decay_blk, fresh_blk = block_item
        return (
            (decay_blk[..., None, None] * state_now + fresh_blk, decay_blk * factor),
            (state_now, factor),
        )

    empty_state = jnp.zeros((groups, heads_per_group, HEAD_DIM, STATE), jnp.float32)
    unit_decay = jnp.ones((groups, heads_per_group), jnp.float32)
    (own_state, own_decay), (local_start, local_factor) = lax.scan(
        block_chain, (empty_state, unit_decay), (block_decay, fresh_state)
    )
    incoming = carried_in((own_decay, own_state), SP, join_states, (unit_decay, empty_state))
    start_states = local_start + local_factor[..., None, None] * incoming[1][None]
    carried_out = (
        jnp.einsum("ctgn,cgrpn->ctgrp", readout, start_states) * jnp.exp(cumulative)[..., None]
    )
    mixed_heads = (
        within_block_output
        + carried_out
        + head_direct_weight.reshape(groups, heads_per_group)[None, None, :, :, None] * values
    )
    mixed_heads = mixed_heads.reshape(length, head_count, HEAD_DIM) * jax.nn.silu(
        output_gate_projected.reshape(length, head_count, HEAD_DIM).astype(jnp.float32)
    )
    normed = mixed_heads * lax.rsqrt(
        jnp.mean(mixed_heads * mixed_heads, axis=-1, keepdims=True) + EPSILON
    )
    heads_out = (
        (normed * head_norm_gain.reshape(head_count, HEAD_DIM))
        .astype(jnp.bfloat16)
        .reshape(length, head_count * HEAD_DIM)
    )
    row_count = residual.shape[0]
    mix_sum = sum_at_owner(
        jnp.dot(heads_out, mixer_output_weight, preferred_element_type=jnp.float32).astype(
            jnp.bfloat16
        ),
        "tp",
        0,
    )
    stream = (residual.astype(jnp.float32) + mix_sum).astype(jnp.bfloat16)
    stream_wide = stream.astype(jnp.float32)
    normed_rows = (
        stream_wide
        * lax.rsqrt(jnp.mean(stream_wide * stream_wide, axis=-1, keepdims=True) + EPSILON)
        * expert_norm_gain
    ).astype(jnp.bfloat16)
    pieces = sent_together((common_gate_weight, common_up_weight, common_down_weight), "tp", 1, 0)
    shared = shared_part(normed_rows, pieces[0], pieces[1], pieces[2])
    local_experts = routed_gate_weight.shape[0]
    experts_all = local_experts * lax.axis_size(SP)
    top_count = routed_expert_index.shape[1]
    capacity = 2 * row_count * top_count // experts_all
    flat_ids = routed_expert_index.reshape(-1)
    expert_hits = (flat_ids[:, None] == jnp.arange(experts_all, dtype=jnp.int32)[None, :]).astype(
        jnp.int32
    )
    slot_ranks = jnp.sum((jnp.cumsum(expert_hits, axis=0) - 1) * expert_hits, axis=1)
    slot_index = flat_ids * capacity + slot_ranks
    slot_rows = (
        jnp.full((experts_all * capacity,), row_count, jnp.int32)
        .at[slot_index]
        .set(jnp.arange(row_count * top_count, dtype=jnp.int32) // top_count)
    )
    padded = jnp.concatenate([normed_rows, jnp.zeros((1, D), jnp.bfloat16)], axis=0)
    outgoing = padded[slot_rows].reshape(experts_all, capacity, D)
    arrived = lax.all_to_all(outgoing, SP, split_axis=0, concat_axis=0, tiled=True)
    sources = arrived.shape[0] // local_experts
    grouped = arrived.reshape(sources, local_experts, arrived.shape[1], D)
    gate_part = jnp.einsum(
        "sekd,edf->sekf", grouped, routed_gate_weight, preferred_element_type=jnp.float32
    )
    lifted = jnp.einsum(
        "sekd,edf->sekf", grouped, routed_up_weight, preferred_element_type=jnp.float32
    )
    hidden = (jax.nn.silu(gate_part) * lifted).astype(jnp.bfloat16)
    result = jnp.einsum(
        "sekf,efd->sekd", hidden, routed_down_weight, preferred_element_type=jnp.float32
    ).astype(jnp.bfloat16)
    returned = lax.all_to_all(
        result.reshape(arrived.shape), SP, split_axis=0, concat_axis=0, tiled=True
    )
    picked = returned.reshape(experts_all * capacity, D)[slot_index]
    routed = jnp.sum(
        (picked.astype(jnp.float32) * routed_expert_weight.reshape(-1)[:, None]).reshape(
            row_count, top_count, D
        ),
        axis=1,
    )
    return (stream_wide + shared + routed).astype(jnp.bfloat16)


def solution(mesh):
    torus = Mesh(mesh.devices.reshape(8, 4, 2, mesh.shape["tp"]), ("sp_0", "sp_1", "sp_2", "tp"))
    return jax.shard_map(
        shards,
        mesh=torus,
        in_specs=(
            P(SP_TP, None),
            P(SP, "tp"),
            P(SP, "tp"),
            P(SP, "tp"),
            P(SP, "tp"),
            P(SP, "tp"),
            P(SP, "tp"),
            P(None, "tp"),
            P(None, "tp"),
            P(None, "tp"),
            P("tp"),
            P("tp"),
            P("tp"),
            P("tp", None),
            P(),
            P(SP_TP, None),
            P(SP_TP, None),
            P(SP, None, None),
            P(SP, None, None),
            P(SP, None, None),
            P(None, "tp"),
            P(None, "tp"),
            P(None, "tp"),
        ),
        out_specs=P(SP_TP, None),
        check_vma=False,
    )
```

profile of v0, /device:TPU:1, one launch (start us, length us, event | category | flops | bytes accessed | tf_op | source)
XLA Modules:
  0.0 299.5 jit_solution(525699985170648099)
XLA Ops:
  6.5 0.9 slice.166
  7.4 0.9 copy.55
  8.3 4.6 %collective-permute-start = (bf16[3,1024]{0,1:T(8,128)(2,1)}, bf16[3,1024]{0,1:T(8,128)(2,1)}, u32[]{:S(2)}, u32[]{:S(2)}) collective-permute-start(bf16[3,1024]{0,1:T(8,128)(2,1)} %copy.55), channel_id=1, source_target_pairs={{0,4},{4,8},{8,12},{12,16},{16,20},{20,24},{24,28},{28,32},{32,36}... | collective-permute-start | bytes 18440 | tf_op jit(solution)/shard_map/ppermute | solution.py:22
  12.9 0.7 slice.182
  13.6 1.9 collective-permute-start.2
  15.5 0.9 slice_convert_fusion.3
  16.4 0.7 exponential_negate_fusion
  17.0 0.8 compare_select_fusion
  18.3 1.1 fusion.118
  19.4 1.0 copy.56
  21.1 3.4 %divide_multiply_fusion = f32[256,1024]{0,1:T(8,128)S(1)} fusion(bf16[256,1024]{0,1:T(8,128)(2,1)} %copy.56, bf16[3,1024]{0,1:T(8,128)(2,1)} %collective-permute-done, f32[1024]{0:T(1024)S(1)} %bitcast.252, f32[1024]{0:T(1024)S(1)} %bitcast.253, f32[1024]{0:T(1024)S(1)} %bitcast.251, f32[1024]{0:T(1024)S(1)} %bitcast.250), kind=kLoop, calls=%fused_computation.56 | loop fusion | flops 6291456 | bytes 1595392 | tf_op jit(solution)/shard_map/jit(silu)/mul | solution.py:79
  24.5 1.5 reshape.290
  26.1 2.7 broadcast_multiply_fusion
  29.1 2.0 while.17
  29.1 0.8 bitcast_dynamic-update-slice_fusion.4
  30.1 0.8 bitcast_dynamic-update-slice_fusion.4
  31.1 2.0 all-gather.2
  33.0 8.0 %all_gather.33 = bf16[4,4,4]{2,1,0:T(4,128)(2,1)S(1)} all-gather(bf16[1,4,4]{2,1,0:T(4,128)(2,1)S(1)} %fusion.99), channel_id=1, replica_groups=mesh['sp_0'=8,'sp_1'=4,'sp_2'=2,'tp'=4] {'sp_1'}, dimensions={0}, use_global_device_ids=true | all-gather | bytes 160 | tf_op jit(solution)/shard_map/all_gather | solution.py:37
  41.1 4.3 %all-gather.1 = bf16[8,4,64,128]{3,2,1,0:T(8,128)(2,1)S(1)} all-gather(bf16[4,4,64,128]{3,2,1,0:T(8,128)(2,1)S(1)} %convert_element_type.432), channel_id=3, replica_groups=mesh['sp_0'=8,'sp_1'=4,'sp_2'=2,'tp'=4] {'sp_2'}, dimensions={0}, use_global_device_ids=true | all-gather | bytes 786432 | tf_op jit(solution)/shard_map/all_gather | solution.py:37
  45.4 0.6 fusion.95
  46.0 1.0 fusion.74
  47.0 24.1 %all-gather.7.cloned.1.call-done = bf16[4,4,4,64,128]{4,3,2,1,0:T(8,128)(2,1)} async-done(((bf16[1,4,4,64,128]{4,3,2,1,0:T(8,128)(2,1)}), bf16[4,4,4,64,128]{4,3,2,1,0:T(8,128)(2,1)}) %all-gather.7.cloned.1.call-update) | async-done | bytes 1048592 | tf_op jit(solution)/shard_map/all_gather | solution.py:37
  71.1 2.2 fusion.72
  73.4 1.3 slice.174
  74.7 4.7 %collective-permute-start.1 = (bf16[3,512]{1,0:T(4,128)(2,1)}, bf16[3,512]{1,0:T(4,128)(2,1)}, u32[]{:S(2)}, u32[]{:S(2)}) collective-permute-start(bf16[3,512]{1,0:T(4,128)(2,1)} %slice.174), channel_id=1, source_target_pairs={{0,4},{4,8},{8,12},{12,16},{16,20},{20,24},{24,28},{28,32},{32,36}... | collective-permute-start | bytes 9224 | tf_op jit(solution)/shard_map/ppermute | solution.py:22
  79.5 2.4 pad_maximum_fusion
  81.9 0.6 broadcast_multiply_fusion.2
  82.6 0.6 slice_convert_fusion.11
  83.4 0.6 reduce-window.6
  84.0 0.7 slice_reduce_fusion
  84.7 0.6 iota_compare_fusion.2
  85.3 0.6 eq.25
  86.0 1.2 copy.71
  87.2 1.5 reshape.328
  88.8 0.7 mul.656
  89.6 0.8 copy.61
  90.4 0.9 copy.75
  91.3 0.6 mul.678
  91.9 0.7 reduce-window.9
  92.6 2.5 divide_multiply_fusion.2
  95.1 1.7 reshape.291
  96.8 2.1 fusion.63
  98.9 14.4 %all_gather.34 = bf16[8,4,4]{2,1,0:T(4,128)(2,1)S(1)} all-gather(bf16[1,4,4]{2,1,0:T(4,128)(2,1)S(1)} %fusion.96), channel_id=1, replica_groups=mesh['sp_0'=8,'sp_1'=4,'sp_2'=2,'tp'=4] {'sp_0'}, dimensions={0}, use_global_device_ids=true | all-gather | bytes 288 | tf_op jit(solution)/shard_map/all_gather | solution.py:37
  113.3 3.4 %fusion.60 = f32[4,4,64,128]{3,2,1,0:T(8,128)S(1)} fusion(bf16[8,4,4,64,128]{4,3,2,1,0:T(8,128)(2,1)} %all-gather.9.cloned.1.call-done, f32[4,4]{1,0:T(4,128)} %get-tuple-element.92, f32[4,4]{1,0:T(4,128)S(1)} %get-tuple-element.122, f32[4,4]{1,0:T(4,128)S(1)} %fusion.107, f32[4,4]{1,0:T(4,128)S(1)} %get-tuple-element.110, ...), kind=kLoop, calls=%fused_computation.77 | loop fusion | flops 7471104 | bytes 4195342 | tf_op jit(solution)/shard_map/mul | solution.py:175
  117.2 0.8 copy-done.2
  118.4 1.3 multiply_reduce_fusion.1
  119.7 0.8 copy.70
  120.9 0.9 copy-done.31
  121.8 2.2 convolution_convert_fusion.1
  124.1 4.1 %all-to-all-start = ((bf16[4,64,2048]{2,1,0:T(8,128)(2,1)}), bf16[4,64,2048]{2,1,0:T(8,128)(2,1)S(1)}, u32[]{:S(2)}, u32[]{:S(2)}) async-start(bf16[4,64,2048]{2,1,0:T(8,128)(2,1)} %bitcast.40), calls=%async_computation | async-start | bytes 2097152 | tf_op jit(solution)/shard_map/all_to_all | solution.py:60
  128.3 1.4 scatter_custom_fusion
  129.8 17.1 %all-to-all-done = bf16[4,64,2048]{2,1,0:T(8,128)(2,1)S(1)} async-done(((bf16[4,64,2048]{2,1,0:T(8,128)(2,1)}), bf16[4,64,2048]{2,1,0:T(8,128)(2,1)S(1)}, u32[]{:S(2)}, u32[]{:S(2)}) %all-to-all-start) | async-done | bytes 1048608 | tf_op jit(solution)/shard_map/all_to_all | solution.py:60
  148.0 2.5 gather_fusion
  150.5 67.1 %all_to_all.15 = bf16[64,8,2048]{2,1,0:T(8,128)(2,1)S(1)} all-to-all(bf16[64,8,2048]{2,1,0:T(8,128)(2,1)S(1)} %bitcast.243), channel_id=1, replica_groups=mesh['sp_0'=8,'sp_1'=4,'sp_2'=2,'tp'=4] {'sp_0','sp_1','sp_2'}, dimensions={0} | all-to-all | bytes 4194304 | tf_op jit(solution)/shard_map/all_to_all | solution.py:229
  217.6 1.4 copy-done.5
  218.9 0.7 convolution_bitcast_fusion.2
  220.2 5.3 %convolution_convert_fusion = bf16[64,8,2048]{2,1,0:T(8,128)(2,1)} fusion(bf16[64,8,2048]{2,1,0:T(8,128)(2,1)} %copy-done.5, bf16[1,256,2048]{2,1,0:T(8,128)(2,1)S(1)} %copy-done, bf16[1,2048,256]{2,1,0:T(8,128)(2,1)S(1)} %copy-done.33, f32[64,1,8,256]{3,2,0,1:T(8,128)S(1)} %convolution_bitcast_fusion.2), kind=kOutput, calls=%fused_computation.8 | convolution fusion | flops 1075576832 | bytes 6815744 | tf_op jit(solution)/shard_map/sekf,efd->sekd/dot_general | solution.py:239
  225.5 7.1 %all-to-all-start.2 = ((bf16[64,8,2048]{2,1,0:T(8,128)(2,1)}), bf16[64,8,2048]{2,1,0:T(8,128)(2,1)S(1)}, u32[]{:S(2)}, u32[]{:S(2)}) async-start(bf16[64,8,2048]{2,1,0:T(8,128)(2,1)} %convolution_convert_fusion), calls=%async_computation.2 | async-start | bytes 4194304 | tf_op jit(solution)/shard_map/all_to_all | solution.py:242
  232.7 2.8 fusion.5
  235.5 46.8 %all-to-all-done.2 = bf16[64,8,2048]{2,1,0:T(8,128)(2,1)S(1)} async-done(((bf16[64,8,2048]{2,1,0:T(8,128)(2,1)}), bf16[64,8,2048]{2,1,0:T(8,128)(2,1)S(1)}, u32[]{:S(2)}, u32[]{:S(2)}) %all-to-all-start.2) | async-done | bytes 2097184 | tf_op jit(solution)/shard_map/all_to_all | solution.py:242
  282.3 2.3 gather_fusion.1
  284.6 1.7 reshape.329
  286.3 2.3 multiply_reduce_fusion
  288.7 4.3 %fusion.1 = bf16[64,2048]{1,0:T(8,128)(2,1)} fusion(f32[64,2048]{1,0:T(8,128)} %multiply_reduce_fusion, bf16[6144,512]{1,0:T(8,128)(2,1)} %all-gather.11.cloned.1.call-done, bf16[64,2048]{1,0:T(8,128)(2,1)S(1)} %copy-done.9, f32[64,512]{1,0:T(8,128)} %fusion.5, f32[2048]{0:T(1024)S(1)} %copy-done.20, f32[64]{0:T(128)S(1)} %add_rsqrt_fusion.1), kind=kOutput, calls=%fused_computation.12 | convolution fusion | flops 269680640 | bytes 5644800 | tf_op jit(solution)/shard_map/rc,dc->rd/dot_general | solution.py:86
  (128 shorter events, 5.4 us)
Async XLA Ops:
  6.5 213.1 %copy-start = (bf16[1,256,2048]{2,1,0:T(8,128)(2,1)S(1)}, bf16[1,256,2048]{2,1,0:T(8,128)(2,1)}, u32[]{:S(2)}) copy-start(bf16[1,256,2048]{2,1,0:T(8,128)(2,1)} %param.44) | copy-start | bytes 3145732
  6.5 12.9 %copy-start.10 = (bf16[256,1024]{1,0:T(8,128)(2,1)S(1)}, bf16[256,1024]{1,0:T(8,128)(2,1)}, u32[]{:S(2)}) copy-start(bf16[256,1024]{1,0:T(8,128)(2,1)} %param.27) | copy-start | bytes 1572868
  6.5 12.8 %copy-start.18 = (bf16[4,512]{1,0:T(4,128)(2,1)S(1)}, bf16[4,512]{1,0:T(4,128)(2,1)}, u32[]{:S(2)}) copy-start(bf16[4,512]{1,0:T(4,128)(2,1)} %param.33) | copy-start | bytes 12292
  6.5 64.6 %all-gather.7.cloned.1.call-start = ((), (), s32[]{:S(2)}) async-start(), calls=%async_computation.3 | async-start | bytes 1310720 | tf_op jit(solution)/shard_map/all_gather | solution.py:37
  8.3 12.8 %collective-permute-start = (bf16[3,1024]{0,1:T(8,128)(2,1)}, bf16[3,1024]{0,1:T(8,128)(2,1)}, u32[]{:S(2)}, u32[]{:S(2)}) collective-permute-start(bf16[3,1024]{0,1:T(8,128)(2,1)} %copy.55), channel_id=1, source_target_pairs={{0,4},{4,8},{8,12},{12,16},{16,20},{20,24},{24,28},{28,32},{32,36}... | collective-permute-start | bytes 18440 | tf_op jit(solution)/shard_map/ppermute | solution.py:22
  13.6 7.1 %collective-permute-start.2 = (bf16[3,512]{1,0:T(4,128)(2,1)S(1)}, bf16[3,512]{1,0:T(4,128)(2,1)S(1)}, u32[]{:S(2)}, u32[]{:S(2)}) collective-permute-start(bf16[3,512]{1,0:T(4,128)(2,1)S(1)} %slice.182), channel_id=1, source_target_pairs={{0,4},{4,8},{8,12},{12,16},{16,20},{20,24},{24,28},{28,32},{32,36}... | collective-permute-start | bytes 9224 | tf_op jit(solution)/shard_map/ppermute | solution.py:22
  18.1 2.6 copy-start.14
  31.1 42.3 %copy-start.24 = (f32[2,4,4]{2,1,0:T(4,128)}, f32[2,4,4]{2,1,0:T(4,128)S(1)}, u32[]{:S(2)}) copy-start(f32[2,4,4]{2,1,0:T(4,128)S(1)} %get-tuple-element.46) | copy-start | bytes 388
  41.0 38.4 %copy-start.12 = (bf16[2048,128]{1,0:T(8,128)(2,1)S(1)}, bf16[2048,128]{1,0:T(8,128)(2,1)}, u32[]{:S(2)}) copy-start(bf16[2048,128]{1,0:T(8,128)(2,1)} %param.47) | copy-start | bytes 1572868
  46.9 66.3 %all-gather.9.cloned.1.call-start = ((), (), s32[]{:S(2)}) async-start(), calls=%async_computation.4 | async-start | bytes 2359296 | tf_op jit(solution)/shard_map/all_gather | solution.py:37
  73.4 159.3 %all-gather.11.cloned.1.call-start = ((), (), s32[]{:S(2)}) async-start(), calls=%async_computation.5 | async-start | bytes 7864320 | tf_op jit(solution)/shard_map/all_gather | solution.py:67
  74.7 7.2 %copy-start.21 = (s32[64,4]{0,1:T(4,128)S(1)}, s32[64,4]{0,1:T(4,128)}, u32[]{:S(2)}) copy-start(s32[64,4]{0,1:T(4,128)} %param.40) | copy-start | bytes 3076
  74.7 7.9 %copy-start.19 = (bf16[4,512]{1,0:T(4,128)(2,1)S(1)}, bf16[4,512]{1,0:T(4,128)(2,1)}, u32[]{:S(2)}) copy-start(bf16[4,512]{1,0:T(4,128)(2,1)} %param.34) | copy-start | bytes 12292
  74.7 17.8 %collective-permute-start.1 = (bf16[3,512]{1,0:T(4,128)(2,1)}, bf16[3,512]{1,0:T(4,128)(2,1)}, u32[]{:S(2)}, u32[]{:S(2)}) collective-permute-start(bf16[3,512]{1,0:T(4,128)(2,1)} %slice.174), channel_id=1, source_target_pairs={{0,4},{4,8},{8,12},{12,16},{16,20},{20,24},{24,28},{28,32},{32,36}... | collective-permute-start | bytes 9224 | tf_op jit(solution)/shard_map/ppermute | solution.py:22
  81.9 6.8 %copy-start.30 = (f32[16]{0:T(128)S(1)}, f32[16]{0:T(128)}, u32[]{:S(2)}) copy-start(f32[16]{0:T(128)} %param.36) | copy-start | bytes 196
  81.9 7.5 %copy-start.4 = (f32[2,128,4,4]{3,2,1,0:T(4,128)S(1)}, f32[2,128,4,4]{3,2,1,0:T(4,128)}, u32[]{:S(2)}) copy-start(f32[2,128,4,4]{3,2,1,0:T(4,128)} %get-tuple-element.95) | copy-start | bytes 49156
  90.4 22.8 %copy-start.1 = (bf16[4,4,4,64,128]{4,3,2,1,0:T(8,128)(2,1)S(1)}, bf16[4,4,4,64,128]{4,3,2,1,0:T(8,128)(2,1)}, u32[]{:S(2)}) copy-start(bf16[4,4,4,64,128]{4,3,2,1,0:T(8,128)(2,1)} %all-gather.7.cloned.1.call-done) | copy-start | bytes 3145732
  92.6 6.3 %copy-start.22 = (s32[64,3]{0,1:T(4,128)}, s32[64,3]{0,1:T(4,128)S(1)}, u32[]{:S(2)}) copy-start(s32[64,3]{0,1:T(4,128)S(1)} %reduce-window.9) | copy-start | bytes 2308
  113.3 3.5 %copy-start.3 = (bf16[2,128,4,128]{3,2,1,0:T(4,128)(2,1)S(1)}, bf16[2,128,4,128]{3,2,1,0:T(4,128)(2,1)}, u32[]{:S(2)}) copy-start(bf16[2,128,4,128]{3,2,1,0:T(4,128)(2,1)} %reshape.291) | copy-start | bytes 786436
  113.3 3.5 %copy-start.7 = (f32[2,4,4,64,128]{4,3,2,1,0:T(8,128)S(1)}, f32[2,4,4,64,128]{4,3,2,1,0:T(8,128)}, u32[]{:S(2)}) copy-start(f32[2,4,4,64,128]{4,3,2,1,0:T(8,128)} %get-tuple-element.45) | copy-start | bytes 3145732
  113.3 3.5 %copy-start.25 = (f32[2,4,4]{2,1,0:T(4,128)S(1)}, f32[2,4,4]{2,1,0:T(4,128)}, u32[]{:S(2)}) copy-start(f32[2,4,4]{2,1,0:T(4,128)} %copy-done.24) | copy-start | bytes 388
  113.3 3.8 %copy-start.13 = (bf16[2,128,4,4,64]{1,0,4,3,2:T(2,128)(2,1)S(1)}, bf16[2,128,4,4,64]{1,0,4,3,2:T(2,128)(2,1)}, u32[]{:S(2)}) copy-start(bf16[2,128,4,4,64]{1,0,4,3,2:T(2,128)(2,1)} %get-tuple-element.94) | copy-start | bytes 1572868
  116.7 1.2 copy-start.2
  116.7 1.5 copy-start.6
  116.7 1.7 copy-start.11
  116.7 1.6 copy-start.16
  116.7 1.6 copy-start.17
  116.7 1.6 copy-start.29
  119.6 0.9 copy-start.23
  119.6 2.2 copy-start.31
  124.1 4.1 %slice-start = ((s32[64,3]{0,1:T(4,128)}), s32[64,2]{0,1:T(2,128)S(1)}, s32[]{:S(2)}) async-start(s32[64,3]{0,1:T(4,128)} %copy-done.22), calls=%async_computation.6 | async-start | bytes 2048 | tf_op jit(solution)/shard_map/slice.1
  124.1 4.1 %copy-start.26 = (s32[256]{0:T(256)S(1)}, s32[256]{0:T(256)}, u32[]{:S(2)}) copy-start(s32[256]{0:T(256)} %eq.25) | copy-start | bytes 3076
  124.1 4.2 %copy-start.27 = (s32[256,1]{0,1:T(1,128)S(1)}, s32[256,1]{0,1:T(1,128)}, u32[]{:S(2)}) copy-start(s32[256,1]{0,1:T(1,128)} %mul.678) | copy-start | bytes 3076
  124.1 23.0 %copy-start.15 = (bf16[64,2048]{1,0:T(8,128)(2,1)S(1)}, bf16[64,2048]{1,0:T(8,128)(2,1)}, u32[]{:S(2)}) copy-start(bf16[64,2048]{1,0:T(8,128)(2,1)} %param.25) | copy-start | bytes 786436
  124.1 23.2 %copy-start.20 = (f32[2048]{0:T(1024)S(1)}, f32[2048]{0:T(1024)}, u32[]{:S(2)}) copy-start(f32[2048]{0:T(1024)} %param.39) | copy-start | bytes 24580
  124.1 22.8 %all-to-all-start = ((bf16[4,64,2048]{2,1,0:T(8,128)(2,1)}), bf16[4,64,2048]{2,1,0:T(8,128)(2,1)S(1)}, u32[]{:S(2)}, u32[]{:S(2)}) async-start(bf16[4,64,2048]{2,1,0:T(8,128)(2,1)} %bitcast.40), calls=%async_computation | async-start | bytes 2097152 | tf_op jit(solution)/shard_map/all_to_all | solution.py:60
  147.2 0.7 copy-start.8
  150.4 68.5 %copy-start.32 = (bf16[1,2048,256]{2,1,0:T(8,128)(2,1)S(1)}, bf16[1,2048,256]{2,1,0:T(8,128)(2,1)}, u32[]{:S(2)}) copy-start(bf16[1,2048,256]{2,1,0:T(8,128)(2,1)} %param.42) | copy-start | bytes 3145732
  217.6 1.4 copy-start.5
  218.9 1.2 copy-start.33
  225.4 7.1 %copy-start.28 = (f32[64,4]{0,1:T(4,128)S(1)}, f32[64,4]{0,1:T(4,128)}, u32[]{:S(2)}) copy-start(f32[64,4]{0,1:T(4,128)} %param.41) | copy-start | bytes 3076
  225.5 7.3 %copy-start.9 = (bf16[64,2048]{1,0:T(8,128)(2,1)S(1)}, bf16[64,2048]{1,0:T(8,128)(2,1)}, u32[]{:S(2)}) copy-start(bf16[64,2048]{1,0:T(8,128)(2,1)} %copy-done.8) | copy-start | bytes 786436
  225.5 56.8 %all-to-all-start.2 = ((bf16[64,8,2048]{2,1,0:T(8,128)(2,1)}), bf16[64,8,2048]{2,1,0:T(8,128)(2,1)S(1)}, u32[]{:S(2)}, u32[]{:S(2)}) async-start(bf16[64,8,2048]{2,1,0:T(8,128)(2,1)} %convolution_convert_fusion), calls=%async_computation.2 | async-start | bytes 4194304 | tf_op jit(solution)/shard_map/all_to_all | solution.py:242
Sparse Core Ops, SparseCore 0:
  47.0 24.0 all-gather.6
  73.5 39.0 all-gather.8
  114.4 82.3 all-gather.10
where the time goes:
time: 301 us; the launch traced here: 299 us
  blocking collectives  95.7 us (32%)
  waiting for transfers between devices  88.1 us (29%)
  other arithmetic  30.6 us (10%)
  local copies, waits for them, and re-layouts  29.6 us (10%)
  starting transfers between devices  22.5 us (7%)
  matrix products  19.3 us (6%)
  between operations  13.7 us (5%)
    all_to_all x1, blocking collectives, shards(): lax.all_to_all(outgoing, SP, split_axis=0, concat_axis=0, tiled=True)  67.1 us
    all_to_all x1, waiting for transfers between devices, shards(): lax.all_to_all(result.reshape(arrived.shape), SP, split_axis=0, concat_ax...  46.8 us
    all_gather x4, blocking collectives, carried_in(): lax.all_gather(part.astype(kind), axis)  28.6 us
    all_gather x2, waiting for transfers between devices, carried_in(): lax.all_gather(part.astype(kind), axis)  24.1 us
    all_to_all x1, waiting for transfers between devices, sum_at_owner(): blocks = lax.all_to_all(cut_along(array, dim, size), axis, 0, 0, tiled=True)  17.1 us
    ppermute x3, starting transfers between devices, shifted(): lax.ppermute(value, axis, [(source, source + steps) for source in range(f...  11.2 us
    unnamed x73, local copies, waits for them, and re-layouts  7.13 us
    all_to_all x1, starting transfers between devices, shards(): lax.all_to_all(result.reshape(arrived.shape), SP, split_axis=0, concat_ax...  7.1 us
  transfers between devices with their start and end apart: 8, of which 3 were waited for; matrix products, arithmetic and copies ran while one was open for 16% of the time, Pallas kernels for 0%

commit v1 on v0

--- a/solution.py
+++ b/solution.py
@@ -1,6 +1,8 @@
 import jax
 import jax.numpy as jnp
 from jax import lax
+from jax.experimental import pallas as pl
+from jax.experimental.pallas import tpu as pltpu
 from jax.sharding import Mesh
 from jax.sharding import PartitionSpec as P
 
@@ -88,6 +90,386 @@
 
 def join_states(earlier, later):
     return (earlier[0] * later[0], later[0][..., None, None] * earlier[1] + later[1])
+
+
+MESH = pl.DeviceIdType.MESH
+BF16 = jnp.bfloat16
+F32 = jnp.float32
+NZ, NY, NC, NX = 8, 4, 2, 4
+PLANE = NY * NC
+ROWS = 64
+HALF = ROWS // 2
+CAP = 8
+FE = 256
+
+
+def place():
+    return tuple(lax.axis_index(name) for name in SP_TP)
+
+
+def device(z, y, c, x):
+    return {"sp_0": z, "sp_1": y, "sp_2": c, "tp": x}
+
+
+def remote(src, dst, send_sem, recv_sem, target):
+    return pltpu.make_async_remote_copy(
+        src_ref=src,
+        dst_ref=dst,
+        send_sem=send_sem,
+        recv_sem=recv_sem,
+        device_id=target,
+        device_id_type=MESH,
+    )
+
+
+def arrive(ref, sem):
+    pltpu.make_async_copy(ref, ref, sem).wait()
+
+
+def greet(targets):
+    barrier = pltpu.get_barrier_semaphore()
+    for target in targets:
+        pl.semaphore_signal(barrier, inc=1, device_id=target, device_id_type=MESH)
+    pl.semaphore_wait(barrier, len(targets))
+
+
+def moe_kernel(
+    rows,
+    stream,
+    meta,
+    rg_hbm,
+    ru_hbm,
+    rd_hbm,
+    cg_hbm,
+    cu_hbm,
+    cd_hbm,
+    out,
+    zall,
+    metas,
+    combine_w,
+    send_rows,
+    expert_rows,
+    expert_out,
+    back_rows,
+    rs_send,
+    rs_recv,
+    xall,
+    sh_send,
+    sh_recv,
+    rg,
+    ru,
+    rd,
+    cg,
+    cu,
+    cd,
+    w_sem,
+    zs_sem,
+    zr_sem,
+    ms_sem,
+    mr_sem,
+    ds_sem,
+    dr_sem,
+    bs_sem,
+    br_sem,
+    rss_sem,
+    rsr_sem,
+    xs_sem,
+    xr_sem,
+    hs_sem,
+    hr_sem,
+):
+    z, y, c, x = place()
+    me = y * NC + c
+    z_up, z_down = lax.rem(z + 1, NZ), lax.rem(z + NZ - 1, NZ)
+    z_peers = [device(lax.rem(z + d, NZ), y, c, x) for d in range(1, NZ)]
+    x_peers = [device(z, y, c, lax.rem(x + d, NX)) for d in range(1, NX)]
+    plane_peers = []
+    for dy in (1, 3, 2, 0):
+        for dc in range(NC):
+            if dy or dc:
+                yy, cc = lax.rem(y + dy, NY), lax.rem(c + dc, NC)
+                plane_peers.append((yy * NC + cc, device(z, yy, cc, x)))
+
+    weights = [
+        pltpu.make_async_copy(far, near, w_sem.at[k])
+        for k, (far, near) in enumerate(
+            ((cg_hbm, cg), (cu_hbm, cu), (cd_hbm, cd), (rg_hbm, rg), (ru_hbm, ru), (rd_hbm, rd))
+        )
+    ]
+    for copy in weights:
+        copy.start()
+    greet(z_peers + x_peers + [peer for _, peer in plane_peers])
+
+    ring = []
+
+    def hop(step, up, half):
+        lo = half * HALF
+        here = ((NZ - step) % NZ) if up else step
+        there = ((NZ - step - 1) % NZ) if up else step + 1
+        source = rows if step == 0 else zall.at[here]
+        k = 0 if up else 1
+        copy = remote(
+            source.at[pl.ds(lo, HALF)],
+            zall.at[there, pl.ds(lo, HALF)],
+            zs_sem.at[k, step, half],
+            zr_sem.at[k, step, half],
+            device(z_up if up else z_down, y, c, x),
+        )
+        copy.start()
+        ring.append(copy)
+
+    def ring_arrived(step, up, half):
+        lo = half * HALF
+        there = ((NZ - step - 1) % NZ) if up else step + 1
+        arrive(zall.at[there, pl.ds(lo, HALF)], zr_sem.at[0 if up else 1, step, half])
+
+    meta_copies = [
+        remote(meta, metas.at[NZ - d], ms_sem.at[d - 1], mr_sem.at[NZ - d - 1], z_peers[d - 1])
+        for d in range(1, NZ)
+    ]
+    for copy in meta_copies:
+        copy.start()
+    for half in range(2):
+        hop(0, True, half)
+        hop(0, False, half)
+    x_copies = [
+        remote(rows, xall.at[x], xs_sem.at[d - 1], xr_sem.at[NX - d - 1], x_peers[d - 1])
+        for d in range(1, NX)
+    ]
+    for copy in x_copies:
+        copy.start()
+
+    token = lax.broadcasted_iota(jnp.int32, (ROWS, ROWS), 0)
+    later = lax.broadcasted_iota(jnp.int32, (ROWS, ROWS), 1)
+    before = jnp.where(token < later, 1.0, 0.0).astype(BF16)
+    expert_row = lax.broadcasted_iota(jnp.int32, (PLANE, ROWS), 0) + z * PLANE
+    expert_row = expert_row.astype(F32)
+    slot = lax.broadcasted_iota(jnp.int32, (PLANE, CAP, ROWS), 1).astype(F32)
+    sends = []
+
+    def dispatch(o):
+        table = meta[...] if o == 0 else metas[o]
+        hits = jnp.zeros((PLANE, ROWS), F32)
+        shares = jnp.zeros((PLANE, ROWS), F32)
+        for k in range(4):
+            hit = jnp.where(expert_row == table[k : k + 1, :ROWS], 1.0, 0.0)
+            hits = hits + hit
+            shares = shares + hit * table[4 + k : 5 + k, :ROWS]
+        rank = jnp.dot(hits.astype(BF16), before, preferred_element_type=F32)
+        chosen = jnp.where(
+            (rank[:, None, :] == slot) & (hits[:, None, :] > 0.5),
+            jnp.ones((PLANE, CAP, ROWS), F32),
+            jnp.zeros((PLANE, CAP, ROWS), F32),
+        )
+        combine_w[o] = (chosen * shares[:, None, :]).reshape(ROWS, ROWS)
+        block = rows[...] if o == 0 else zall[o]
+        packed = jnp.dot(
+            chosen.reshape(ROWS, ROWS).astype(BF16), block, preferred_element_type=F32
+        )
+        send_rows[o] = packed.reshape(PLANE, CAP, D).astype(BF16)
+        for index, peer in plane_peers:
+            copy = remote(
+                send_rows.at[o, index], expert_rows.at[o, me], ds_sem.at[o], dr_sem.at[o], peer
+            )
+            copy.start()
+        sends.append((send_rows.at[o], ds_sem.at[o]))
+        expert_rows[o, me] = send_rows[o, me]
+
+    def run_expert(blocks):
+        for o in blocks:
+            arrive(expert_rows.at[o, pl.ds(0, PLANE - 1)], dr_sem.at[o])
+        inputs = jnp.concatenate(
+            [expert_rows[o].astype(F32).reshape(ROWS, D) for o in blocks], axis=0
+        ).astype(BF16)
+        gate = jnp.dot(inputs, rg[...], preferred_element_type=F32)
+        lifted = jnp.dot(inputs, ru[...], preferred_element_type=F32)
+        hidden = (jax.nn.silu(gate) * lifted).astype(BF16)
+        result = jnp.dot(hidden, rd[...], preferred_element_type=F32)
+        for k, o in enumerate(blocks):
+            expert_out[o] = (
+                result[k * ROWS : (k + 1) * ROWS].reshape(PLANE, CAP, D).astype(BF16)
+            )
+
+    def give_back(o):
+        for index, peer in plane_peers:
+            copy = remote(
+                expert_out.at[o, index], back_rows.at[o, me], bs_sem.at[o], br_sem.at[o], peer
+            )
+            copy.start()
+        sends.append((expert_out.at[o], bs_sem.at[o]))
+        back_rows[o, me] = expert_out[o, me]
+
+    def combined(o):
+        arrive(back_rows.at[o, pl.ds(0, PLANE - 1)], br_sem.at[o])
+        returned = back_rows[o].astype(F32).reshape(ROWS, D).astype(BF16)
+        return lax.dot_general(
+            combine_w[o].astype(BF16),
+            returned,
+            (((0,), (0,)), ((), ())),
+            preferred_element_type=F32,
+        )
+
+    dispatch(0)
+    for d in range(1, NZ):
+        arrive(metas.at[NZ - d], mr_sem.at[NZ - d - 1])
+    for half in range(2):
+        for up in (True, False):
+            ring_arrived(0, up, half)
+            hop(1, up, half)
+    dispatch(7)
+    dispatch(1)
+    for copy in weights:
+        copy.wait()
+    run_expert((0,))
+    for half in range(2):
+        for up in (True, False):
+            ring_arrived(1, up, half)
+            hop(2, up, half)
+    dispatch(6)
+    dispatch(2)
+    run_expert((7, 1))
+    ring_arrived(2, True, 0)
+    hop(3, True, 0)
+    ring_arrived(2, False, 1)
+    hop(3, False, 1)
+    ring_arrived(2, True, 1)
+    ring_arrived(2, False, 0)
+    dispatch(5)
+    dispatch(3)
+    run_expert((6, 2))
+
+    for d in range(1, NX):
+        arrive(xall.at[0], xr_sem.at[d - 1])
+    xall[x] = rows[...]
+    share_copies = []
+    hidden_rows = xall[...].reshape(NX * ROWS, D)
+    gate = jnp.dot(hidden_rows, cg[...], preferred_element_type=F32)
+    lifted = jnp.dot(hidden_rows, cu[...], preferred_element_type=F32)
+    hidden = (jax.nn.silu(gate) * lifted).astype(BF16)
+    shared = lax.dot_general(
+        hidden, cd[...], (((1,), (1,)), ((), ())), preferred_element_type=F32
+    )
+    sh_send[...] = shared.reshape(NX, ROWS, D).astype(BF16)
+    for d in range(1, NX):
+        xx = lax.rem(x + d, NX)
+        copy = remote(
+            sh_send.at[xx],
+            sh_recv.at[NX - d - 1],
+            hs_sem.at[d - 1],
+            hr_sem.at[NX - d - 1],
+            x_peers[d - 1],
+        )
+        copy.start()
+        share_copies.append(copy)
+
+    ring_arrived(3, True, 0)
+    ring_arrived(3, False, 1)
+    dispatch(4)
+    run_expert((5, 3))
+    run_expert((4,))
+    for o in (4, 3, 5, 2, 6, 1, 7, 0):
+        give_back(o)
+
+    def pass_on(step, up, half):
+        k = 0 if up else 1
+        lo = half * HALF
+        copy = remote(
+            rs_send.at[k, step, pl.ds(lo, HALF)],
+            rs_recv.at[k, step, pl.ds(lo, HALF)],
+            rss_sem.at[k, step, half],
+            rsr_sem.at[k, step, half],
+            device(z_up if up else z_down, y, c, x),
+        )
+        copy.start()
+        ring.append(copy)
+
+    def sum_arrived(step, up, half):
+        k = 0 if up else 1
+        part = rs_recv.at[k, step, pl.ds(half * HALF, HALF)]
+        arrive(part, rsr_sem.at[k, step, half])
+        return rs_recv[k, step, pl.ds(half * HALF, HALF)].astype(F32)
+
+    first = combined(4).astype(BF16)
+    rs_send[0, 0, :HALF] = first[:HALF]
+    pass_on(0, True, 0)
+    rs_send[1, 0, HALF:] = first[HALF:]
+    pass_on(0, False, 1)
+    for step in range(1, 4):
+        parts = (combined(4 - step), combined(4 + step))
+        for turn in range(2):
+            for k, up in enumerate((True, False)):
+                half = turn if up else 1 - turn
+                piece = parts[k][half * HALF : (half + 1) * HALF]
+                if step > 1 or turn == 0:
+                    piece = piece + sum_arrived(step - 1, up, half)
+                rs_send[k, step, pl.ds(half * HALF, HALF)] = piece.astype(BF16)
+                pass_on(step, up, half)
+    total = combined(0) + stream[...].astype(F32)
+    total = total + sh_send[x].astype(F32)
+    for d in range(1, NX):
+        arrive(sh_recv.at[d - 1], hr_sem.at[d - 1])
+        total = total + sh_recv[d - 1].astype(F32)
+    for half in range(2):
+        piece = total[half * HALF : (half + 1) * HALF]
+        for up in (True, False):
+            piece = piece + sum_arrived(3, up, half if up else half)
+        out[half * HALF : (half + 1) * HALF] = piece.astype(BF16)
+
+    for copy in ring + meta_copies + x_copies + share_copies:
+        copy.wait_send()
+    for ref, sem in sends:
+        arrive(ref.at[pl.ds(0, PLANE - 1)], sem)
+
+
+def moe(rows, stream, meta, rg, ru, rd, cg, cu, cd):
+    vmem = pl.BlockSpec(memory_space=pltpu.VMEM)
+    hbm = pl.BlockSpec(memory_space=pl.ANY)
+    blocks = (NZ, PLANE, CAP, D)
+    dma = pltpu.SemaphoreType.DMA
+    return pl.pallas_call(
+        moe_kernel,
+        out_shape=jax.ShapeDtypeStruct((ROWS, D), BF16),
+        in_specs=[vmem] * 3 + [hbm] * 6,
+        out_specs=vmem,
+        scratch_shapes=[
+            pltpu.VMEM((NZ, ROWS, D), BF16),
+            pltpu.VMEM((NZ, 8, 128), F32),
+            pltpu.VMEM((NZ, ROWS, ROWS), F32),
+            pltpu.VMEM(blocks, BF16),
+            pltpu.VMEM(blocks, BF16),
+            pltpu.VMEM(blocks, BF16),
+            pltpu.VMEM(blocks, BF16),
+            pltpu.VMEM((2, 4, ROWS, D), BF16),
+            pltpu.VMEM((2, 4, ROWS, D), BF16),
+            pltpu.VMEM((NX, ROWS, D), BF16),
+            pltpu.VMEM((NX, ROWS, D), BF16),
+            pltpu.VMEM((NX - 1, ROWS, D), BF16),
+            pltpu.VMEM(rg.shape, BF16),
+            pltpu.VMEM(ru.shape, BF16),
+            pltpu.VMEM(rd.shape, BF16),
+            pltpu.VMEM(cg.shape, BF16),
+            pltpu.VMEM(cu.shape, BF16),
+            pltpu.VMEM(cd.shape, BF16),
+            dma((6,)),
+            dma((2, 4, 2)),
+            dma((2, 4, 2)),
+            dma((NZ - 1,)),
+            dma((NZ - 1,)),
+            dma((NZ,)),
+            dma((NZ,)),
+            dma((NZ,)),
+            dma((NZ,)),
+            dma((2, 4, 2)),
+            dma((2, 4, 2)),
+            dma((NX - 1,)),
+            dma((NX - 1,)),
+            dma((NX - 1,)),
+            dma((NX - 1,)),
+        ],
+        compiler_params=pltpu.CompilerParams(
+            collective_id=1, has_side_effects=True, vmem_limit_bytes=56 * 1024 * 1024
+        ),
+    )(rows, stream, meta, rg, ru, rd, cg, cu, cd)
 
 
 def shards(
@@ -207,49 +589,21 @@
         * lax.rsqrt(jnp.mean(stream_wide * stream_wide, axis=-1, keepdims=True) + EPSILON)
         * expert_norm_gain
     ).astype(jnp.bfloat16)
-    pieces = sent_together((common_gate_weight, common_up_weight, common_down_weight), "tp", 1, 0)
-    shared = shared_part(normed_rows, pieces[0], pieces[1], pieces[2])
-    local_experts = routed_gate_weight.shape[0]
-    experts_all = local_experts * lax.axis_size(SP)
-    top_count = routed_expert_index.shape[1]
-    capacity = 2 * row_count * top_count // experts_all
-    flat_ids = routed_expert_index.reshape(-1)
-    expert_hits = (flat_ids[:, None] == jnp.arange(experts_all, dtype=jnp.int32)[None, :]).astype(
-        jnp.int32
-    )
-    slot_ranks = jnp.sum((jnp.cumsum(expert_hits, axis=0) - 1) * expert_hits, axis=1)
-    slot_index = flat_ids * capacity + slot_ranks
-    slot_rows = (
-        jnp.full((experts_all * capacity,), row_count, jnp.int32)
-        .at[slot_index]
-        .set(jnp.arange(row_count * top_count, dtype=jnp.int32) // top_count)
-    )
-    padded = jnp.concatenate([normed_rows, jnp.zeros((1, D), jnp.bfloat16)], axis=0)
-    outgoing = padded[slot_rows].reshape(experts_all, capacity, D)
-    arrived = lax.all_to_all(outgoing, SP, split_axis=0, concat_axis=0, tiled=True)
-    sources = arrived.shape[0] // local_experts
-    grouped = arrived.reshape(sources, local_experts, arrived.shape[1], D)
-    gate_part = jnp.einsum(
-        "sekd,edf->sekf", grouped, routed_gate_weight, preferred_element_type=jnp.float32
-    )
-    lifted = jnp.einsum(
-        "sekd,edf->sekf", grouped, routed_up_weight, preferred_element_type=jnp.float32
-    )
-    hidden = (jax.nn.silu(gate_part) * lifted).astype(jnp.bfloat16)
-    result = jnp.einsum(
-        "sekf,efd->sekd", hidden, routed_down_weight, preferred_element_type=jnp.float32
-    ).astype(jnp.bfloat16)
-    returned = lax.all_to_all(
-        result.reshape(arrived.shape), SP, split_axis=0, concat_axis=0, tiled=True
-    )
-    picked = returned.reshape(experts_all * capacity, D)[slot_index]
-    routed = jnp.sum(
-        (picked.astype(jnp.float32) * routed_expert_weight.reshape(-1)[:, None]).reshape(
-            row_count, top_count, D
-        ),
-        axis=1,
-    )
-    return (stream_wide + shared + routed).astype(jnp.bfloat16)
+    meta = jnp.concatenate(
+        [routed_expert_index.T.astype(F32), routed_expert_weight.T.astype(F32)], axis=0
+    )
+    meta = jnp.pad(meta, ((0, 0), (0, 128 - row_count)))
+    return moe(
+        normed_rows,
+        stream,
+        meta,
+        routed_gate_weight[0],
+        routed_up_weight[0],
+        routed_down_weight[0],
+        common_gate_weight,
+        common_up_weight,
+        common_down_weight,
+    )
 
 
 def solution(mesh):

time: 301 us -> 218 us (0.72)
  Pallas kernels: 0 us -> 75.3 us
  blocking collectives: 95.7 us -> 28.2 us
  waiting for transfers between devices: 88.1 us -> 44.3 us
  local copies, waits for them, and re-layouts: 29.6 us -> 12.9 us
  matrix products: 19.3 us -> 6.19 us
  other arithmetic: 30.6 us -> 21.3 us
  starting transfers between devices: 22.5 us -> 15.2 us
    pallas_call x0 -> x1, Pallas kernels: none -> 75.3 us  [moe(): pl.pallas_call(moe_kernel, out_shape=jax.ShapeDtypeStruct((ROWS, D), BF16...]
    all_to_all x1 -> x0, blocking collectives: 67.1 us -> none  [shards(): lax.all_to_all(outgoing, SP, split_axis=0, concat_axis=0, tiled=True)]
    all_to_all x1 -> x0, waiting for transfers between devices: 46.8 us -> none  [shards(): lax.all_to_all(result.reshape(arrived.shape), SP, split_axis=0, concat_ax...]
    dot_general x4 -> x0, matrix products: 13.1 us -> none  [the longest x1 5.28 us: shards(): jnp.einsum('sekf,efd->sekd', hidden, routed_down_weight, preferred_elemen...]
    all_gather x2, waiting for transfers between devices: 24.1 us -> 35.1 us  [carried_in(): lax.all_gather(part.astype(kind), axis)]
    all_to_all x1, waiting for transfers between devices: 17.1 us -> 9.13 us  [sum_at_owner(): blocks = lax.all_to_all(cut_along(array, dim, size), axis, 0, 0, tiled=True)]
    all_to_all x1 -> x0, starting transfers between devices: 7.1 us -> none  [shards(): lax.all_to_all(result.reshape(arrived.shape), SP, split_axis=0, concat_ax...]
    gather x2 -> x0, local copies, waits for them, and re-layouts: 4.78 us -> none  [the longest x1 2.47 us: shards(): outgoing = padded[slot_rows].reshape(experts_all, capacity, D)]
  transfers between devices with their start and end apart: 8 -> 6, of which waited for: 3 -> 3; matrix products, arithmetic and copies ran while one was open for 16% -> 7% of each run, Pallas kernels for 0% -> 0%
where the time goes in v1:
time: 218 us; the launch traced here: 217 us
  Pallas kernels  75.3 us (35%)
  waiting for transfers between devices  44.3 us (20%)
  blocking collectives  28.2 us (13%)
  other arithmetic  21.3 us (10%)
  starting transfers between devices  15.2 us (7%)
  between operations  13.9 us (6%)
  local copies, waits for them, and re-layouts  12.9 us (6%)
  matrix products  6.19 us (3%)
    pallas_call x1, Pallas kernels, moe(): pl.pallas_call(moe_kernel, out_shape=jax.ShapeDtypeStruct((ROWS, D), BF16...  75.3 us
    all_gather x2, waiting for transfers between devices, carried_in(): lax.all_gather(part.astype(kind), axis)  35.1 us
    all_gather x4, blocking collectives, carried_in(): lax.all_gather(part.astype(kind), axis)  28.2 us
    ppermute x3, starting transfers between devices, shifted(): lax.ppermute(value, axis, [(source, source + steps) for source in range(f...  11.1 us
    all_to_all x1, waiting for transfers between devices, sum_at_owner(): blocks = lax.all_to_all(cut_along(array, dim, size), axis, 0, 0, tiled=True)  9.13 us
    mul x3, other arithmetic, short_conv(): return jax.nn.silu(totals)  5.43 us
    unnamed x46, local copies, waits for them, and re-layouts  4.91 us
  transfers between devices with their start and end apart: 6, of which 3 were waited for; matrix products, arithmetic and copies ran while one was open for 7% of the time, Pallas kernels for 0%

profile of v1, /device:TPU:1, one launch (start us, length us, event | category | flops | bytes accessed | tf_op | source)
XLA Modules:
  0.0 217.3 jit_solution(9519294270940563431)
XLA Ops:
  6.5 0.8 slice.160
  7.3 0.2 copy.49
  7.5 4.6 %collective-permute-start = (bf16[3,1024]{0,1:T(8,128)(2,1)S(1)}, bf16[3,1024]{0,1:T(8,128)(2,1)S(1)}, u32[]{:S(2)}, u32[]{:S(2)}) collective-permute-start(bf16[3,1024]{0,1:T(8,128)(2,1)S(1)} %copy.49), channel_id=1, source_target_pairs={{0,4},{4,8},{8,12},{12,16},{16,20},{20,24},{24,28},{28,32},{32,36}... | collective-permute-start | bytes 18440 | tf_op jit(solution)/shard_map/ppermute | solution.py:24
  12.1 0.7 slice.176
  12.8 1.9 collective-permute-start.2
  14.8 0.9 slice_convert_fusion.3
  15.6 0.7 exponential_negate_fusion
  16.3 0.8 compare_select_fusion
  17.1 0.3 copy.54
  17.4 0.1 fusion.75
  17.5 1.1 fusion.74
  18.7 0.2 copy.50
  18.9 0.2 copy.58
  19.2 0.4 divide_multiply_fusion.1
  19.5 0.1 reshape.206
  19.6 0.7 copy-done.11
  20.3 2.5 %divide_multiply_fusion = f32[256,1024]{0,1:T(8,128)S(1)} fusion(bf16[256,1024]{0,1:T(8,128)(2,1)S(1)} %copy.50, bf16[3,1024]{0,1:T(8,128)(2,1)} %copy-done.11, f32[1024]{0:T(1024)S(1)} %bitcast.201, f32[1024]{0:T(1024)S(1)} %bitcast.202, f32[1024]{0:T(1024)S(1)} %bitcast.200, f32[1024]{0:T(1024)S(1)} %bitcast.199), kind=kLoop, calls=%fused_computation.32 | loop fusion | flops 6291456 | bytes 1595392 | tf_op jit(solution)/shard_map/jit(silu)/mul | solution.py:81
  22.8 0.5 reshape.204
  23.3 1.5 broadcast_multiply_fusion
  24.8 0.3 fusion.18
  25.1 2.0 while.17
  25.1 0.9 bitcast_dynamic-update-slice_fusion.4
  26.0 0.1 bitcast_add_fusion.2
  26.2 0.9 bitcast_dynamic-update-slice_fusion.4
  27.0 0.1 bitcast_add_fusion.2
  27.2 2.0 all-gather.2
  29.1 8.0 %all_gather.30 = bf16[4,4,4]{2,1,0:T(4,128)(2,1)S(1)} all-gather(bf16[1,4,4]{2,1,0:T(4,128)(2,1)S(1)} %fusion.62), channel_id=1, replica_groups=mesh['sp_0'=8,'sp_1'=4,'sp_2'=2,'tp'=4] {'sp_1'}, dimensions={0}, use_global_device_ids=true | all-gather | bytes 160 | tf_op jit(solution)/shard_map/all_gather | solution.py:39
  37.2 4.3 %all-gather.1 = bf16[8,4,64,128]{3,2,1,0:T(8,128)(2,1)S(1)} all-gather(bf16[4,4,64,128]{3,2,1,0:T(8,128)(2,1)S(1)} %convert_element_type.413), channel_id=3, replica_groups=mesh['sp_0'=8,'sp_1'=4,'sp_2'=2,'tp'=4] {'sp_2'}, dimensions={0}, use_global_device_ids=true | all-gather | bytes 786432 | tf_op jit(solution)/shard_map/all_gather | solution.py:39
  41.5 1.0 fusion.47
  42.4 0.0 all-gather.6.cloned.1.call-update
  42.4 0.0 all-gather.8.cloned.1.call-start
  42.5 24.1 %all-gather.6.cloned.1.call-done = bf16[4,4,4,64,128]{4,3,2,1,0:T(8,128)(2,1)} async-done(((bf16[1,4,4,64,128]{4,3,2,1,0:T(8,128)(2,1)}), bf16[4,4,4,64,128]{4,3,2,1,0:T(8,128)(2,1)}) %all-gather.6.cloned.1.call-update) | async-done | bytes 1048592 | tf_op jit(solution)/shard_map/all_gather | solution.py:39
  66.6 2.3 %fusion.45 = bf16[1,4,4,64,128]{4,3,2,1,0:T(8,128)(2,1)} fusion(f32[4,4]{1,0:T(4,128)S(1)} %get-tuple-element.110, f32[4,4]{1,0:T(4,128)S(1)} %get-tuple-element.113, f32[4,4]{1,0:T(4,128)S(1)} %get-tuple-element.112, f32[4,4]{1,0:T(4,128)S(1)} %get-tuple-element.111, bf16[4,4,4,64,128]{4,3,2,1,0:T(8,128)(2,1)} %all-gather.6.cloned.1.call-done), kind=kLoop, calls=%fused_computation.62 | loop fusion | flops 1572864 | bytes 1310976 | tf_op jit(solution)/shard_map/convert_element_type | solution.py:39
  68.9 0.0 all-gather.8.cloned.1.call-update
  68.9 0.7 slice.168
  69.6 4.6 %collective-permute-start.1 = (bf16[3,512]{1,0:T(4,128)(2,1)S(1)}, bf16[3,512]{1,0:T(4,128)(2,1)S(1)}, u32[]{:S(2)}, u32[]{:S(2)}) collective-permute-start(bf16[3,512]{1,0:T(4,128)(2,1)S(1)} %slice.168), channel_id=1, source_target_pairs={{0,4},{4,8},{8,12},{12,16},{16,20},{20,24},{24,28},{28,32},{32,36}... | collective-permute-start | bytes 9224 | tf_op jit(solution)/shard_map/ppermute | solution.py:24
  74.3 0.2 copy.62
  74.5 0.2 copy.55
  74.7 0.2 copy.65
  74.9 1.5 reshape.235
  76.4 0.1 mul.614
  76.5 2.6 %divide_multiply_fusion.2 = bf16[256,512]{1,0:T(8,128)(2,1)} fusion(bf16[256,512]{1,0:T(8,128)(2,1)} %param.29, bf16[3,512]{1,0:T(4,128)(2,1)S(1)} %collective-permute-done.1, f32[512]{0:T(512)S(1)} %bitcast.205, f32[512]{0:T(512)S(1)} %bitcast.206, f32[512]{0:T(512)S(1)} %bitcast.204, f32[512]{0:T(512)S(1)} %bitcast.203), kind=kLoop, calls=%fused_computation.70 | loop fusion | flops 3276800 | bytes 535552 | tf_op jit(solution)/shard_map/jit(silu)/mul | solution.py:81
  79.1 1.7 reshape.205
  80.8 2.0 fusion.41
  82.9 13.9 %all_gather.31 = bf16[8,4,4]{2,1,0:T(4,128)(2,1)S(1)} all-gather(bf16[1,4,4]{2,1,0:T(4,128)(2,1)S(1)} %fusion.59), channel_id=1, replica_groups=mesh['sp_0'=8,'sp_1'=4,'sp_2'=2,'tp'=4] {'sp_0'}, dimensions={0}, use_global_device_ids=true | all-gather | bytes 288 | tf_op jit(solution)/shard_map/all_gather | solution.py:39
  96.8 11.0 %all-gather.8.cloned.1.call-done = bf16[8,4,4,64,128]{4,3,2,1,0:T(8,128)(2,1)} async-done(((bf16[1,4,4,64,128]{4,3,2,1,0:T(8,128)(2,1)}), bf16[8,4,4,64,128]{4,3,2,1,0:T(8,128)(2,1)}) %all-gather.8.cloned.1.call-update) | async-done | bytes 2097168 | tf_op jit(solution)/shard_map/all_gather | solution.py:39
  107.8 3.3 %fusion.38 = f32[4,4,64,128]{3,2,1,0:T(8,128)S(1)} fusion(bf16[8,4,4,64,128]{4,3,2,1,0:T(8,128)(2,1)} %all-gather.8.cloned.1.call-done, f32[4,4]{1,0:T(4,128)S(1)} %get-tuple-element.92, f32[4,4]{1,0:T(4,128)S(1)} %get-tuple-element.122, f32[4,4]{1,0:T(4,128)S(1)} %fusion.70, f32[4,4]{1,0:T(4,128)S(1)} %get-tuple-element.110, ...), kind=kLoop, calls=%fused_computation.53 | loop fusion | flops 7471104 | bytes 4195342 | tf_op jit(solution)/shard_map/mul | solution.py:557
  111.2 0.4 fusion.11
  111.6 0.8 copy-done.4
  112.4 0.1 copy-done.8
  112.5 0.2 copy-done.9
  112.7 1.3 multiply_reduce_fusion
  114.0 0.8 copy.64
  114.8 0.4 fusion.17
  115.2 0.9 copy-done.20
  116.1 2.3 %convolution_convert_fusion = bf16[256,2048]{1,0:T(8,128)(2,1)} fusion(bf16[256,1024]{0,1:T(8,128)(2,1)S(1)} %fusion.17, bf16[1024,2048]{1,0:T(8,128)(2,1)S(1)} %copy-done.20), kind=kOutput, calls=%fused_computation.5 | convolution fusion | flops 1074266112 | bytes 5767168 | tf_op jit(solution)/shard_map/dot_general | solution.py:579
  118.4 4.1 %all-to-all-start = ((bf16[4,64,2048]{2,1,0:T(8,128)(2,1)}), bf16[4,64,2048]{2,1,0:T(8,128)(2,1)S(1)}, u32[]{:S(2)}, u32[]{:S(2)}) async-start(bf16[4,64,2048]{2,1,0:T(8,128)(2,1)} %bitcast.40), calls=%async_computation | async-start | bytes 2097152 | tf_op jit(solution)/shard_map/all_to_all | solution.py:62
  122.5 0.6 select_maximum_fusion.meta
  123.1 9.1 %all-to-all-done = bf16[4,64,2048]{2,1,0:T(8,128)(2,1)S(1)} async-done(((bf16[4,64,2048]{2,1,0:T(8,128)(2,1)}), bf16[4,64,2048]{2,1,0:T(8,128)(2,1)S(1)}, u32[]{:S(2)}, u32[]{:S(2)}) %all-to-all-start) | async-done | bytes 1048608 | tf_op jit(solution)/shard_map/all_to_all | solution.py:62
  132.3 0.2 convert_reduce_fusion
  132.4 0.2 fusion.28
  132.6 0.8 fusion.30.rows
  133.5 75.3 %shard_map.217 = bf16[64,2048]{1,0:T(8,128)(2,1)} custom-call(bf16[64,2048]{1,0:T(8,128)(2,1)} %fusion.30.rows, bf16[64,2048]{1,0:T(8,128)(2,1)} %copy-done.1, f32[8,128]{1,0:T(8,128)} %select_maximum_fusion.meta, bf16[2048,256]{1,0:T(8,128)(2,1)} %bitcast.194, bf16[2048,256]{1,0:T(8,128)(2,1)} %bitcast.195, bf16[256,2048]{1,0:T(8,128)(2,1)} %bitcast.196, ...), custom_call_target="tpu_custom_call" | custom-call | tf_op jit(solution)/shard_map/pallas_call | solution.py:429
  208.8 1.7 copy.116
  (70 shorter events, 0.3 us)
Async XLA Ops:
  6.5 12.1 %copy-start.6 = (bf16[256,1024]{1,0:T(8,128)(2,1)S(1)}, bf16[256,1024]{1,0:T(8,128)(2,1)}, u32[]{:S(2)}) copy-start(bf16[256,1024]{1,0:T(8,128)(2,1)} %param.27) | copy-start | bytes 1572868
  6.5 12.1 %copy-start.13 = (bf16[4,512]{1,0:T(4,128)(2,1)S(1)}, bf16[4,512]{1,0:T(4,128)(2,1)}, u32[]{:S(2)}) copy-start(bf16[4,512]{1,0:T(4,128)(2,1)} %param.33) | copy-start | bytes 12292
  6.5 60.1 %all-gather.6.cloned.1.call-start = ((), (), s32[]{:S(2)}) async-start(), calls=%async_computation.1 | async-start | bytes 1310720 | tf_op jit(solution)/shard_map/all_gather | solution.py:39
  7.5 12.1 %collective-permute-start = (bf16[3,1024]{0,1:T(8,128)(2,1)S(1)}, bf16[3,1024]{0,1:T(8,128)(2,1)S(1)}, u32[]{:S(2)}, u32[]{:S(2)}) collective-permute-start(bf16[3,1024]{0,1:T(8,128)(2,1)S(1)} %copy.49), channel_id=1, source_target_pairs={{0,4},{4,8},{8,12},{12,16},{16,20},{20,24},{24,28},{28,32},{32,36}... | collective-permute-start | bytes 18440 | tf_op jit(solution)/shard_map/ppermute | solution.py:24
  12.8 6.3 %collective-permute-start.2 = (bf16[3,512]{1,0:T(4,128)(2,1)S(1)}, bf16[3,512]{1,0:T(4,128)(2,1)S(1)}, u32[]{:S(2)}, u32[]{:S(2)}) collective-permute-start(bf16[3,512]{1,0:T(4,128)(2,1)S(1)} %slice.176), channel_id=1, source_target_pairs={{0,4},{4,8},{8,12},{12,16},{16,20},{20,24},{24,28},{28,32},{32,36}... | collective-permute-start | bytes 9224 | tf_op jit(solution)/shard_map/ppermute | solution.py:24
  17.4 1.8 copy-start.10
  19.6 0.7 copy-start.11
  37.1 37.1 %copy-start.14 = (bf16[4,512]{1,0:T(4,128)(2,1)S(1)}, bf16[4,512]{1,0:T(4,128)(2,1)}, u32[]{:S(2)}) copy-start(bf16[4,512]{1,0:T(4,128)(2,1)} %param.34) | copy-start | bytes 12292
  37.1 37.2 %copy-start.3 = (f32[2,128,4,4]{3,2,1,0:T(4,128)S(1)}, f32[2,128,4,4]{3,2,1,0:T(4,128)}, u32[]{:S(2)}) copy-start(f32[2,128,4,4]{3,2,1,0:T(4,128)} %get-tuple-element.95) | copy-start | bytes 49156
  41.5 33.2 %copy-start.7 = (bf16[256,1024]{1,0:T(8,128)(2,1)S(1)}, bf16[256,1024]{1,0:T(8,128)(2,1)}, u32[]{:S(2)}) copy-start(bf16[256,1024]{1,0:T(8,128)(2,1)} %param.26) | copy-start | bytes 1572868
  42.4 65.4 %all-gather.8.cloned.1.call-start = ((), (), s32[]{:S(2)}) async-start(), calls=%async_computation.2 | async-start | bytes 2359296 | tf_op jit(solution)/shard_map/all_gather | solution.py:39
  68.9 7.5 %copy-start.19 = (f32[16]{0:T(128)S(1)}, f32[16]{0:T(128)}, u32[]{:S(2)}) copy-start(f32[16]{0:T(128)} %param.36) | copy-start | bytes 196
  69.6 6.8 %collective-permute-start.1 = (bf16[3,512]{1,0:T(4,128)(2,1)S(1)}, bf16[3,512]{1,0:T(4,128)(2,1)S(1)}, u32[]{:S(2)}, u32[]{:S(2)}) collective-permute-start(bf16[3,512]{1,0:T(4,128)(2,1)S(1)} %slice.168), channel_id=1, source_target_pairs={{0,4},{4,8},{8,12},{12,16},{16,20},{20,24},{24,28},{28,32},{32,36}... | collective-permute-start | bytes 9224 | tf_op jit(solution)/shard_map/ppermute | solution.py:24
  74.9 32.9 %copy-start = (bf16[4,4,4,64,128]{4,3,2,1,0:T(8,128)(2,1)S(1)}, bf16[4,4,4,64,128]{4,3,2,1,0:T(8,128)(2,1)}, u32[]{:S(2)}) copy-start(bf16[4,4,4,64,128]{4,3,2,1,0:T(8,128)(2,1)} %all-gather.6.cloned.1.call-done) | copy-start | bytes 3145732
  107.8 3.4 %copy-start.2 = (bf16[2,128,4,128]{3,2,1,0:T(4,128)(2,1)S(1)}, bf16[2,128,4,128]{3,2,1,0:T(4,128)(2,1)}, u32[]{:S(2)}) copy-start(bf16[2,128,4,128]{3,2,1,0:T(4,128)(2,1)} %reshape.205) | copy-start | bytes 786436
  107.8 3.4 %copy-start.5 = (f32[2,4,4,64,128]{4,3,2,1,0:T(8,128)S(1)}, f32[2,4,4,64,128]{4,3,2,1,0:T(8,128)}, u32[]{:S(2)}) copy-start(f32[2,4,4,64,128]{4,3,2,1,0:T(8,128)} %get-tuple-element.45) | copy-start | bytes 3145732
  111.2 1.2 copy-start.4
  111.2 1.3 copy-start.8
  111.2 1.5 copy-start.9
  113.9 0.9 copy-start.16
  114.0 2.2 %copy-start.20 = (bf16[1024,2048]{1,0:T(8,128)(2,1)S(1)}, bf16[1024,2048]{1,0:T(8,128)(2,1)}, u32[]{:S(2)}) copy-start(bf16[1024,2048]{1,0:T(8,128)(2,1)} %param.38) | copy-start | bytes 12582916
  118.4 4.1 %copy-start.17 = (s32[64,4]{0,1:T(4,128)S(1)}, s32[64,4]{0,1:T(4,128)}, u32[]{:S(2)}) copy-start(s32[64,4]{0,1:T(4,128)} %param.40) | copy-start | bytes 3076
  118.4 4.1 %copy-start.18 = (f32[64,4]{0,1:T(4,128)S(1)}, f32[64,4]{0,1:T(4,128)}, u32[]{:S(2)}) copy-start(f32[64,4]{0,1:T(4,128)} %param.41) | copy-start | bytes 3076
  118.4 14.0 %copy-start.12 = (bf16[64,2048]{1,0:T(8,128)(2,1)S(1)}, bf16[64,2048]{1,0:T(8,128)(2,1)}, u32[]{:S(2)}) copy-start(bf16[64,2048]{1,0:T(8,128)(2,1)} %param.25) | copy-start | bytes 786436
  118.4 14.2 %copy-start.15 = (f32[2048]{0:T(1024)S(1)}, f32[2048]{0:T(1024)}, u32[]{:S(2)}) copy-start(f32[2048]{0:T(1024)} %param.39) | copy-start | bytes 24580
  118.4 13.9 %all-to-all-start = ((bf16[4,64,2048]{2,1,0:T(8,128)(2,1)}), bf16[4,64,2048]{2,1,0:T(8,128)(2,1)S(1)}, u32[]{:S(2)}, u32[]{:S(2)}) async-start(bf16[4,64,2048]{2,1,0:T(8,128)(2,1)} %bitcast.40), calls=%async_computation | async-start | bytes 2097152 | tf_op jit(solution)/shard_map/all_to_all | solution.py:62
  132.6 0.9 copy-start.1
Sparse Core Ops, SparseCore 0:
  42.6 24.0 all-gather.5
  69.0 38.7 all-gather.7

commit v2 on v1

--- a/solution.py
+++ b/solution.py
@@ -10,86 +10,11 @@
 HEAD_DIM = 64
 STATE = 128
 CONV = 4
-BLOCK_POSITIONS = 128
 SP = ("sp_0", "sp_1", "sp_2")
 SP_TP = ("sp_0", "sp_1", "sp_2", "tp")
 
 
 EPSILON = 1e-06
-
-
-def shifted(value, axis, steps):
-    count = lax.axis_size(axis)
-    first, last = (max(0, -steps), min(count, count - steps))
-    return lax.ppermute(value, axis, [(source, source + steps) for source in range(first, last)])
-
-
-def filled_with(array, identity):
-    return jax.tree.map(
-        lambda part, zero: jnp.zeros_like(part) + jnp.asarray(zero, part.dtype), array, identity
-    )
-
-
-def carried_in(array, axes, combine, identity):
-    before = start = filled_with(array, identity)
-    total = array
-    for axis in reversed(axes):
-        size, index = (lax.axis_size(axis), lax.axis_index(axis))
-        pieces = jax.tree.map(
-            lambda part, kind: lax.all_gather(part.astype(kind), axis),
-            total,
-            (jnp.bfloat16, jnp.bfloat16),
-        )
-        inside, total = (start, start)
-        for k in range(size):
-            passed = k < index
-            total = combine(
-                total, jax.tree.map(lambda part, own: part[k].astype(own.dtype), pieces, array)
-            )
-            inside = jax.tree.map(lambda new, old: jnp.where(passed, new, old), total, inside)
-        before = combine(inside, before)
-    return before
-
-
-def cut_along(array, dim, size):
-    lengths = array.shape
-    blocks = array.reshape(*lengths[:dim], size, lengths[dim] // size, *lengths[dim + 1 :])
-    return jnp.moveaxis(blocks, dim, 0)
-
-
-def sum_at_owner(array, axis, dim):
-    size = lax.axis_size(axis)
-    blocks = lax.all_to_all(cut_along(array, dim, size), axis, 0, 0, tiled=True)
-    return jnp.sum(blocks.astype(jnp.float32), axis=0)
-
-
-def sent_together(arrays, axis, dim, along):
-    widths = [a.shape[along] for a in arrays]
-    both = jnp.concatenate(arrays, axis=along)
-    filled = lax.all_gather(both, axis, axis=dim, tiled=True)
-    return tuple(jnp.split(filled, [sum(widths[:k]) for k in range(1, len(widths))], axis=along))
-
-
-def short_conv(inputs, rim_rows, weights):
-    length = inputs.shape[0]
-    extended = jnp.concatenate([rim_rows, inputs], axis=0)
-    totals = jnp.zeros(inputs.shape, jnp.float32)
-    for tap_index in range(CONV):
-        totals = totals + extended[tap_index : tap_index + length].astype(jnp.float32) * weights[
-            tap_index
-        ].astype(jnp.float32)
-    return jax.nn.silu(totals)
-
-
-def shared_part(rows, gate_piece, up_piece, down_piece):
-    gate_part = jnp.dot(rows, gate_piece, preferred_element_type=jnp.float32)
-    lifted = jnp.dot(rows, up_piece, preferred_element_type=jnp.float32)
-    hidden = (jax.nn.silu(gate_part) * lifted).astype(jnp.bfloat16)
-    return jnp.einsum("rc,dc->rd", hidden, down_piece, preferred_element_type=jnp.float32)
-
-
-def join_states(earlier, later):
-    return (earlier[0] * later[0], later[0][..., None, None] * earlier[1] + later[1])
 
 
 MESH = pl.DeviceIdType.MESH
@@ -472,6 +397,485 @@
     )(rows, stream, meta, rg, ru, rd, cg, cu, cd)
 
 
+LENGTH = 256
+HEADS_HERE = 16
+GROUPS_HERE = 4
+WIDE = 256
+PAIRS = 8
+RIM = 16
+COLS = 512
+
+
+def split_terms(value, count):
+    terms = []
+    for _ in range(count):
+        term = value.astype(BF16)
+        terms.append(term)
+        value = value - term.astype(F32)
+    return terms
+
+
+def mixer_kernel(
+    residual,
+    gate_hbm,
+    value_hbm,
+    state_hbm,
+    read_hbm,
+    step_hbm,
+    extra_hbm,
+    value_taps,
+    state_taps,
+    read_taps,
+    rates,
+    direct,
+    head_gain,
+    w_hbm,
+    expert_gain,
+    stream_out,
+    rows_out,
+    gate_in,
+    value_in,
+    state_raw,
+    read_raw,
+    step_in,
+    extra_in,
+    w_out,
+    value_rim,
+    state_rim,
+    read_rim,
+    ext,
+    values,
+    weighted,
+    state_in,
+    readout,
+    mixed,
+    heads_out,
+    own,
+    own_send,
+    other,
+    chips,
+    y_before,
+    planes,
+    z_before,
+    logs,
+    plane_logs,
+    weights_ref,
+    mix_send,
+    mix_recv,
+    load_sem,
+    rim_s,
+    rim_r,
+    log_s,
+    log_r,
+    pair_s,
+    pair_r,
+    chip_s,
+    chip_r,
+    plog_s,
+    plog_r,
+    slice_s,
+    slice_r,
+    yo_s,
+    yo_r,
+    zb_s,
+    zb_r,
+    mix_s,
+    mix_r,
+):
+    z, y, c, x = place()
+    me = y * NC + c
+    partner = device(z, y, 1 - c, x)
+    y_peers = [device(z, lax.rem(y + d, NY), c, x) for d in range(1, NY)]
+    z_peers = [device(lax.rem(z + d, NZ), y, c, x) for d in range(1, NZ)]
+    x_peers = [device(z, y, c, lax.rem(x + d, NX)) for d in range(1, NX)]
+    plane_peers = []
+    for dy in (1, 3, 2, 0):
+        for dc in range(NC):
+            if dy or dc:
+                away = dy * NC + dc
+                back = ((NY - dy) % NY) * NC + dc
+                target = device(z, lax.rem(y + dy, NY), lax.rem(c + dc, NC), x)
+                plane_peers.append((away - 1, back - 1, target))
+
+    def along(step):
+        flat = lax.rem((z * NY + y) * NC + c + step + NZ * NY * NC, NZ * NY * NC)
+        return device(flat // (NY * NC), lax.rem(flat // NC, NY), lax.rem(flat, NC), x)
+
+    loads = [
+        pltpu.make_async_copy(far, near, load_sem.at[k])
+        for k, (far, near) in enumerate(
+            (
+                (value_hbm, value_in),
+                (state_hbm, state_raw),
+                (read_hbm, read_raw),
+                (step_hbm, step_in),
+                (extra_hbm, extra_in),
+                (gate_hbm, gate_in),
+                (w_hbm, w_out),
+            )
+        )
+    ]
+    for load in loads:
+        load.start()
+    greet(
+        [target for _, _, target in plane_peers]
+        + z_peers
+        + x_peers
+        + [along(1), along(-1)]
+    )
+    started = []
+
+    def send(src, dst, send_sem, recv_sem, target):
+        copy = remote(src, dst, send_sem, recv_sem, target)
+        copy.start()
+        started.append(copy)
+
+    for k in range(3):
+        loads[k].wait()
+    for k, (near, rim) in enumerate(
+        ((value_in, value_rim), (state_raw, state_rim), (read_raw, read_rim))
+    ):
+        send(near.at[pl.ds(LENGTH - RIM, RIM)], rim, rim_s.at[k], rim_r.at[k], along(1))
+
+    loads[3].wait()
+    loads[4].wait()
+    sizes = jax.nn.softplus(step_in[...])
+    log_decay = sizes * (-jnp.exp(rates[...])) + extra_in[...]
+    early = lax.broadcasted_iota(jnp.int32, (LENGTH, LENGTH), 0)
+    late = lax.broadcasted_iota(jnp.int32, (LENGTH, LENGTH), 1)
+    causal = early >= late
+    lower = jnp.where(causal, 1.0, 0.0).astype(BF16)
+    upper = jnp.where(early <= late, 1.0, 0.0).astype(BF16)
+    cumulative = jnp.zeros((LENGTH, HEADS_HERE), F32)
+    by_head = jnp.zeros((HEADS_HERE, LENGTH), F32)
+    for term in split_terms(log_decay, 3):
+        cumulative = cumulative + jnp.dot(lower, term, preferred_element_type=F32)
+        by_head = by_head + lax.dot_general(
+            term, upper, (((0,), (0,)), ((), ())), preferred_element_type=F32
+        )
+    head_row = lax.broadcasted_iota(jnp.int32, (HEADS_HERE, WIDE), 0)
+    lane_head = lax.broadcasted_iota(jnp.int32, (HEADS_HERE, WIDE), 1) // HEAD_DIM
+    spreads = [
+        jnp.where(head_row == lane_head + 4 * g, 1.0, 0.0).astype(BF16) for g in range(GROUPS_HERE)
+    ]
+
+    def spread(value, g, count):
+        wide = jnp.zeros((value.shape[0], WIDE), F32)
+        for term in split_terms(value, count):
+            wide = wide + jnp.dot(term, spreads[g], preferred_element_type=F32)
+        return wide
+
+    total = cumulative[LENGTH - 1 :, :]
+    total_rows = jnp.broadcast_to(total, (8, HEADS_HERE))
+    for g in range(GROUPS_HERE):
+        wide = spread(total_rows, g, 3)
+        for k in range(2):
+            logs[me, pl.ds(2 * g + k, 1)] = wide[:1, k * 128 : (k + 1) * 128]
+    for away, back, target in plane_peers:
+        send(logs.at[me], logs.at[me], log_s.at[away], log_r.at[back], target)
+
+    first = jnp.where(z + y + c == 0, 0.0, 1.0)
+
+    def convolved(near, rim, taps, lo):
+        ext[:8] = rim[8:16, lo : lo + WIDE].astype(F32) * first
+        ext[8:] = near[:, lo : lo + WIDE].astype(F32)
+        weights = taps[:, lo : lo + WIDE].astype(F32)
+        sums = ext[5 : 5 + LENGTH] * weights[0:1]
+        for k in range(1, CONV):
+            sums = sums + ext[5 + k : 5 + k + LENGTH] * weights[k : k + 1]
+        return jax.nn.silu(sums)
+
+    arrive(value_rim, rim_r.at[0])
+    arrive(state_rim, rim_r.at[1])
+    for lo in range(0, GROUPS_HERE * STATE, WIDE):
+        state_in[:, lo : lo + WIDE] = convolved(state_raw, state_rim, state_taps, lo).astype(BF16)
+    ends = jnp.exp(total - cumulative) * sizes
+    for g in range(GROUPS_HERE):
+        lo = g * WIDE
+        value = convolved(value_in, value_rim, value_taps, lo)
+        values[:, lo : lo + WIDE] = value
+        weighted[:, lo : lo + WIDE] = (value * spread(sizes, g, 2)).astype(BF16)
+        ending = (value * spread(ends, g, 2)).astype(BF16)
+        fresh = lax.dot_general(
+            state_in[:, g * STATE : (g + 1) * STATE],
+            ending,
+            (((0,), (0,)), ((), ())),
+            preferred_element_type=F32,
+        )
+        for k in range(2):
+            piece = fresh[:, k * 128 : (k + 1) * 128]
+            own[2 * g + k] = piece
+            own_send[2 * g + k] = piece.astype(BF16)
+    theirs, mine = (1 - c) * 4, c * 4
+    send(own_send.at[pl.ds(theirs, 4)], other.at[pl.ds(theirs, 4)], pair_s.at[0], pair_r.at[0], partner)
+    send(own_send.at[pl.ds(mine, 4)], other.at[pl.ds(mine, 4)], pair_s.at[1], pair_r.at[1], partner)
+
+    for away, back, target in plane_peers:
+        arrive(logs.at[0], log_r.at[away])
+    chip_logs = [logs[2 * k] + logs[2 * k + 1] for k in range(NY)]
+    plane_log = chip_logs[0] + chip_logs[1] + chip_logs[2] + chip_logs[3]
+    plane_logs[z] = plane_log
+    for d in range(1, NZ):
+        send(plane_logs.at[z], plane_logs.at[z], plog_s.at[d - 1], plog_r.at[NZ - d - 1], z_peers[d - 1])
+    log_even, log_odd = logs[y * NC], logs[y * NC + 1]
+    keep_odd = jnp.exp(log_odd)
+    one = jnp.ones((PAIRS, 128), F32)
+    weights_ref[0] = jnp.where(c == 0, keep_odd, one)
+    weights_ref[1] = jnp.where(c == 0, one, keep_odd)
+    for k in range(NY):
+        weights_ref[2 + k] = jnp.exp(chip_logs[k])
+
+    arrive(read_rim, rim_r.at[2])
+    for lo in range(0, GROUPS_HERE * STATE, WIDE):
+        readout[:, lo : lo + WIDE] = convolved(read_raw, read_rim, read_taps, lo).astype(BF16)
+
+    arrive(other.at[pl.ds(0, 4)], pair_r.at[0])
+    for j in range(4):
+        pair = mine + j
+        chips[y, j] = (
+            own[pair] * weights_ref[0, pl.ds(pair, 1)]
+            + other[pair].astype(F32) * weights_ref[1, pl.ds(pair, 1)]
+        ).astype(BF16)
+    for d in range(1, NY):
+        send(chips.at[y], chips.at[y], chip_s.at[d - 1], chip_r.at[NY - d - 1], y_peers[d - 1])
+
+    def within(g):
+        scores = lax.dot_general(
+            readout[:, g * STATE : (g + 1) * STATE],
+            state_in[:, g * STATE : (g + 1) * STATE],
+            (((1,), (1,)), ((), ())),
+            preferred_element_type=F32,
+        )
+        scores = jnp.where(causal, scores, 0.0)
+        group_values = weighted[:, g * WIDE : (g + 1) * WIDE]
+        lane = lax.broadcasted_iota(jnp.int32, (LENGTH, WIDE), 1) // HEAD_DIM
+        result = jnp.zeros((LENGTH, WIDE), F32)
+        for r in range(4):
+            h = 4 * g + r
+            span = cumulative[:, h : h + 1] - by_head[h : h + 1, :]
+            decay = jnp.exp(jnp.where(causal, span, -jnp.inf))
+            chosen = jnp.where(lane == r, group_values, jnp.zeros_like(group_values))
+            result = result + jnp.dot(
+                (scores * decay).astype(BF16), chosen, preferred_element_type=F32
+            )
+        mixed[:, g * WIDE : (g + 1) * WIDE] = result
+
+    within(0)
+    within(1)
+
+    for d in range(1, NY):
+        arrive(chips.at[0], chip_r.at[d - 1])
+    mine_pair = mine + y
+    whole = jnp.zeros((STATE, 128), F32)
+    for k in range(NY):
+        whole = whole * weights_ref[2 + k, pl.ds(mine_pair, 1)] + chips[k, y].astype(F32)
+    planes[z] = whole.astype(BF16)
+    for d in range(1, NZ):
+        send(planes.at[z], planes.at[z], slice_s.at[d - 1], slice_r.at[NZ - d - 1], z_peers[d - 1])
+    for j in range(4):
+        pair = mine + j
+        carried = jnp.zeros((STATE, 128), F32)
+        for k in range(NY - 1):
+            joined = carried * weights_ref[2 + k, pl.ds(pair, 1)] + chips[k, j].astype(F32)
+            carried = jnp.where(k < y, joined, carried)
+        y_before[pair] = carried.astype(BF16)
+    send(y_before.at[pl.ds(mine, 4)], y_before.at[pl.ds(mine, 4)], yo_s, yo_r, partner)
+
+    within(2)
+    within(3)
+
+    for d in range(1, NZ):
+        arrive(plane_logs.at[0], plog_r.at[d - 1])
+    for k in range(NZ - 1):
+        weights_ref[6 + k] = jnp.exp(plane_logs[k])
+    for d in range(1, NZ):
+        arrive(planes.at[0], slice_r.at[d - 1])
+    carried = jnp.zeros((STATE, 128), F32)
+    for k in range(NZ - 1):
+        joined = carried * weights_ref[6 + k, pl.ds(mine_pair, 1)] + planes[k].astype(F32)
+        carried = jnp.where(k < z, joined, carried)
+    z_before[mine_pair] = carried.astype(BF16)
+    for away, back, target in plane_peers:
+        send(
+            z_before.at[mine_pair], z_before.at[mine_pair], zb_s.at[away], zb_r.at[back], target
+        )
+
+    loads[5].wait()
+    direct_rows = jnp.broadcast_to(direct[...], (8, HEADS_HERE))
+    for g in range(GROUPS_HERE):
+        at = slice(g * WIDE, (g + 1) * WIDE)
+        mixed[:, at] = mixed[:, at] + values[:, at] * spread(direct_rows, g, 3)[:1]
+        gate = gate_in[:, at].astype(F32)
+        values[:, at] = jax.nn.silu(gate)
+    from_start = jnp.exp(cumulative)
+    since = jnp.zeros((PAIRS, 128), F32)
+    for k in range(NY - 1):
+        since = since + jnp.where(k < y, chip_logs[k], jnp.zeros_like(since))
+    plane_keep = jnp.exp(since)
+    core_keep = jnp.exp(log_even)
+    lane_a = lax.broadcasted_iota(jnp.int32, (WIDE, WIDE), 0) // HEAD_DIM
+    lane_b = lax.broadcasted_iota(jnp.int32, (WIDE, WIDE), 1) // HEAD_DIM
+    same_head = jnp.where(lane_a == lane_b, 1.0, 0.0).astype(BF16)
+
+    arrive(y_before.at[pl.ds(0, 4)], yo_r)
+    arrive(other.at[pl.ds(0, 4)], pair_r.at[1])
+    for away, back, target in plane_peers:
+        arrive(z_before.at[0], zb_r.at[away])
+    for g in range(GROUPS_HERE):
+        at = slice(g * WIDE, (g + 1) * WIDE)
+        halves = []
+        for k in range(2):
+            pair = 2 * g + k
+            state = z_before[pair].astype(F32) * plane_keep[pair : pair + 1]
+            state = state + y_before[pair].astype(F32)
+            joined = state * core_keep[pair : pair + 1] + other[pair].astype(F32)
+            halves.append(jnp.where(c == 1, joined, state).astype(BF16))
+        carried_out = jnp.dot(
+            readout[:, g * STATE : (g + 1) * STATE],
+            jnp.concatenate(halves, axis=1),
+            preferred_element_type=F32,
+        )
+        gated = (mixed[:, at] + carried_out * spread(from_start, g, 2)) * values[:, at]
+        squares = jnp.zeros((LENGTH, WIDE), F32)
+        for term in split_terms(gated * gated, 2):
+            squares = squares + jnp.dot(term, same_head, preferred_element_type=F32)
+        normed = gated * lax.rsqrt(squares * (1.0 / HEAD_DIM) + EPSILON) * head_gain[:, at]
+        heads_out[:, at] = normed.astype(BF16)
+
+    loads[6].wait()
+    for n in range(D // COLS):
+        partial = jnp.dot(
+            heads_out[...], w_out[:, n * COLS : (n + 1) * COLS], preferred_element_type=F32
+        )
+        mix_send[n] = partial.astype(BF16)
+        for d in range(1, NX):
+            xx = lax.rem(x + d, NX)
+            send(
+                mix_send.at[n, pl.ds(pl.multiple_of(xx * ROWS, ROWS), ROWS)],
+                mix_recv.at[NX - d - 1, n],
+                mix_s.at[d - 1, n],
+                mix_r.at[NX - d - 1, n],
+                x_peers[d - 1],
+            )
+    squares = jnp.zeros((ROWS, 1), F32)
+    for n in range(D // COLS):
+        at = slice(n * COLS, (n + 1) * COLS)
+        summed = mix_send[n, pl.ds(pl.multiple_of(x * ROWS, ROWS), ROWS)].astype(F32)
+        for d in range(1, NX):
+            arrive(mix_recv.at[d - 1, n], mix_r.at[d - 1, n])
+            summed = summed + mix_recv[d - 1, n].astype(F32)
+        stream = (residual[:, at].astype(F32) + summed).astype(BF16)
+        stream_out[:, at] = stream
+        wide = stream.astype(F32)
+        squares = squares + jnp.sum(wide * wide, axis=-1, keepdims=True)
+    scale = lax.rsqrt(squares * (1.0 / D) + EPSILON)
+    for n in range(D // COLS):
+        at = slice(n * COLS, (n + 1) * COLS)
+        rows_out[:, at] = (stream_out[:, at].astype(F32) * scale * expert_gain[:, at]).astype(BF16)
+    for copy in started:
+        copy.wait_send()
+
+
+def mixer(
+    residual,
+    gate,
+    value,
+    state,
+    read,
+    step,
+    extra,
+    value_taps,
+    state_taps,
+    read_taps,
+    rates,
+    direct,
+    head_gain,
+    weight,
+    expert_gain,
+):
+    vmem = pl.BlockSpec(memory_space=pltpu.VMEM)
+    hbm = pl.BlockSpec(memory_space=pl.ANY)
+    dma = pltpu.SemaphoreType.DMA
+    inner = HEADS_HERE * HEAD_DIM
+    narrow = GROUPS_HERE * STATE
+    pair_block = (PAIRS, STATE, 128)
+    return pl.pallas_call(
+        mixer_kernel,
+        out_shape=[jax.ShapeDtypeStruct((ROWS, D), BF16)] * 2,
+        in_specs=[vmem] + [hbm] * 6 + [vmem] * 6 + [hbm, vmem],
+        out_specs=[vmem, vmem],
+        scratch_shapes=[
+            pltpu.VMEM((LENGTH, inner), BF16),
+            pltpu.VMEM((LENGTH, inner), BF16),
+            pltpu.VMEM((LENGTH, narrow), BF16),
+            pltpu.VMEM((LENGTH, narrow), BF16),
+            pltpu.VMEM((LENGTH, HEADS_HERE), F32),
+            pltpu.VMEM((LENGTH, HEADS_HERE), F32),
+            pltpu.VMEM((inner, D), BF16),
+            pltpu.VMEM((RIM, inner), BF16),
+            pltpu.VMEM((RIM, narrow), BF16),
+            pltpu.VMEM((RIM, narrow), BF16),
+            pltpu.VMEM((LENGTH + 8, WIDE), F32),
+            pltpu.VMEM((LENGTH, inner), F32),
+            pltpu.VMEM((LENGTH, inner), BF16),
+            pltpu.VMEM((LENGTH, narrow), BF16),
+            pltpu.VMEM((LENGTH, narrow), BF16),
+            pltpu.VMEM((LENGTH, inner), F32),
+            pltpu.VMEM((LENGTH, inner), BF16),
+            pltpu.VMEM(pair_block, F32),
+            pltpu.VMEM(pair_block, BF16),
+            pltpu.VMEM(pair_block, BF16),
+            pltpu.VMEM((NY, 4, STATE, 128), BF16),
+            pltpu.VMEM(pair_block, BF16),
+            pltpu.VMEM((NZ, STATE, 128), BF16),
+            pltpu.VMEM(pair_block, BF16),
+            pltpu.VMEM((PLANE, PAIRS, 128), F32),
+            pltpu.VMEM((NZ, PAIRS, 128), F32),
+            pltpu.VMEM((13, PAIRS, 128), F32),
+            pltpu.VMEM((D // COLS, LENGTH, COLS), BF16),
+            pltpu.VMEM((NX - 1, D // COLS, ROWS, COLS), BF16),
+            dma((7,)),
+            dma((3,)),
+            dma((3,)),
+            dma((PLANE - 1,)),
+            dma((PLANE - 1,)),
+            dma((2,)),
+            dma((2,)),
+            dma((NY - 1,)),
+            dma((NY - 1,)),
+            dma((NZ - 1,)),
+            dma((NZ - 1,)),
+            dma((NZ - 1,)),
+            dma((NZ - 1,)),
+            dma,
+            dma,
+            dma((PLANE - 1,)),
+            dma((PLANE - 1,)),
+            dma((NX - 1, D // COLS)),
+            dma((NX - 1, D // COLS)),
+        ],
+        compiler_params=pltpu.CompilerParams(
+            collective_id=2, has_side_effects=True, vmem_limit_bytes=56 * 1024 * 1024
+        ),
+    )(
+        residual,
+        gate,
+        value,
+        state,
+        read,
+        step,
+        extra,
+        value_taps,
+        state_taps,
+        read_taps,
+        rates,
+        direct,
+        head_gain,
+        weight,
+        expert_gain,
+    )
+
+
 def shards(
     residual,
     output_gate_projected,
@@ -497,98 +901,24 @@
     common_up_weight,
     common_down_weight,
 ):
-    head_count = step_preactivation.shape[1]
-    groups = state_projected_input.shape[1] // STATE
-    heads_per_group = head_count // groups
-    length = value_projected_input.shape[0]
-    block_list = length // BLOCK_POSITIONS
-    conv_tails = (
-        value_projected_input[length - CONV + 1 :],
-        state_projected_input[length - CONV + 1 :],
-        readout_projected_input[length - CONV + 1 :],
+    row_count = residual.shape[0]
+    stream, normed_rows = mixer(
+        residual,
+        output_gate_projected,
+        value_projected_input,
+        state_projected_input,
+        readout_projected_input,
+        step_preactivation,
+        position_decay_extra,
+        value_conv_kernel,
+        state_conv_kernel,
+        readout_conv_kernel,
+        head_log_decay_rates[None, :],
+        head_direct_weight[None, :],
+        head_norm_gain[None, :],
+        mixer_output_weight,
+        expert_norm_gain[None, :],
     )
-    value_rim, input_rim, readout_rim = shifted(
-        (conv_tails[0], conv_tails[1], conv_tails[2]), SP, 1
-    )
-    values = short_conv(value_projected_input, value_rim, value_conv_kernel).reshape(
-        block_list, BLOCK_POSITIONS, groups, heads_per_group, HEAD_DIM
-    )
-    state_in = short_conv(state_projected_input, input_rim, state_conv_kernel).reshape(
-        block_list, BLOCK_POSITIONS, groups, STATE
-    )
-    readout = short_conv(readout_projected_input, readout_rim, readout_conv_kernel).reshape(
-        block_list, BLOCK_POSITIONS, groups, STATE
-    )
-    head_step_lengths = jax.nn.softplus(step_preactivation)
-    decay_logarithm = (
-        head_step_lengths * (-jnp.exp(head_log_decay_rates))[None, :] + position_decay_extra
-    ).reshape(block_list, BLOCK_POSITIONS, groups, heads_per_group)
-    head_step_lengths = head_step_lengths.reshape(
-        block_list, BLOCK_POSITIONS, groups, heads_per_group
-    )
-    causal = jnp.arange(BLOCK_POSITIONS)[:, None] >= jnp.arange(BLOCK_POSITIONS)[None, :]
-    cumulative = jnp.cumsum(decay_logarithm, axis=1)
-    weighted_output = values * head_step_lengths[..., None]
-    by_head = jnp.transpose(cumulative, (0, 2, 3, 1))
-    span_logs = by_head[..., :, None] - by_head[..., None, :]
-    decay_factors = jnp.exp(jnp.where(causal, span_logs, -jnp.inf))
-    attention_scores = jnp.einsum("ctgn,csgn->cgts", readout, state_in)
-    within_block_output = jnp.einsum(
-        "cgrts,csgrp->ctgrp", attention_scores[:, :, None] * decay_factors, weighted_output
-    )
-    to_end = jnp.exp(cumulative[:, -1:] - cumulative)
-    fresh_state = jnp.einsum("csgn,csgrp->cgrpn", state_in, weighted_output * to_end[..., None])
-    block_decay = jnp.exp(cumulative[:, -1])
-
-    def block_chain(carried, block_item):
-        state_now, factor = carried
-        decay_blk, fresh_blk = block_item
-        return (
-            (decay_blk[..., None, None] * state_now + fresh_blk, decay_blk * factor),
-            (state_now, factor),
-        )
-
-    empty_state = jnp.zeros((groups, heads_per_group, HEAD_DIM, STATE), jnp.float32)
-    unit_decay = jnp.ones((groups, heads_per_group), jnp.float32)
-    (own_state, own_decay), (local_start, local_factor) = lax.scan(
-        block_chain, (empty_state, unit_decay), (block_decay, fresh_state)
-    )
-    incoming = carried_in((own_decay, own_state), SP, join_states, (unit_decay, empty_state))
-    start_states = local_start + local_factor[..., None, None] * incoming[1][None]
-    carried_out = (
-        jnp.einsum("ctgn,cgrpn->ctgrp", readout, start_states) * jnp.exp(cumulative)[..., None]
-    )
-    mixed_heads = (
-        within_block_output
-        + carried_out
-        + head_direct_weight.reshape(groups, heads_per_group)[None, None, :, :, None] * values
-    )
-    mixed_heads = mixed_heads.reshape(length, head_count, HEAD_DIM) * jax.nn.silu(
-        output_gate_projected.reshape(length, head_count, HEAD_DIM).astype(jnp.float32)
-    )
-    normed = mixed_heads * lax.rsqrt(
-        jnp.mean(mixed_heads * mixed_heads, axis=-1, keepdims=True) + EPSILON
-    )
-    heads_out = (
-        (normed * head_norm_gain.reshape(head_count, HEAD_DIM))
-        .astype(jnp.bfloat16)
-        .reshape(length, head_count * HEAD_DIM)
-    )
-    row_count = residual.shape[0]
-    mix_sum = sum_at_owner(
-        jnp.dot(heads_out, mixer_output_weight, preferred_element_type=jnp.float32).astype(
-            jnp.bfloat16
-        ),
-        "tp",
-        0,
-    )
-    stream = (residual.astype(jnp.float32) + mix_sum).astype(jnp.bfloat16)
-    stream_wide = stream.astype(jnp.float32)
-    normed_rows = (
-        stream_wide
-        * lax.rsqrt(jnp.mean(stream_wide * stream_wide, axis=-1, keepdims=True) + EPSILON)
-        * expert_norm_gain
-    ).astype(jnp.bfloat16)
     meta = jnp.concatenate(
         [routed_expert_index.T.astype(F32), routed_expert_weight.T.astype(F32)], axis=0
     )

time: 218 us -> 132 us (0.61)
  Pallas kernels: 75.3 us -> 126 us
  waiting for transfers between devices: 44.3 us -> 0 us
  blocking collectives: 28.2 us -> 0 us
  other arithmetic: 21.3 us -> 0.61 us
  starting transfers between devices: 15.2 us -> 0 us
  between operations: 13.9 us -> 0.04 us
  local copies, waits for them, and re-layouts: 12.9 us -> 4.64 us
  matrix products: 6.19 us -> 0 us
    pallas_call x0 -> x1, Pallas kernels: none -> 58.6 us  [mixer(): pl.pallas_call(mixer_kernel, out_shape=[jax.ShapeDtypeStruct((ROWS, D), B...]
    all_gather x2 -> x0, waiting for transfers between devices: 35.1 us -> none  [carried_in(): lax.all_gather(part.astype(kind), axis)]
    all_gather x4 -> x0, blocking collectives: 28.2 us -> none  [carried_in(): lax.all_gather(part.astype(kind), axis)]
    mul x12 -> x0, other arithmetic: 11.2 us -> none  [the longest x3 5.43 us: short_conv(): return jax.nn.silu(totals)]
    ppermute x3 -> x0, starting transfers between devices: 11.1 us -> none  [shifted(): lax.ppermute(value, axis, [(source, source + steps) for source in range(f...]
    all_to_all x1 -> x0, waiting for transfers between devices: 9.13 us -> none  [sum_at_owner(): blocks = lax.all_to_all(cut_along(array, dim, size), axis, 0, 0, tiled=True)]
    pallas_call x1, Pallas kernels: 75.3 us -> 67.7 us  [moe(): pl.pallas_call(moe_kernel, out_shape=jax.ShapeDtypeStruct((ROWS, D), BF16...]
    dot_general x5 -> x0, matrix products: 6.19 us -> none  [the longest x1 2.25 us: shards(): jnp.dot(heads_out, mixer_output_weight, preferred_element_type=jnp.float32)]
  transfers between devices with their start and end apart: 6 -> 0, of which waited for: 3 -> 0; matrix products, arithmetic and copies ran while one was open for 7% -> 0% of each run, Pallas kernels for 0% -> 0%
where the time goes in v2:
time: 132 us
  Pallas kernels  126 us (95%)
  local copies, waits for them, and re-layouts  4.64 us (4%)
    pallas_call x1, Pallas kernels, moe(): pl.pallas_call(moe_kernel, out_shape=jax.ShapeDtypeStruct((ROWS, D), BF16...  67.7 us
    pallas_call x1, Pallas kernels, mixer(): pl.pallas_call(mixer_kernel, out_shape=[jax.ShapeDtypeStruct((ROWS, D), B...  58.6 us
    unnamed x7, local copies, waits for them, and re-layouts  4.64 us

profile of v2, /device:TPU:1, one launch (start us, length us, event | category | flops | bytes accessed | tf_op | source)
XLA Modules:
  0.0 131.6 jit_solution(5061143660402727151)
XLA Ops:
  0.0 0.0 copy-start
  0.0 0.0 copy-start.1
  0.0 1.5 %copy.24.step_hbm = f32[256,16]{1,0:T(8,128)} copy(f32[256,16]{0,1:T(8,128)} %param.28) | data formatting | bytes 32768 | tf_op args[5]
  1.5 1.5 %copy.25.extra_hbm = f32[256,16]{1,0:T(8,128)} copy(f32[256,16]{0,1:T(8,128)} %param.29) | data formatting | bytes 32768 | tf_op args[6]
  3.0 58.6 %shard_map.217 = (bf16[64,2048]{1,0:T(8,128)(2,1)}, bf16[64,2048]{1,0:T(8,128)(2,1)}) custom-call(bf16[64,2048]{1,0:T(8,128)(2,1)} %residual.1, bf16[256,1024]{1,0:T(8,128)(2,1)} %gate_hbm.1, bf16[256,1024]{1,0:T(8,128)(2,1)} %value_hbm.1, bf16[256,512]{1,0:T(8,128)(2,1)} %state_hbm.1, bf16[256,512]{1,0:T(8,128)(2,1)} %read_hbm.1, f32[256,16]{1,0:T(8,128)} %copy.24.step_hbm, ...), custom_call_target="tpu_custom_call" | custom-call | tf_op jit(solution)/shard_map/pallas_call | solution.py:802
  61.6 0.0 copy-done
  61.6 0.0 copy-done.1
  61.6 0.6 select_maximum_fusion.meta
  62.2 67.7 %shard_map.218 = bf16[64,2048]{1,0:T(8,128)(2,1)} custom-call(bf16[64,2048]{1,0:T(8,128)(2,1)} %get-tuple-element.7.rows, bf16[64,2048]{1,0:T(8,128)(2,1)} %get-tuple-element.8.stream, f32[8,128]{1,0:T(8,128)} %select_maximum_fusion.meta, bf16[2048,256]{1,0:T(8,128)(2,1)} %bitcast.10, bf16[2048,256]{1,0:T(8,128)(2,1)} %bitcast.11, ...), custom_call_target="tpu_custom_call" | custom-call | tf_op jit(solution)/shard_map/pallas_call | solution.py:354
  130.0 1.7 %copy.27 = bf16[64,2048]{1,0:T(8,128)(2,1)} copy(bf16[64,2048]{1,0:T(8,128)(2,1)} %shard_map.218) | data formatting | bytes 524288
  (1 shorter events, 0.0 us)
Async XLA Ops:
  0.0 61.6 %copy-start = (s32[64,4]{0,1:T(4,128)S(1)}, s32[64,4]{0,1:T(4,128)}, u32[]{:S(2)}) copy-start(s32[64,4]{0,1:T(4,128)} %param.38) | copy-start | bytes 3076
  0.0 61.6 %copy-start.1 = (f32[64,4]{0,1:T(4,128)S(1)}, f32[64,4]{0,1:T(4,128)}, u32[]{:S(2)}) copy-start(f32[64,4]{0,1:T(4,128)} %param.39) | copy-start | bytes 3076

commit v3 on v1

v3 whole, which is shorter than its diff:
```python
import jax
import jax.numpy as jnp
from jax import lax
from jax.experimental import pallas as pl
from jax.experimental.pallas import tpu as pltpu
from jax.sharding import Mesh
from jax.sharding import PartitionSpec as P

D = 2048
HEAD_DIM = 64
STATE = 128
CONV = 4
SP = ("sp_0", "sp_1", "sp_2")
SP_TP = ("sp_0", "sp_1", "sp_2", "tp")
EPSILON = 1e-06
MESH = pl.DeviceIdType.MESH
BF16 = jnp.bfloat16
F32 = jnp.float32
NZ, NY, NC, NX = 8, 4, 2, 4
PLANE = NY * NC
ROWS = 64
HALF = ROWS // 2
CAP = 8
FE = 256
TOPK = 4
LENGTH = 256
HEADS_HERE = 16
GROUPS_HERE = 4
INNER = HEADS_HERE * HEAD_DIM
NARROW = GROUPS_HERE * STATE
WIDE = 256
PAIRS = 8
RIM = 16
COLS = 512


def device(z, y, c, x):
    return {"sp_0": z, "sp_1": y, "sp_2": c, "tp": x}


def arrive(ref, sem):
    pltpu.make_async_copy(ref, ref, sem).wait()


def split_terms(value, count):
    terms = []
    for _ in range(count):
        term = value.astype(BF16)
        terms.append(term)
        value = value - term.astype(F32)
    return terms


def over(a, b, dims):
    return lax.dot_general(a, b, (dims, ((), ())), preferred_element_type=F32)


def layer_kernel(
    residual,
    gate_hbm,
    value_hbm,
    state_hbm,
    read_hbm,
    step_raw,
    extra_raw,
    value_taps,
    state_taps,
    read_taps,
    rates,
    direct,
    head_gain,
    w_hbm,
    expert_gain,
    index_raw,
    share_raw,
    rg_hbm,
    ru_hbm,
    rd_hbm,
    cg_hbm,
    cu_hbm,
    cd_hbm,
    out,
    gate_in,
    value_in,
    state_raw,
    read_raw,
    w_out,
    value_rim,
    state_rim,
    read_rim,
    ext,
    top,
    values,
    weighted,
    state_in,
    readout,
    mixed,
    heads_out,
    own_send,
    gathered,
    before_me,
    planes,
    incoming_send,
    incoming,
    logs,
    plane_logs,
    factors,
    mix_send,
    mix_recv,
    stream,
    rows,
    meta,
    zall,
    metas,
    combine_w,
    send_rows,
    expert_rows,
    expert_out,
    back_rows,
    rs_send,
    rs_recv,
    xall,
    sh_send,
    sh_recv,
    rg,
    ru,
    rd,
    cg,
    cu,
    cd,
    load_sem,
    rim_s,
    rim_r,
    log_s,
    log_r,
    own_s,
    own_r,
    plog_s,
    plog_r,
    slice_s,
    slice_r,
    in_s,
    in_r,
    mix_s,
    mix_r,
    zs_sem,
    zr_sem,
    ms_sem,
    mr_sem,
    ds_sem,
    dr_sem,
    bs_sem,
    br_sem,
    rss_sem,
    rsr_sem,
    xs_sem,
    xr_sem,
    hs_sem,
    hr_sem,
):
    z, y, c, x = tuple(lax.axis_index(name) for name in SP_TP)
    me = y * NC + c
    turn = 1 - 2 * c

    def z_at(steps):
        return lax.rem(z + turn * steps + NZ, NZ)

    x_peers = [device(z, y, c, lax.rem(x + d, NX)) for d in range(1, NX)]
    z_peers = [device(z_at(d), y, c, x) for d in range(1, NZ)]
    plane_peers = []
    for dy in (1, 3, 2, 0):
        for dc in range(NC):
            if dy or dc:
                yy, cc = lax.rem(y + dy, NY), lax.rem(c + dc, NC)
                back = ((NY - dy) % NY) * NC + dc
                plane_peers.append((dy * NC + dc - 1, back - 1, yy * NC + cc, device(z, yy, cc, x)))

    def along(step):
        count = NZ * NY * NC
        flat = lax.rem((z * NY + y) * NC + c + step + count, count)
        return device(flat // (NY * NC), lax.rem(flat // NC, NY), lax.rem(flat, NC), x)

    loads = [
        pltpu.make_async_copy(far, near, load_sem.at[k])
        for k, (far, near) in enumerate(
            (
                (value_hbm, value_in),
                (state_hbm, state_raw),
                (read_hbm, read_raw),
                (gate_hbm, gate_in),
                (w_hbm, w_out),
                (rg_hbm, rg),
                (ru_hbm, ru),
                (rd_hbm, rd),
                (cg_hbm, cg),
                (cu_hbm, cu),
                (cd_hbm, cd),
            )
        )
    ]
    for load in loads:
        load.start()
    greeted = x_peers + z_peers + [peer[3] for peer in plane_peers] + [along(1), along(-1)]
    barrier = pltpu.get_barrier_semaphore()
    for target in greeted:
        pl.semaphore_signal(barrier, inc=1, device_id=target, device_id_type=MESH)
    started = []

    def send(src, dst, send_sem, recv_sem, target):
        copy = pltpu.make_async_remote_copy(
            src_ref=src,
            dst_ref=dst,
            send_sem=send_sem,
            recv_sem=recv_sem,
            device_id=target,
            device_id_type=MESH,
        )
        copy.start()
        started.append(copy)

    meta[...] = jnp.zeros((8, 128), F32)
    meta[:TOPK, :ROWS] = index_raw[...].astype(F32)
    meta[TOPK:, :ROWS] = share_raw[...]
    sizes = jax.nn.softplus(step_raw[...])
    head_a = lax.broadcasted_iota(jnp.int32, (HEADS_HERE, HEADS_HERE), 0)
    head_b = lax.broadcasted_iota(jnp.int32, (HEADS_HERE, HEADS_HERE), 1)

    def as_column(row):
        square = jnp.broadcast_to(row, (HEADS_HERE, HEADS_HERE))
        return jnp.sum(jnp.where(head_a == head_b, square, 0.0), axis=1, keepdims=True)

    log_decay = sizes * as_column(-jnp.exp(rates[...])) + extra_raw[...]
    early = lax.broadcasted_iota(jnp.int32, (LENGTH, LENGTH), 0)
    late = lax.broadcasted_iota(jnp.int32, (LENGTH, LENGTH), 1)
    causal = early >= late
    lower = jnp.where(causal, 1.0, 0.0).astype(BF16)
    cumulative = jnp.zeros((LENGTH, HEADS_HERE), F32)
    by_head = jnp.zeros((HEADS_HERE, LENGTH), F32)
    for term in split_terms(log_decay, 3):
        cumulative = cumulative + over(lower, term, ((1,), (1,)))
        by_head = by_head + over(term, lower, ((1,), (1,)))
    head_row = lax.broadcasted_iota(jnp.int32, (HEADS_HERE, WIDE), 0)
    lane_head = lax.broadcasted_iota(jnp.int32, (HEADS_HERE, WIDE), 1) // HEAD_DIM
    spreads = [
        jnp.where(head_row == lane_head + 4 * g, 1.0, 0.0).astype(BF16) for g in range(GROUPS_HERE)
    ]

    def spread(value, g, count):
        wide = jnp.zeros((value.shape[1], WIDE), F32)
        for term in split_terms(value, count):
            wide = wide + over(term, spreads[g], ((0,), (0,)))
        return wide

    total = by_head[:, LENGTH - 1 :]
    total_wide = jnp.broadcast_to(total, (HEADS_HERE, 128))
    for g in range(GROUPS_HERE):
        wide = spread(total_wide, g, 3)
        for k in range(2):
            logs[me, pl.ds(2 * g + k, 1)] = wide[:1, k * 128 : (k + 1) * 128]

    for k in range(3):
        loads[k].wait()
    pl.semaphore_wait(barrier, len(greeted))
    convs = (
        (value_in, value_rim, value_taps),
        (state_raw, state_rim, state_taps),
        (read_raw, read_rim, read_taps),
    )
    for k, (near, rim, _) in enumerate(convs):
        send(near.at[pl.ds(LENGTH - RIM, RIM)], rim, rim_s.at[k], rim_r.at[k], along(1))
    for away, back, _, target in plane_peers:
        send(logs.at[me], logs.at[me], log_s.at[away], log_r.at[back], target)
    for d in range(1, NZ):
        send(meta, metas.at[NZ - d], ms_sem.at[d - 1], mr_sem.at[NZ - d - 1], z_peers[d - 1])

    def late_rows(which, lo):
        near, _, taps = convs[which]
        ext[...] = near[:, lo : lo + WIDE].astype(F32)
        weights = taps[:, lo : lo + WIDE].astype(F32)
        sums = ext[RIM - 3 : LENGTH - 3] * weights[0:1]
        for k in range(1, CONV):
            sums = sums + ext[RIM - 3 + k : LENGTH - 3 + k] * weights[k : k + 1]
        return jax.nn.silu(sums)

    first = jnp.where(z + y + c == 0, 0.0, 1.0)

    def early_rows(which, lo):
        near, rim, taps = convs[which]
        top[:8] = rim[:, lo : lo + WIDE].astype(F32)[RIM - 8 :] * first
        top[8:] = near[:RIM, lo : lo + WIDE].astype(F32)
        weights = taps[:, lo : lo + WIDE].astype(F32)
        sums = top[5 : 5 + RIM] * weights[0:1]
        for k in range(1, CONV):
            sums = sums + top[5 + k : 5 + k + RIM] * weights[k : k + 1]
        return jax.nn.silu(sums)

    for lo in range(0, NARROW, WIDE):
        state_in[RIM:, lo : lo + WIDE] = late_rows(1, lo).astype(BF16)
    for lo in range(0, INNER, WIDE):
        values[RIM:, lo : lo + WIDE] = late_rows(0, lo)
    arrive(state_rim, rim_r.at[1])
    for lo in range(0, NARROW, WIDE):
        state_in[:RIM, lo : lo + WIDE] = early_rows(1, lo).astype(BF16)
    arrive(value_rim, rim_r.at[0])
    for lo in range(0, INNER, WIDE):
        values[:RIM, lo : lo + WIDE] = early_rows(0, lo)
    ends = jnp.exp(total - by_head) * sizes
    for g in range(GROUPS_HERE):
        at = slice(g * WIDE, (g + 1) * WIDE)
        ending = (values[:, at] * spread(ends, g, 2)).astype(BF16)
        fresh = over(state_in[:, g * STATE : (g + 1) * STATE], ending, ((0,), (0,)))
        for k in range(2):
            own_send[2 * g + k] = fresh[:, k * 128 : (k + 1) * 128].astype(BF16)
    for away, back, index, target in plane_peers:
        send(own_send.at[index], gathered.at[me], own_s.at[away], own_r.at[back], target)
    gathered[me] = own_send[me]

    for away, _, _, _ in plane_peers:
        arrive(logs.at[0], log_r.at[away])
    reach = jnp.zeros((PAIRS, 128), F32)
    for k in range(PLANE):
        factors[k] = jnp.exp(logs[k])
        factors[PLANE + k] = jnp.exp(reach)
        reach = reach + logs[k]
    plane_logs[z] = reach
    for d in range(1, NZ):
        send(plane_logs.at[z], plane_logs.at[z], plog_s.at[d - 1], plog_r.at[NZ - d - 1], z_peers[d - 1])

    for lo in range(0, NARROW, WIDE):
        readout[RIM:, lo : lo + WIDE] = late_rows(2, lo).astype(BF16)
    arrive(read_rim, rim_r.at[2])
    for lo in range(0, NARROW, WIDE):
        readout[:RIM, lo : lo + WIDE] = early_rows(2, lo).astype(BF16)
    for g in range(GROUPS_HERE):
        at = slice(g * WIDE, (g + 1) * WIDE)
        weighted[:, at] = (values[:, at] * spread(sizes, g, 2)).astype(BF16)

    def within(g):
        scores = over(
            readout[:, g * STATE : (g + 1) * STATE],
            state_in[:, g * STATE : (g + 1) * STATE],
            ((1,), (1,)),
        )
        scores = jnp.where(causal, scores, 0.0)
        group_values = weighted[:, g * WIDE : (g + 1) * WIDE]
        lane = lax.broadcasted_iota(jnp.int32, (LENGTH, WIDE), 1) // HEAD_DIM
        result = jnp.zeros((LENGTH, WIDE), F32)
        for r in range(4):
            h = 4 * g + r
            span = cumulative[:, h : h + 1] - by_head[h : h + 1, :]
            decay = jnp.exp(jnp.where(causal, span, -jnp.inf))
            chosen = jnp.where(lane == r, group_values, jnp.zeros_like(group_values))
            result = result + over((scores * decay).astype(BF16), chosen, ((1,), (0,)))
        mixed[:, g * WIDE : (g + 1) * WIDE] = result

    within(0)

    for away, _, _, _ in plane_peers:
        arrive(gathered.at[0], own_r.at[away])
    carried = jnp.zeros((STATE, 128), F32)
    for k in range(PLANE):
        before_me[k] = carried
        carried = carried * factors[k, pl.ds(me, 1)] + gathered[k].astype(F32)
    planes[z] = carried.astype(BF16)
    for d in range(1, NZ):
        send(planes.at[z], planes.at[z], slice_s.at[d - 1], slice_r.at[NZ - d - 1], z_peers[d - 1])

    within(1)
    within(2)
    within(3)
    loads[3].wait()
    direct_wide = jnp.broadcast_to(as_column(direct[...]), (HEADS_HERE, 128))
    for g in range(GROUPS_HERE):
        at = slice(g * WIDE, (g + 1) * WIDE)
        mixed[:, at] = mixed[:, at] + values[:, at] * spread(direct_wide, g, 3)[:1]
        values[:, at] = jax.nn.silu(gate_in[:, at].astype(F32))
    from_start = jnp.exp(by_head)
    lane_a = lax.broadcasted_iota(jnp.int32, (WIDE, WIDE), 0) // HEAD_DIM
    lane_b = lax.broadcasted_iota(jnp.int32, (WIDE, WIDE), 1) // HEAD_DIM
    same_head = jnp.where(lane_a == lane_b, 1.0, 0.0).astype(BF16)

    for d in range(1, NZ):
        arrive(plane_logs.at[0], plog_r.at[d - 1])
    for k in range(NZ - 1):
        factors[2 * PLANE + k] = jnp.exp(plane_logs[k])
    for d in range(1, NZ):
        arrive(planes.at[0], slice_r.at[d - 1])
    carried = jnp.zeros((STATE, 128), F32)
    for k in range(NZ - 1):
        joined = carried * factors[2 * PLANE + k, pl.ds(me, 1)] + planes[k].astype(F32)
        carried = jnp.where(k < z, joined, carried)
    for k in range(PLANE):
        incoming_send[k] = (carried * factors[PLANE + k, pl.ds(me, 1)] + before_me[k]).astype(BF16)
    for away, back, index, target in plane_peers:
        send(incoming_send.at[index], incoming.at[me], in_s.at[away], in_r.at[back], target)
    incoming[me] = incoming_send[me]
    loads[4].wait()
    for away, _, _, _ in plane_peers:
        arrive(incoming.at[0], in_r.at[away])
    for g in range(GROUPS_HERE):
        at = slice(g * WIDE, (g + 1) * WIDE)
        state = jnp.concatenate([incoming[2 * g], incoming[2 * g + 1]], axis=1)
        carried_out = over(readout[:, g * STATE : (g + 1) * STATE], state, ((1,), (0,)))
        gated = (mixed[:, at] + carried_out * spread(from_start, g, 2)) * values[:, at]
        squares = jnp.zeros((LENGTH, WIDE), F32)
        for term in split_terms(gated * gated, 2):
            squares = squares + over(term, same_head, ((1,), (0,)))
        normed = gated * lax.rsqrt(squares * (1.0 / HEAD_DIM) + EPSILON) * head_gain[:, at]
        heads_out[:, at] = normed.astype(BF16)

    for n in range(D // COLS):
        partial = over(heads_out[...], w_out[:, n * COLS : (n + 1) * COLS], ((1,), (0,)))
        mix_send[n] = partial.astype(BF16)
        for d in range(1, NX):
            xx = lax.rem(x + d, NX)
            send(
                mix_send.at[n, pl.ds(pl.multiple_of(xx * ROWS, ROWS), ROWS)],
                mix_recv.at[NX - d - 1, n],
                mix_s.at[d - 1, n],
                mix_r.at[NX - d - 1, n],
                x_peers[d - 1],
            )
    squares = jnp.zeros((ROWS, 1), F32)
    for n in range(D // COLS):
        at = slice(n * COLS, (n + 1) * COLS)
        summed = mix_send[n, pl.ds(pl.multiple_of(x * ROWS, ROWS), ROWS)].astype(F32)
        for d in range(1, NX):
            arrive(mix_recv.at[d - 1, n], mix_r.at[d - 1, n])
            summed = summed + mix_recv[d - 1, n].astype(F32)
        joined = (residual[:, at].astype(F32) + summed).astype(BF16)
        stream[:, at] = joined
        wide = joined.astype(F32)
        squares = squares + jnp.sum(wide * wide, axis=-1, keepdims=True)
    scale = lax.rsqrt(squares * (1.0 / D) + EPSILON)
    for n in range(D // COLS):
        at = slice(n * COLS, (n + 1) * COLS)
        rows[:, at] = (stream[:, at].astype(F32) * scale * expert_gain[:, at]).astype(BF16)

    def hop(step, up, half):
        lo = half * HALF
        here = ((NZ - step) % NZ) if up else step
        there = ((NZ - step - 1) % NZ) if up else step + 1
        source = rows if step == 0 else zall.at[here]
        k = 0 if up else 1
        send(
            source.at[pl.ds(lo, HALF)],
            zall.at[there, pl.ds(lo, HALF)],
            zs_sem.at[k, step, half],
            zr_sem.at[k, step, half],
            device(z_at(1 if up else -1), y, c, x),
        )

    def ring_arrived(step, up, half):
        lo = half * HALF
        there = ((NZ - step - 1) % NZ) if up else step + 1
        arrive(zall.at[there, pl.ds(lo, HALF)], zr_sem.at[0 if up else 1, step, half])

    for half in range(2):
        for up in (True, False):
            hop(0, up, half)

    token = lax.broadcasted_iota(jnp.int32, (ROWS, ROWS), 0)
    later = lax.broadcasted_iota(jnp.int32, (ROWS, ROWS), 1)
    before = jnp.where(token < later, 1.0, 0.0).astype(BF16)
    expert_row = lax.broadcasted_iota(jnp.int32, (PLANE, ROWS), 0) + z * PLANE
    expert_row = expert_row.astype(F32)
    slot = lax.broadcasted_iota(jnp.int32, (PLANE, CAP, ROWS), 1).astype(F32)
    sends = []

    def dispatch(o):
        table = meta[...] if o == 0 else metas[o]
        hits = jnp.zeros((PLANE, ROWS), F32)
        shares = jnp.zeros((PLANE, ROWS), F32)
        for k in range(TOPK):
            hit = jnp.where(expert_row == table[k : k + 1, :ROWS], 1.0, 0.0)
            hits = hits + hit
            shares = shares + hit * table[TOPK + k : TOPK + k + 1, :ROWS]
        rank = over(hits.astype(BF16), before, ((1,), (0,)))
        chosen = jnp.where(
            (rank[:, None, :] == slot) & (hits[:, None, :] > 0.5),
            jnp.ones((PLANE, CAP, ROWS), F32),
            jnp.zeros((PLANE, CAP, ROWS), F32),
        )
        combine_w[o] = (chosen * shares[:, None, :]).reshape(ROWS, ROWS)
        block = rows[...] if o == 0 else zall[o]
        packed = over(chosen.reshape(ROWS, ROWS).astype(BF16), block, ((1,), (0,)))
        send_rows[o] = packed.reshape(PLANE, CAP, D).astype(BF16)
        for _, _, index, peer in plane_peers:
            copy = pltpu.make_async_remote_copy(
                src_ref=send_rows.at[o, index],
                dst_ref=expert_rows.at[o, me],
                send_sem=ds_sem.at[o],
                recv_sem=dr_sem.at[o],
                device_id=peer,
                device_id_type=MESH,
            )
            copy.start()
        sends.append((send_rows.at[o], ds_sem.at[o]))
        expert_rows[o, me] = send_rows[o, me]

    def run_expert(blocks):
        for o in blocks:
            arrive(expert_rows.at[o, pl.ds(0, PLANE - 1)], dr_sem.at[o])
        inputs = jnp.concatenate(
            [expert_rows[o].astype(F32).reshape(ROWS, D) for o in blocks], axis=0
        ).astype(BF16)
        gate = over(inputs, rg[...], ((1,), (0,)))
        lifted = over(inputs, ru[...], ((1,), (0,)))
        hidden = (jax.nn.silu(gate) * lifted).astype(BF16)
        result = over(hidden, rd[...], ((1,), (0,)))
        for k, o in enumerate(blocks):
            expert_out[o] = (
                result[k * ROWS : (k + 1) * ROWS].reshape(PLANE, CAP, D).astype(BF16)
            )

    def give_back(o):
        for _, _, index, peer in plane_peers:
            copy = pltpu.make_async_remote_copy(
                src_ref=expert_out.at[o, index],
                dst_ref=back_rows.at[o, me],
                send_sem=bs_sem.at[o],
                recv_sem=br_sem.at[o],
                device_id=peer,
                device_id_type=MESH,
            )
            copy.start()
        sends.append((expert_out.at[o], bs_sem.at[o]))
        back_rows[o, me] = expert_out[o, me]

    def combined(o):
        arrive(back_rows.at[o, pl.ds(0, PLANE - 1)], br_sem.at[o])
        returned = back_rows[o].astype(F32).reshape(ROWS, D).astype(BF16)
        return over(combine_w[o].astype(BF16), returned, ((0,), (0,)))

    dispatch(0)
    for d in range(1, NZ):
        arrive(metas.at[NZ - d], mr_sem.at[NZ - d - 1])
    for half in range(2):
        for up in (True, False):
            ring_arrived(0, up, half)
            hop(1, up, half)
    dispatch(7)
    dispatch(1)
    for d in range(1, NX):
        send(rows, xall.at[x], xs_sem.at[d - 1], xr_sem.at[NX - d - 1], x_peers[d - 1])
    for k in range(5, 11):
        loads[k].wait()
    run_expert((0,))
    for half in range(2):
        for up in (True, False):
            ring_arrived(1, up, half)
            hop(2, up, half)
    dispatch(6)
    dispatch(2)
    run_expert((7, 1))
    ring_arrived(2, True, 0)
    hop(3, True, 0)
    ring_arrived(2, False, 1)
    hop(3, False, 1)
    ring_arrived(2, True, 1)
    ring_arrived(2, False, 0)
    dispatch(5)
    dispatch(3)
    run_expert((6, 2))

    for d in range(1, NX):
        arrive(xall.at[0], xr_sem.at[d - 1])
    xall[x] = rows[...]
    hidden_rows = xall[...].reshape(NX * ROWS, D)
    gate = over(hidden_rows, cg[...], ((1,), (0,)))
    lifted = over(hidden_rows, cu[...], ((1,), (0,)))
    hidden = (jax.nn.silu(gate) * lifted).astype(BF16)
    shared = over(hidden, cd[...], ((1,), (1,)))
    sh_send[...] = shared.reshape(NX, ROWS, D).astype(BF16)

    ring_arrived(3, True, 0)
    ring_arrived(3, False, 1)
    dispatch(4)
    for d in range(1, NX):
        send(
            sh_send.at[lax.rem(x + d, NX)],
            sh_recv.at[NX - d - 1],
            hs_sem.at[d - 1],
            hr_sem.at[NX - d - 1],
            x_peers[d - 1],
        )
    run_expert((5, 3))
    run_expert((4,))
    for o in (4, 3, 5, 2, 6, 1, 7, 0):
        give_back(o)

    def pass_on(step, up, half):
        k = 0 if up else 1
        lo = half * HALF
        send(
            rs_send.at[k, step, pl.ds(lo, HALF)],
            rs_recv.at[k, step, pl.ds(lo, HALF)],
            rss_sem.at[k, step, half],
            rsr_sem.at[k, step, half],
            device(z_at(1 if up else -1), y, c, x),
        )

    def sum_arrived(step, up, half):
        k = 0 if up else 1
        arrive(rs_recv.at[k, step, pl.ds(half * HALF, HALF)], rsr_sem.at[k, step, half])
        return rs_recv[k, step, pl.ds(half * HALF, HALF)].astype(F32)

    far = combined(4).astype(BF16)
    rs_send[0, 0, :HALF] = far[:HALF]
    pass_on(0, True, 0)
    rs_send[1, 0, HALF:] = far[HALF:]
    pass_on(0, False, 1)
    for step in range(1, 4):
        for k, up in enumerate((True, False)):
            part = combined(4 - step if up else 4 + step)
            for half in (k, 1 - k):
                piece = part[half * HALF : (half + 1) * HALF]
                if step > 1 or half == k:
                    piece = piece + sum_arrived(step - 1, up, half)
                rs_send[k, step, pl.ds(half * HALF, HALF)] = piece.astype(BF16)
                pass_on(step, up, half)
    total_rows = stream[...].astype(F32) + sh_send[x].astype(F32)
    for d in range(1, NX):
        arrive(sh_recv.at[d - 1], hr_sem.at[d - 1])
        total_rows = total_rows + sh_recv[d - 1].astype(F32)
    total_rows = total_rows + combined(0)
    for half in (1, 0):
        piece = total_rows[half * HALF : (half + 1) * HALF]
        for up in (True, False):
            piece = piece + sum_arrived(3, up, half)
        out[half * HALF : (half + 1) * HALF] = piece.astype(BF16)

    for copy in started:
        copy.wait_send()
    for ref, sem in sends:
        arrive(ref.at[pl.ds(0, PLANE - 1)], sem)


def layer(*arrays):
    vmem = pl.BlockSpec(memory_space=pltpu.VMEM)
    hbm = pl.BlockSpec(memory_space=pl.ANY)
    dma = pltpu.SemaphoreType.DMA
    return pl.pallas_call(
        layer_kernel,
        out_shape=jax.ShapeDtypeStruct((ROWS, D), BF16),
        in_specs=[vmem] + [hbm] * 4 + [vmem] * 8 + [hbm] + [vmem] * 3 + [hbm] * 6,
        out_specs=vmem,
        scratch_shapes=[
            pltpu.VMEM((LENGTH, INNER), BF16),
            pltpu.VMEM((LENGTH, INNER), BF16),
            pltpu.VMEM((LENGTH, NARROW), BF16),
            pltpu.VMEM((LENGTH, NARROW), BF16),
            pltpu.VMEM((INNER, D), BF16),
            pltpu.VMEM((RIM, INNER), BF16),
            pltpu.VMEM((RIM, NARROW), BF16),
            pltpu.VMEM((RIM, NARROW), BF16),
            pltpu.VMEM((LENGTH, WIDE), F32),
            pltpu.VMEM((8 + RIM, WIDE), F32),
            pltpu.VMEM((LENGTH, INNER), F32),
            pltpu.VMEM((LENGTH, INNER), BF16),
            pltpu.VMEM((LENGTH, NARROW), BF16),
            pltpu.VMEM((LENGTH, NARROW), BF16),
            pltpu.VMEM((LENGTH, INNER), F32),
            pltpu.VMEM((LENGTH, INNER), BF16),
            pltpu.VMEM((PAIRS, STATE, 128), BF16),
            pltpu.VMEM((PAIRS, STATE, 128), BF16),
            pltpu.VMEM((PAIRS, STATE, 128), F32),
            pltpu.VMEM((NZ, STATE, 128), BF16),
            pltpu.VMEM((PAIRS, STATE, 128), BF16),
            pltpu.VMEM((PAIRS, STATE, 128), BF16),
            pltpu.VMEM((PLANE, PAIRS, 128), F32),
            pltpu.VMEM((NZ, PAIRS, 128), F32),
            pltpu.VMEM((2 * PLANE + NZ, PAIRS, 128), F32),
            pltpu.VMEM((D // COLS, LENGTH, COLS), BF16),
            pltpu.VMEM((NX - 1, D // COLS, ROWS, COLS), BF16),
            pltpu.VMEM((ROWS, D), BF16),
            pltpu.VMEM((ROWS, D), BF16),
            pltpu.VMEM((8, 128), F32),
            pltpu.VMEM((NZ, ROWS, D), BF16),
            pltpu.VMEM((NZ, 8, 128), F32),
            pltpu.VMEM((NZ, ROWS, ROWS), F32),
            pltpu.VMEM((NZ, PLANE, CAP, D), BF16),
            pltpu.VMEM((NZ, PLANE, CAP, D), BF16),
            pltpu.VMEM((NZ, PLANE, CAP, D), BF16),
            pltpu.VMEM((NZ, PLANE, CAP, D), BF16),
            pltpu.VMEM((2, 4, ROWS, D), BF16),
            pltpu.VMEM((2, 4, ROWS, D), BF16),
            pltpu.VMEM((NX, ROWS, D), BF16),
            pltpu.VMEM((NX, ROWS, D), BF16),
            pltpu.VMEM((NX - 1, ROWS, D), BF16),
            pltpu.VMEM((D, FE), BF16),
            pltpu.VMEM((D, FE), BF16),
            pltpu.VMEM((FE, D), BF16),
            pltpu.VMEM((D, 128), BF16),
            pltpu.VMEM((D, 128), BF16),
            pltpu.VMEM((D, 128), BF16),
            dma((11,)),
            dma((3,)),
            dma((3,)),
            dma((PLANE - 1,)),
            dma((PLANE - 1,)),
            dma((PLANE - 1,)),
            dma((PLANE - 1,)),
            dma((NZ - 1,)),
            dma((NZ - 1,)),
            dma((NZ - 1,)),
            dma((NZ - 1,)),
            dma((PLANE - 1,)),
            dma((PLANE - 1,)),
            dma((NX - 1, D // COLS)),
            dma((NX - 1, D // COLS)),
            dma((2, 4, 2)),
            dma((2, 4, 2)),
            dma((NZ - 1,)),
            dma((NZ - 1,)),
            dma((NZ,)),
            dma((NZ,)),
            dma((NZ,)),
            dma((NZ,)),
            dma((2, 4, 2)),
            dma((2, 4, 2)),
            dma((NX - 1,)),
            dma((NX - 1,)),
            dma((NX - 1,)),
            dma((NX - 1,)),
        ],
        compiler_params=pltpu.CompilerParams(
            collective_id=1, has_side_effects=True, vmem_limit_bytes=60 * 1024 * 1024
        ),
    )(*arrays)


def shards(
    residual,
    output_gate_projected,
    value_projected_input,
    state_projected_input,
    readout_projected_input,
    step_preactivation,
    position_decay_extra,
    value_conv_kernel,
    state_conv_kernel,
    readout_conv_kernel,
    head_log_decay_rates,
    head_direct_weight,
    head_norm_gain,
    mixer_output_weight,
    expert_norm_gain,
    routed_expert_index,
    routed_expert_weight,
    routed_gate_weight,
    routed_up_weight,
    routed_down_weight,
    common_gate_weight,
    common_up_weight,
    common_down_weight,
):
    return layer(
        residual,
        output_gate_projected,
        value_projected_input,
        state_projected_input,
        readout_projected_input,
        step_preactivation.T,
        position_decay_extra.T,
        value_conv_kernel,
        state_conv_kernel,
        readout_conv_kernel,
        head_log_decay_rates[None, :],
        head_direct_weight[None, :],
        head_norm_gain[None, :],
        mixer_output_weight,
        expert_norm_gain[None, :],
        routed_expert_index.T,
        routed_expert_weight.T,
        routed_gate_weight[0],
        routed_up_weight[0],
        routed_down_weight[0],
        common_gate_weight,
        common_up_weight,
        common_down_weight,
    )


def solution(mesh):
    torus = Mesh(mesh.devices.reshape(8, 4, 2, mesh.shape["tp"]), ("sp_0", "sp_1", "sp_2", "tp"))
    return jax.shard_map(
        shards,
        mesh=torus,
        in_specs=(
            P(SP_TP, None),
            P(SP, "tp"),
            P(SP, "tp"),
            P(SP, "tp"),
            P(SP, "tp"),
            P(SP, "tp"),
            P(SP, "tp"),
            P(None, "tp"),
            P(None, "tp"),
            P(None, "tp"),
            P("tp"),
            P("tp"),
            P("tp"),
            P("tp", None),
            P(),
            P(SP_TP, None),
            P(SP_TP, None),
            P(SP, None, None),
            P(SP, None, None),
            P(SP, None, None),
            P(None, "tp"),
            P(None, "tp"),
            P(None, "tp"),
        ),
        out_specs=P(SP_TP, None),
        check_vma=False,
    )
```

time: 218 us -> 116 us (0.53)
  waiting for transfers between devices: 44.3 us -> 0 us
  Pallas kernels: 75.3 us -> 114 us
  blocking collectives: 28.2 us -> 0 us
  other arithmetic: 21.3 us -> 0 us
  starting transfers between devices: 15.2 us -> 0 us
  between operations: 13.9 us -> 0.01 us
  local copies, waits for them, and re-layouts: 12.9 us -> 1.67 us
  matrix products: 6.19 us -> 0 us
    pallas_call x1, Pallas kernels: 75.3 us -> 114 us  [layer(): pl.pallas_call(layer_kernel, out_shape=jax.ShapeDtypeStruct((ROWS, D), BF...]
    all_gather x2 -> x0, waiting for transfers between devices: 35.1 us -> none  [carried_in(): lax.all_gather(part.astype(kind), axis)]
    all_gather x4 -> x0, blocking collectives: 28.2 us -> none  [carried_in(): lax.all_gather(part.astype(kind), axis)]
    mul x12 -> x0, other arithmetic: 11.2 us -> none  [the longest x3 5.43 us: short_conv(): return jax.nn.silu(totals)]
    ppermute x3 -> x0, starting transfers between devices: 11.1 us -> none  [shifted(): lax.ppermute(value, axis, [(source, source + steps) for source in range(f...]
    all_to_all x1 -> x0, waiting for transfers between devices: 9.13 us -> none  [sum_at_owner(): blocks = lax.all_to_all(cut_along(array, dim, size), axis, 0, 0, tiled=True)]
    dot_general x5 -> x0, matrix products: 6.19 us -> none  [the longest x1 2.25 us: shards(): jnp.dot(heads_out, mixer_output_weight, preferred_element_type=jnp.float32)]
    convert_element_type x11 -> x0, other arithmetic: 4.49 us -> none  [the longest x5 3.27 us: carried_in(): part.astype(kind)]
  transfers between devices with their start and end apart: 6 -> 0, of which waited for: 3 -> 0; matrix products, arithmetic and copies ran while one was open for 7% -> 0% of each run, Pallas kernels for 0% -> 0%
where the time goes in v3:
time: 116 us
  Pallas kernels  114 us (98%)
  local copies, waits for them, and re-layouts  1.67 us (1%)
    pallas_call x1, Pallas kernels, layer(): pl.pallas_call(layer_kernel, out_shape=jax.ShapeDtypeStruct((ROWS, D), BF...  114 us

profile of v3, /device:TPU:1, one launch (start us, length us, event | category | flops | bytes accessed | tf_op | source)
XLA Modules:
  0.0 116.1 jit_solution(3322146326265244868)
XLA Ops:
  0.0 114.4 %shard_map.217 = bf16[64,2048]{1,0:T(8,128)(2,1)} custom-call(bf16[64,2048]{1,0:T(8,128)(2,1)} %residual.1, bf16[256,1024]{1,0:T(8,128)(2,1)} %gate_hbm.1, bf16[256,1024]{1,0:T(8,128)(2,1)} %value_hbm.1, bf16[256,512]{1,0:T(8,128)(2,1)} %state_hbm.1, bf16[256,512]{1,0:T(8,128)(2,1)} %read_hbm.1, f32[16,256]{1,0:T(8,128)} %bitcast.14, f32[16,256]{1,0:T(8,128)} %bitcast.15, ...), custom_call_target="tpu_custom_call" | custom-call | tf_op jit(solution)/shard_map/pallas_call | solution.py:643
  114.4 1.7 %copy.25 = bf16[64,2048]{1,0:T(8,128)(2,1)} copy(bf16[64,2048]{1,0:T(8,128)(2,1)} %shard_map.217) | data formatting | bytes 524288

commit v4 on v3

v4 whole, which is shorter than its diff:
```python
import jax
import jax.numpy as jnp
from jax import lax
from jax.experimental import pallas as pl
from jax.experimental.pallas import tpu as pltpu
from jax.sharding import Mesh
from jax.sharding import PartitionSpec as P

D = 2048
HEAD_DIM = 64
STATE = 128
CONV = 4
SP = ("sp_0", "sp_1", "sp_2")
SP_TP = ("sp_0", "sp_1", "sp_2", "tp")
EPSILON = 1e-06
MESH = pl.DeviceIdType.MESH
BF16 = jnp.bfloat16
F32 = jnp.float32
NZ, NY, NC, NX = 8, 4, 2, 4
PLANE = NY * NC
ROWS = 64
HALF = ROWS // 2
CAP = 8
FE = 256
FAR_Z = (4, 3, 5, 2, 6, 1, 7)
FAR_X = (2, 1, 3)
TOPK = 4
LENGTH = 256
HEADS_HERE = 16
GROUPS_HERE = 4
INNER = HEADS_HERE * HEAD_DIM
NARROW = GROUPS_HERE * STATE
WIDE = 256
PAIRS = 8
RIM = 16
COLS = 512
PIECES = D // COLS


def device(z, y, c, x):
    return {"sp_0": z, "sp_1": y, "sp_2": c, "tp": x}


def arrive(ref, sem):
    pltpu.make_async_copy(ref, ref, sem).wait()


def split_terms(value, count):
    terms = []
    for _ in range(count):
        term = value.astype(BF16)
        terms.append(term)
        value = value - term.astype(F32)
    return terms


def over(a, b, dims):
    return lax.dot_general(a, b, (dims, ((), ())), preferred_element_type=F32)


def layer_kernel(
    residual,
    gate_hbm,
    value_hbm,
    state_hbm,
    read_hbm,
    step_raw,
    extra_raw,
    value_taps,
    state_taps,
    read_taps,
    rates,
    direct,
    head_gain,
    w_hbm,
    expert_gain,
    index_raw,
    share_raw,
    rg_hbm,
    ru_hbm,
    rd_hbm,
    cg_hbm,
    cu_hbm,
    cd_hbm,
    out,
    gate_in,
    value_in,
    state_raw,
    read_raw,
    w_out,
    value_rim,
    state_rim,
    read_rim,
    ext,
    top,
    values,
    weighted,
    ending,
    first_sized,
    first_ended,
    state_in,
    readout,
    mixed,
    heads_out,
    own_send,
    gathered,
    before_me,
    planes,
    incoming_send,
    incoming,
    logs,
    plane_logs,
    factors,
    mix_send,
    mix_recv,
    stream,
    rows,
    meta,
    zall,
    scale_send,
    scales,
    slot_send,
    slot_scales,
    chosen_w,
    metas,
    combine_w,
    send_rows,
    expert_rows,
    expert_out,
    back_rows,
    rs_send,
    rs_recv,
    xall,
    sh_send,
    sh_recv,
    rg,
    ru,
    rd,
    cg,
    cu,
    cd,
    load_sem,
    rim_s,
    rim_r,
    log_s,
    log_r,
    own_s,
    own_r,
    plog_s,
    plog_r,
    slice_s,
    slice_r,
    in_s,
    in_r,
    mix_s,
    mix_r,
    zs_sem,
    zr_sem,
    sc_s,
    sc_r,
    sl_s,
    sl_r,
    ms_sem,
    mr_sem,
    ds_sem,
    dr_sem,
    bs_sem,
    br_sem,
    rss_sem,
    rsr_sem,
    xs_sem,
    xr_sem,
    hs_sem,
    hr_sem,
):
    z, y, c, x = tuple(lax.axis_index(name) for name in SP_TP)
    me = y * NC + c
    turn = 1 - 2 * c

    def z_at(steps):
        return lax.rem(z + turn * steps + NZ, NZ)

    x_peers = [device(z, y, c, lax.rem(x + d, NX)) for d in range(1, NX)]
    z_peers = [device(z_at(d), y, c, x) for d in range(1, NZ)]
    plane_peers = []
    for dy in (2, 1, 3, 0):
        for dc in range(NC):
            if dy or dc:
                yy, cc = lax.rem(y + dy, NY), lax.rem(c + dc, NC)
                plane_peers.append((yy * NC + cc, device(z, yy, cc, x)))

    def along(step):
        count = NZ * NY * NC
        flat = lax.rem((z * NY + y) * NC + c + step + count, count)
        return device(flat // (NY * NC), lax.rem(flat // NC, NY), lax.rem(flat, NC), x)

    loads = [
        pltpu.make_async_copy(far, near, load_sem.at[k])
        for k, (far, near) in enumerate(
            (
                (value_hbm, value_in),
                (state_hbm, state_raw),
                (read_hbm, read_raw),
                (gate_hbm, gate_in),
                (w_hbm, w_out),
                (rg_hbm, rg),
                (ru_hbm, ru),
                (rd_hbm, rd),
                (cg_hbm, cg),
                (cu_hbm, cu),
                (cd_hbm, cd),
            )
        )
    ]
    for load in loads:
        load.start()
    greeted = x_peers + z_peers + [peer for _, peer in plane_peers] + [along(1), along(-1)]
    barrier = pltpu.get_barrier_semaphore()
    for target in greeted:
        pl.semaphore_signal(barrier, inc=1, device_id=target, device_id_type=MESH)

    def send(src, dst, send_sem, recv_sem, target):
        copy = pltpu.make_async_remote_copy(
            src_ref=src,
            dst_ref=dst,
            send_sem=send_sem,
            recv_sem=recv_sem,
            device_id=target,
            device_id_type=MESH,
        )
        copy.start()

    meta[...] = jnp.zeros((8, 128), F32)
    meta[:TOPK, :ROWS] = index_raw[...].astype(F32)
    meta[TOPK:, :ROWS] = share_raw[...]
    sizes = jax.nn.softplus(step_raw[...])
    head_a = lax.broadcasted_iota(jnp.int32, (HEADS_HERE, HEADS_HERE), 0)
    head_b = lax.broadcasted_iota(jnp.int32, (HEADS_HERE, HEADS_HERE), 1)

    def as_column(row):
        square = jnp.broadcast_to(row, (HEADS_HERE, HEADS_HERE))
        return jnp.sum(jnp.where(head_a == head_b, square, 0.0), axis=1, keepdims=True)

    log_decay = sizes * as_column(-jnp.exp(rates[...])) + extra_raw[...]
    early = lax.broadcasted_iota(jnp.int32, (LENGTH, LENGTH), 0)
    late = lax.broadcasted_iota(jnp.int32, (LENGTH, LENGTH), 1)
    causal = early >= late
    lower = jnp.where(causal, 1.0, 0.0).astype(BF16)
    cumulative = jnp.zeros((LENGTH, HEADS_HERE), F32)
    by_head = jnp.zeros((HEADS_HERE, LENGTH), F32)
    for term in split_terms(log_decay, 3):
        cumulative = cumulative + over(lower, term, ((1,), (1,)))
        by_head = by_head + over(term, lower, ((1,), (1,)))
    head_row = lax.broadcasted_iota(jnp.int32, (HEADS_HERE, WIDE), 0)
    lane_head = lax.broadcasted_iota(jnp.int32, (HEADS_HERE, WIDE), 1) // HEAD_DIM
    spreads = [
        jnp.where(head_row == lane_head + 4 * g, 1.0, 0.0).astype(BF16) for g in range(GROUPS_HERE)
    ]

    def spread(value, g, count):
        wide = jnp.zeros((value.shape[1], WIDE), F32)
        for term in split_terms(value, count):
            wide = wide + over(term, spreads[g], ((0,), (0,)))
        return wide

    total = by_head[:, LENGTH - 1 :]
    total_wide = jnp.broadcast_to(total, (HEADS_HERE, 128))
    for g in range(GROUPS_HERE):
        wide = spread(total_wide, g, 3)
        for k in range(2):
            logs[me, pl.ds(2 * g + k, 1)] = wide[:1, k * 128 : (k + 1) * 128]

    for k in range(3):
        loads[k].wait()
    pl.semaphore_wait(barrier, len(greeted))
    convs = (
        (value_in, value_rim, value_taps),
        (state_raw, state_rim, state_taps),
        (read_raw, read_rim, read_taps),
    )
    for k, (near, rim, _) in enumerate(convs):
        send(near.at[pl.ds(LENGTH - RIM, RIM)], rim, rim_s.at[k], rim_r.at[k], along(1))
    for _, target in plane_peers:
        send(logs.at[me], logs.at[me], log_s, log_r, target)
    for d in FAR_Z:
        send(meta, metas.at[NZ - d], ms_sem, mr_sem, z_peers[d - 1])

    def late_rows(which, lo):
        near, _, taps = convs[which]
        ext[...] = near[:, lo : lo + WIDE].astype(F32)
        weights = taps[:, lo : lo + WIDE].astype(F32)
        sums = ext[RIM - 3 : LENGTH - 3] * weights[0:1]
        for k in range(1, CONV):
            sums = sums + ext[RIM - 3 + k : LENGTH - 3 + k] * weights[k : k + 1]
        return jax.nn.silu(sums)

    first = jnp.where(z + y + c == 0, 0.0, 1.0)

    def early_rows(which, lo):
        near, rim, taps = convs[which]
        top[:8] = rim[:, lo : lo + WIDE].astype(F32)[RIM - 8 :] * first
        top[8:] = near[:RIM, lo : lo + WIDE].astype(F32)
        weights = taps[:, lo : lo + WIDE].astype(F32)
        sums = top[5 : 5 + RIM] * weights[0:1]
        for k in range(1, CONV):
            sums = sums + top[5 + k : 5 + k + RIM] * weights[k : k + 1]
        return jax.nn.silu(sums)

    ends = jnp.exp(total - by_head) * sizes
    for lo in range(0, NARROW, WIDE):
        state_in[RIM:, lo : lo + WIDE] = late_rows(1, lo).astype(BF16)
    for g in range(GROUPS_HERE):
        at = slice(g * WIDE, (g + 1) * WIDE)
        value = late_rows(0, g * WIDE)
        values[RIM:, at] = value
        sized = spread(sizes, g, 2)
        ended = spread(ends, g, 2)
        weighted[RIM:, at] = (value * sized[RIM:]).astype(BF16)
        ending[RIM:, at] = (value * ended[RIM:]).astype(BF16)
        first_sized[:, at] = sized[:RIM]
        first_ended[:, at] = ended[:RIM]
    for lo in range(0, NARROW, WIDE):
        readout[RIM:, lo : lo + WIDE] = late_rows(2, lo).astype(BF16)
    arrive(state_rim, rim_r.at[1])
    for lo in range(0, NARROW, WIDE):
        state_in[:RIM, lo : lo + WIDE] = early_rows(1, lo).astype(BF16)
    arrive(value_rim, rim_r.at[0])
    for g in range(GROUPS_HERE):
        at = slice(g * WIDE, (g + 1) * WIDE)
        value = early_rows(0, g * WIDE)
        values[:RIM, at] = value
        ending[:RIM, at] = (value * first_ended[:, at]).astype(BF16)
        fresh = over(state_in[:, g * STATE : (g + 1) * STATE], ending[:, at], ((0,), (0,)))
        for k in range(2):
            own_send[2 * g + k] = fresh[:, k * 128 : (k + 1) * 128].astype(BF16)
    for index, target in plane_peers:
        send(own_send.at[index], gathered.at[me], own_s, own_r, target)
    gathered[me] = own_send[me]

    arrive(logs.at[pl.ds(0, PLANE - 1)], log_r)
    reach = jnp.zeros((PAIRS, 128), F32)
    for k in range(PLANE):
        factors[k] = jnp.exp(logs[k])
        factors[PLANE + k] = jnp.exp(reach)
        reach = reach + logs[k]
    plane_logs[z] = reach
    for d in FAR_Z:
        send(plane_logs.at[z], plane_logs.at[z], plog_s, plog_r, z_peers[d - 1])

    arrive(read_rim, rim_r.at[2])
    for lo in range(0, NARROW, WIDE):
        readout[:RIM, lo : lo + WIDE] = early_rows(2, lo).astype(BF16)
    weighted[:RIM] = (values[:RIM] * first_sized[...]).astype(BF16)

    def within(g):
        scores = over(
            readout[:, g * STATE : (g + 1) * STATE],
            state_in[:, g * STATE : (g + 1) * STATE],
            ((1,), (1,)),
        )
        scores = jnp.where(causal, scores, 0.0)
        group_values = weighted[:, g * WIDE : (g + 1) * WIDE]
        lane = lax.broadcasted_iota(jnp.int32, (LENGTH, WIDE), 1) // HEAD_DIM
        result = jnp.zeros((LENGTH, WIDE), F32)
        for r in range(4):
            h = 4 * g + r
            span = cumulative[:, h : h + 1] - by_head[h : h + 1, :]
            decay = jnp.exp(jnp.where(causal, span, -jnp.inf))
            chosen = jnp.where(lane == r, group_values, jnp.zeros_like(group_values))
            result = result + over((scores * decay).astype(BF16), chosen, ((1,), (0,)))
        mixed[:, g * WIDE : (g + 1) * WIDE] = result

    within(0)

    arrive(gathered.at[pl.ds(0, PLANE - 1)], own_r)
    carried = jnp.zeros((STATE, 128), F32)
    for k in range(PLANE):
        before_me[k] = carried
        carried = carried * factors[k, pl.ds(me, 1)] + gathered[k].astype(F32)
    planes[z] = carried.astype(BF16)
    for d in FAR_Z:
        send(planes.at[z], planes.at[z], slice_s, slice_r, z_peers[d - 1])

    within(1)
    within(2)
    within(3)
    loads[3].wait()
    from_start = jnp.exp(by_head)
    direct_wide = jnp.broadcast_to(as_column(direct[...]), (HEADS_HERE, 128))
    for g in range(GROUPS_HERE):
        at = slice(g * WIDE, (g + 1) * WIDE)
        gate = jax.nn.silu(gate_in[:, at].astype(F32))
        mixed[:, at] = (mixed[:, at] + values[:, at] * spread(direct_wide, g, 3)[:1]) * gate
        values[:, at] = spread(from_start, g, 2) * gate
    lane_a = lax.broadcasted_iota(jnp.int32, (WIDE, WIDE), 0) // HEAD_DIM
    lane_b = lax.broadcasted_iota(jnp.int32, (WIDE, WIDE), 1) // HEAD_DIM
    same_head = jnp.where(lane_a == lane_b, 1.0, 0.0).astype(BF16)

    token = lax.broadcasted_iota(jnp.int32, (ROWS, ROWS), 0)
    later = lax.broadcasted_iota(jnp.int32, (ROWS, ROWS), 1)
    before = jnp.where(token < later, 1.0, 0.0).astype(BF16)
    expert_row = lax.broadcasted_iota(jnp.int32, (PLANE, ROWS), 0) + z * PLANE
    expert_row = expert_row.astype(F32)
    slot = lax.broadcasted_iota(jnp.int32, (PLANE, CAP, ROWS), 1).astype(F32)
    arrive(metas.at[pl.ds(0, NZ - 1)], mr_sem)
    for o in range(NZ):
        table = meta[...] if o == 0 else metas[o]
        hits = jnp.zeros((PLANE, ROWS), F32)
        shares = jnp.zeros((PLANE, ROWS), F32)
        for k in range(TOPK):
            hit = jnp.where(expert_row == table[k : k + 1, :ROWS], 1.0, 0.0)
            hits = hits + hit
            shares = shares + hit * table[TOPK + k : TOPK + k + 1, :ROWS]
        rank = over(hits.astype(BF16), before, ((1,), (0,)))
        chosen = jnp.where(
            (rank[:, None, :] == slot) & (hits[:, None, :] > 0.5),
            jnp.ones((PLANE, CAP, ROWS), F32),
            jnp.zeros((PLANE, CAP, ROWS), F32),
        )
        chosen_w[o] = chosen.reshape(ROWS, ROWS)
        combine_w[o] = (chosen * shares[:, None, :]).reshape(ROWS, ROWS)

    arrive(plane_logs.at[pl.ds(0, NZ - 1)], plog_r)
    for k in range(NZ - 1):
        factors[2 * PLANE + k] = jnp.exp(plane_logs[k])
    arrive(planes.at[pl.ds(0, NZ - 1)], slice_r)
    carried = jnp.zeros((STATE, 128), F32)
    for k in range(NZ - 1):
        joined = carried * factors[2 * PLANE + k, pl.ds(me, 1)] + planes[k].astype(F32)
        carried = jnp.where(k < z, joined, carried)
    for k in range(PLANE):
        incoming_send[k] = (carried * factors[PLANE + k, pl.ds(me, 1)] + before_me[k]).astype(BF16)
    for index, target in plane_peers:
        send(incoming_send.at[index], incoming.at[me], in_s, in_r, target)
    incoming[me] = incoming_send[me]
    loads[4].wait()
    arrive(incoming.at[pl.ds(0, PLANE - 1)], in_r)
    for g in range(GROUPS_HERE):
        at = slice(g * WIDE, (g + 1) * WIDE)
        state = jnp.concatenate([incoming[2 * g], incoming[2 * g + 1]], axis=1)
        carried_out = over(readout[:, g * STATE : (g + 1) * STATE], state, ((1,), (0,)))
        gated = mixed[:, at] + carried_out * values[:, at]
        squares = jnp.zeros((LENGTH, WIDE), F32)
        for term in split_terms(gated * gated, 2):
            squares = squares + over(term, same_head, ((1,), (0,)))
        normed = gated * lax.rsqrt(squares * (1.0 / HEAD_DIM) + EPSILON) * head_gain[:, at]
        heads_out[:, at] = normed.astype(BF16)

    for n in range(PIECES):
        partial = over(heads_out[...], w_out[:, n * COLS : (n + 1) * COLS], ((1,), (0,)))
        mix_send[n] = partial.astype(BF16)
        for d in FAR_X:
            xx = lax.rem(x + d, NX)
            send(
                mix_send.at[n, pl.ds(pl.multiple_of(xx * ROWS, ROWS), ROWS)],
                mix_recv.at[n, NX - d - 1],
                mix_s,
                mix_r.at[n],
                x_peers[d - 1],
            )
    def hop(step, up, n):
        here = ((NZ - step) % NZ) if up else step
        there = ((NZ - step - 1) % NZ) if up else step + 1
        k = 0 if up else 1
        send(
            stream.at[n] if step == 0 else zall.at[here, n],
            zall.at[there, n],
            zs_sem,
            zr_sem.at[k, step, n],
            device(z_at(1 if up else -1), y, c, x),
        )

    def ring_arrived(step, up, n):
        there = ((NZ - step - 1) % NZ) if up else step + 1
        arrive(zall.at[there, n], zr_sem.at[0 if up else 1, step, n])

    def relay(step, n):
        for up in (True, False):
            if step < 2:
                ring_arrived(step, up, n)
                hop(step + 1, up, n)
            elif step == 2:
                ring_arrived(step, up, n)
                if (n < 2) == up:
                    hop(3, up, n)
            elif (n < 2) == up:
                ring_arrived(3, up, n)

    def dispatch(o, m):
        for n in range(2):
            block = stream[2 * m + n] if o == 0 else zall[o, 2 * m + n]
            packed = over(chosen_w[o].astype(BF16), block, ((1,), (0,)))
            send_rows[o, m, :, :, n * COLS : (n + 1) * COLS] = packed.reshape(
                PLANE, CAP, COLS
            ).astype(BF16)
        for index, peer in plane_peers:
            copy = pltpu.make_async_remote_copy(
                src_ref=send_rows.at[o, m, index],
                dst_ref=expert_rows.at[o, m * PLANE + me],
                send_sem=ds_sem,
                recv_sem=dr_sem.at[o],
                device_id=peer,
                device_id_type=MESH,
            )
            copy.start()
        expert_rows[o, m * PLANE + me] = send_rows[o, m, me]

    def run_expert(blocks):
        halves = []
        for m in range(2):
            parts = []
            gain = expert_gain[:, m * (D // 2) : (m + 1) * (D // 2)]
            for o in blocks:
                if m == 0:
                    arrive(expert_rows.at[o, pl.ds(0, 2 * PLANE - 2)], dr_sem.at[o])
                wide = expert_rows[o, m * PLANE : (m + 1) * PLANE].astype(F32) * slot_scales[:, :, o : o + 1]
                parts.append(wide.reshape(ROWS, D // 2))
            halves.append((jnp.concatenate(parts, axis=0) * gain).astype(BF16))
        gate = over(halves[0], rg[: D // 2], ((1,), (0,))) + over(halves[1], rg[D // 2 :], ((1,), (0,)))
        lifted = over(halves[0], ru[: D // 2], ((1,), (0,))) + over(halves[1], ru[D // 2 :], ((1,), (0,)))
        hidden = (jax.nn.silu(gate) * lifted).astype(BF16)
        for m in range(2):
            result = over(hidden, rd[:, m * (D // 2) : (m + 1) * (D // 2)], ((1,), (0,)))
            for k, o in enumerate(blocks):
                expert_out[o, m] = (
                    result[k * ROWS : (k + 1) * ROWS].reshape(PLANE, CAP, D // 2).astype(BF16)
                )

    def give_back(o, m):
        for index, peer in plane_peers:
            copy = pltpu.make_async_remote_copy(
                src_ref=expert_out.at[o, m, index],
                dst_ref=back_rows.at[o, m, me],
                send_sem=bs_sem,
                recv_sem=br_sem.at[o, m],
                device_id=peer,
                device_id_type=MESH,
            )
            copy.start()
        back_rows[o, m, me] = expert_out[o, m, me]

    def combined(o, m):
        arrive(back_rows.at[o, m, pl.ds(0, PLANE - 1)], br_sem.at[o, m])
        returned = back_rows[o, m].astype(F32).reshape(ROWS, D // 2).astype(BF16)
        return over(combine_w[o].astype(BF16), returned, ((0,), (0,)))

    square_sums = []

    def take_piece(n):
        at = slice(n * COLS, (n + 1) * COLS)
        summed = mix_send[n, pl.ds(pl.multiple_of(x * ROWS, ROWS), ROWS)].astype(F32)
        arrive(mix_recv.at[n], mix_r.at[n])
        for d in range(1, NX):
            summed = summed + mix_recv[n, d - 1].astype(F32)
        joined = (residual[:, at].astype(F32) + summed).astype(BF16)
        stream[n] = joined
        hop(0, True, n)
        hop(0, False, n)
        wide = joined.astype(F32)
        square_sums.append(jnp.sum(wide * wide, axis=-1, keepdims=True))

    take_piece(0)
    take_piece(1)
    dispatch(0, 0)
    relay(0, 0)
    take_piece(2)
    relay(0, 1)
    dispatch(7, 0)
    dispatch(1, 0)
    relay(1, 0)
    take_piece(3)
    squares = square_sums[0] + square_sums[1] + square_sums[2] + square_sums[3]
    scale = lax.rsqrt(squares * (1.0 / D) + EPSILON)
    scale_row = jnp.sum(jnp.where(token == later, scale, 0.0), axis=0, keepdims=True)
    scale_send[...] = jnp.zeros((8, 128), F32)
    scale_send[:1, :ROWS] = scale_row
    for d in FAR_Z:
        send(scale_send, scales.at[NZ - d], sc_s, sc_r, z_peers[d - 1])
    dispatch(0, 1)
    for n in range(PIECES):
        at = slice(n * COLS, (n + 1) * COLS)
        rows[:, at] = (stream[n].astype(F32) * scale * expert_gain[:, at]).astype(BF16)
    for d in FAR_X:
        send(rows, xall.at[x], xs_sem, xr_sem, x_peers[d - 1])
    relay(0, 2)
    relay(1, 1)
    dispatch(6, 0)
    dispatch(2, 0)
    relay(2, 0)
    relay(0, 3)
    dispatch(7, 1)
    dispatch(1, 1)
    lane = lax.broadcasted_iota(jnp.int32, (PLANE, CAP, 128), 2)
    by_slot = jnp.zeros((PLANE, CAP, 128), F32)
    arrive(scales.at[pl.ds(0, NZ - 1)], sc_r)
    for o in range(NZ):
        known = scale_row if o == 0 else scales[o, :1, :ROWS]
        found = jnp.sum(chosen_w[o] * known, axis=1, keepdims=True).reshape(PLANE, CAP, 1)
        by_slot = jnp.where(lane == o, found, by_slot)
    slot_send[...] = by_slot
    for index, target in plane_peers:
        send(slot_send.at[index], slot_scales.at[me], sl_s, sl_r, target)
    slot_scales[me] = slot_send[me]
    relay(1, 2)
    relay(2, 1)
    dispatch(5, 0)
    dispatch(3, 0)
    relay(3, 0)
    relay(1, 3)
    dispatch(6, 1)
    dispatch(2, 1)
    for k in range(5, 11):
        loads[k].wait()
    arrive(slot_scales.at[pl.ds(0, PLANE - 1)], sl_r)
    run_expert((0,))
    relay(2, 2)
    relay(3, 1)
    dispatch(4, 0)
    relay(2, 3)
    dispatch(5, 1)
    dispatch(3, 1)
    run_expert((7, 1))
    relay(3, 2)
    relay(3, 3)
    dispatch(4, 1)
    arrive(xall.at[pl.ds(0, NX - 1)], xr_sem)
    xall[x] = rows[...]
    hidden_rows = xall[...].reshape(NX * ROWS, D)
    gate = over(hidden_rows, cg[...], ((1,), (0,)))
    lifted = over(hidden_rows, cu[...], ((1,), (0,)))
    hidden = (jax.nn.silu(gate) * lifted).astype(BF16)
    shared = over(hidden, cd[...], ((1,), (1,)))
    sh_send[...] = shared.reshape(NX, ROWS, D).astype(BF16)
    for d in FAR_X:
        send(
            sh_send.at[lax.rem(x + d, NX)],
            sh_recv.at[NX - d - 1],
            hs_sem,
            hr_sem,
            x_peers[d - 1],
        )
    run_expert((6, 2))
    run_expert((5, 3))
    run_expert((4,))
    for o in (4, 3, 5, 2, 6, 1, 7, 0):
        for m in range(2):
            give_back(o, m)

    def cell(step, up, m):
        if step == 0:
            return 12 + m
        return (step - 1) * 4 + (0 if up else 2) + m

    def pass_on(step, up, m):
        k = cell(step, up, m)
        send(
            rs_send.at[k],
            rs_recv.at[k],
            rss_sem,
            rsr_sem.at[k],
            device(z_at(1 if up else -1), y, c, x),
        )

    def sum_arrived(step, up, m):
        k = cell(step, up, m)
        arrive(rs_recv.at[k], rsr_sem.at[k])
        return rs_recv[k].astype(F32)

    for m, up in ((0, True), (1, False)):
        rs_send[cell(0, up, m)] = combined(4, m).astype(BF16)
        pass_on(0, up, m)
    for step in range(1, 4):
        for k, up in enumerate((True, False)):
            for m in (k, 1 - k):
                piece = combined(4 - step if up else 4 + step, m)
                if step > 1 or m == k:
                    piece = piece + sum_arrived(step - 1, up, m)
                rs_send[cell(step, up, m)] = piece.astype(BF16)
                pass_on(step, up, m)
    arrive(sh_recv, hr_sem)
    for m in range(2):
        at = slice(m * (D // 2), (m + 1) * (D // 2))
        piece = jnp.concatenate([stream[2 * m], stream[2 * m + 1]], axis=1).astype(F32)
        piece = piece + sh_send[x, :, at].astype(F32)
        for d in range(1, NX):
            piece = piece + sh_recv[d - 1, :, at].astype(F32)
        piece = piece + combined(0, m)
        for up in (True, False):
            piece = piece + sum_arrived(3, up, m)
        out[:, at] = piece.astype(BF16)

    for k, (near, _, _) in enumerate(convs):
        arrive(near.at[pl.ds(0, RIM)], rim_s.at[k])
    for ref, sem in (
        (logs.at[pl.ds(0, PLANE - 1)], log_s),
        (metas.at[pl.ds(0, NZ - 1)], ms_sem),
        (own_send.at[pl.ds(0, PLANE - 1)], own_s),
        (plane_logs.at[pl.ds(0, NZ - 1)], plog_s),
        (planes.at[pl.ds(0, NZ - 1)], slice_s),
        (incoming_send.at[pl.ds(0, PLANE - 1)], in_s),
        (mix_recv, mix_s),
        (scales.at[pl.ds(0, NZ - 1)], sc_s),
        (slot_send.at[pl.ds(0, PLANE - 1)], sl_s),
        (xall.at[pl.ds(0, NX - 1)], xs_sem),
        (sh_recv, hs_sem),
        (zall.at[pl.ds(0, NZ - 1)], zs_sem),
        (send_rows.at[pl.ds(0, NZ - 1)], ds_sem),
        (expert_out.at[pl.ds(0, NZ - 1)], bs_sem),
        (rs_send, rss_sem),
    ):
        arrive(ref, sem)


def layer(*arrays):
    vmem = pl.BlockSpec(memory_space=pltpu.VMEM)
    hbm = pl.BlockSpec(memory_space=pl.ANY)
    dma = pltpu.SemaphoreType.DMA
    return pl.pallas_call(
        layer_kernel,
        out_shape=jax.ShapeDtypeStruct((ROWS, D), BF16),
        in_specs=[vmem] + [hbm] * 4 + [vmem] * 8 + [hbm] + [vmem] * 3 + [hbm] * 6,
        out_specs=vmem,
        scratch_shapes=[
            pltpu.VMEM((LENGTH, INNER), BF16),
            pltpu.VMEM((LENGTH, INNER), BF16),
            pltpu.VMEM((LENGTH, NARROW), BF16),
            pltpu.VMEM((LENGTH, NARROW), BF16),
            pltpu.VMEM((INNER, D), BF16),
            pltpu.VMEM((RIM, INNER), BF16),
            pltpu.VMEM((RIM, NARROW), BF16),
            pltpu.VMEM((RIM, NARROW), BF16),
            pltpu.VMEM((LENGTH, WIDE), F32),
            pltpu.VMEM((8 + RIM, WIDE), F32),
            pltpu.VMEM((LENGTH, INNER), F32),
            pltpu.VMEM((LENGTH, INNER), BF16),
            pltpu.VMEM((LENGTH, INNER), BF16),
            pltpu.VMEM((RIM, INNER), F32),
            pltpu.VMEM((RIM, INNER), F32),
            pltpu.VMEM((LENGTH, NARROW), BF16),
            pltpu.VMEM((LENGTH, NARROW), BF16),
            pltpu.VMEM((LENGTH, INNER), F32),
            pltpu.VMEM((LENGTH, INNER), BF16),
            pltpu.VMEM((PAIRS, STATE, 128), BF16),
            pltpu.VMEM((PAIRS, STATE, 128), BF16),
            pltpu.VMEM((PAIRS, STATE, 128), F32),
            pltpu.VMEM((NZ, STATE, 128), BF16),
            pltpu.VMEM((PAIRS, STATE, 128), BF16),
            pltpu.VMEM((PAIRS, STATE, 128), BF16),
            pltpu.VMEM((PLANE, PAIRS, 128), F32),
            pltpu.VMEM((NZ, PAIRS, 128), F32),
            pltpu.VMEM((2 * PLANE + NZ, PAIRS, 128), F32),
            pltpu.VMEM((PIECES, LENGTH, COLS), BF16),
            pltpu.VMEM((PIECES, NX - 1, ROWS, COLS), BF16),
            pltpu.VMEM((PIECES, ROWS, COLS), BF16),
            pltpu.VMEM((ROWS, D), BF16),
            pltpu.VMEM((8, 128), F32),
            pltpu.VMEM((NZ, PIECES, ROWS, COLS), BF16),
            pltpu.VMEM((8, 128), F32),
            pltpu.VMEM((NZ, 8, 128), F32),
            pltpu.VMEM((PLANE, CAP, 128), F32),
            pltpu.VMEM((PLANE, CAP, 128), F32),
            pltpu.VMEM((NZ, ROWS, ROWS), F32),
            pltpu.VMEM((NZ, 8, 128), F32),
            pltpu.VMEM((NZ, ROWS, ROWS), F32),
            pltpu.VMEM((NZ, 2, PLANE, CAP, D // 2), BF16),
            pltpu.VMEM((NZ, 2 * PLANE, CAP, D // 2), BF16),
            pltpu.VMEM((NZ, 2, PLANE, CAP, D // 2), BF16),
            pltpu.VMEM((NZ, 2, PLANE, CAP, D // 2), BF16),
            pltpu.VMEM((14, ROWS, D // 2), BF16),
            pltpu.VMEM((14, ROWS, D // 2), BF16),
            pltpu.VMEM((NX, ROWS, D), BF16),
            pltpu.VMEM((NX, ROWS, D), BF16),
            pltpu.VMEM((NX - 1, ROWS, D), BF16),
            pltpu.VMEM((D, FE), BF16),
            pltpu.VMEM((D, FE), BF16),
            pltpu.VMEM((FE, D), BF16),
            pltpu.VMEM((D, 128), BF16),
            pltpu.VMEM((D, 128), BF16),
            pltpu.VMEM((D, 128), BF16),
            dma((11,)),
            dma((3,)),
            dma((3,)),
            dma,
            dma,
            dma,
            dma,
            dma,
            dma,
            dma,
            dma,
            dma,
            dma,
            dma,
            dma((PIECES,)),
            dma,
            dma((2, 4, PIECES)),
            dma,
            dma,
            dma,
            dma,
            dma,
            dma,
            dma,
            dma((NZ,)),
            dma,
            dma((NZ, 2)),
            dma,
            dma((14,)),
            dma,
            dma,
            dma,
            dma,
        ],
        compiler_params=pltpu.CompilerParams(
            collective_id=1, has_side_effects=True, vmem_limit_bytes=60 * 1024 * 1024
        ),
    )(*arrays)


def shards(
    residual,
    output_gate_projected,
    value_projected_input,
    state_projected_input,
    readout_projected_input,
    step_preactivation,
    position_decay_extra,
    value_conv_kernel,
    state_conv_kernel,
    readout_conv_kernel,
    head_log_decay_rates,
    head_direct_weight,
    head_norm_gain,
    mixer_output_weight,
    expert_norm_gain,
    routed_expert_index,
    routed_expert_weight,
    routed_gate_weight,
    routed_up_weight,
    routed_down_weight,
    common_gate_weight,
    common_up_weight,
    common_down_weight,
):
    return layer(
        residual,
        output_gate_projected,
        value_projected_input,
        state_projected_input,
        readout_projected_input,
        step_preactivation.T,
        position_decay_extra.T,
        value_conv_kernel,
        state_conv_kernel,
        readout_conv_kernel,
        head_log_decay_rates[None, :],
        head_direct_weight[None, :],
        head_norm_gain[None, :],
        mixer_output_weight,
        expert_norm_gain[None, :],
        routed_expert_index.T,
        routed_expert_weight.T,
        routed_gate_weight[0],
        routed_up_weight[0],
        routed_down_weight[0],
        common_gate_weight,
        common_up_weight,
        common_down_weight,
    )


def solution(mesh):
    torus = Mesh(mesh.devices.reshape(8, 4, 2, mesh.shape["tp"]), ("sp_0", "sp_1", "sp_2", "tp"))
    return jax.shard_map(
        shards,
        mesh=torus,
        in_specs=(
            P(SP_TP, None),
            P(SP, "tp"),
            P(SP, "tp"),
            P(SP, "tp"),
            P(SP, "tp"),
            P(SP, "tp"),
            P(SP, "tp"),
            P(None, "tp"),
            P(None, "tp"),
            P(None, "tp"),
            P("tp"),
            P("tp"),
            P("tp"),
            P("tp", None),
            P(),
            P(SP_TP, None),
            P(SP_TP, None),
            P(SP, None, None),
            P(SP, None, None),
            P(SP, None, None),
            P(None, "tp"),
            P(None, "tp"),
            P(None, "tp"),
        ),
        out_specs=P(SP_TP, None),
        check_vma=False,
    )
```

time: 116 us -> 103 us (0.89)
  Pallas kernels: 114 us -> 102 us
    pallas_call x1, Pallas kernels: 114 us -> 102 us  [layer(): pl.pallas_call(layer_kernel, out_shape=jax.ShapeDtypeStruct((ROWS, D), BF...]
where the time goes in v4:
time: 103 us
  Pallas kernels  102 us (99%)
  local copies, waits for them, and re-layouts  1.67 us (2%)
    pallas_call x1, Pallas kernels, layer(): pl.pallas_call(layer_kernel, out_shape=jax.ShapeDtypeStruct((ROWS, D), BF...  102 us

profile of v4, /device:TPU:1, one launch (start us, length us, event | category | flops | bytes accessed | tf_op | source)
XLA Modules:
  0.0 103.3 jit_solution(1454884582794616932)
XLA Ops:
  0.0 101.6 %shard_map.217 = bf16[64,2048]{1,0:T(8,128)(2,1)} custom-call(bf16[64,2048]{1,0:T(8,128)(2,1)} %residual.1, bf16[256,1024]{1,0:T(8,128)(2,1)} %gate_hbm.1, bf16[256,1024]{1,0:T(8,128)(2,1)} %value_hbm.1, bf16[256,512]{1,0:T(8,128)(2,1)} %state_hbm.1, bf16[256,512]{1,0:T(8,128)(2,1)} %read_hbm.1, f32[16,256]{1,0:T(8,128)} %bitcast.14, f32[16,256]{1,0:T(8,128)} %bitcast.15, ...), custom_call_target="tpu_custom_call" | custom-call | tf_op jit(solution)/shard_map/pallas_call | solution.py:718
  101.6 1.7 %copy.25 = bf16[64,2048]{1,0:T(8,128)(2,1)} copy(bf16[64,2048]{1,0:T(8,128)(2,1)} %shard_map.217) | data formatting | bytes 524288

commit v5 on v4

--- a/solution.py
+++ b/solution.py
@@ -59,11 +59,31 @@
 
 
 def layer_kernel(
-    residual,
+    residual_hbm,
     gate_hbm,
     value_hbm,
     state_hbm,
     read_hbm,
+    step_hbm,
+    extra_hbm,
+    value_taps_hbm,
+    state_taps_hbm,
+    read_taps_hbm,
+    rates_hbm,
+    direct_hbm,
+    head_gain_hbm,
+    w_hbm,
+    expert_gain_hbm,
+    index_hbm,
+    share_hbm,
+    rg_hbm,
+    ru_hbm,
+    rd_hbm,
+    cg_hbm,
+    cu_hbm,
+    cd_hbm,
+    out,
+    residual,
     step_raw,
     extra_raw,
     value_taps,
@@ -72,17 +92,9 @@
     rates,
     direct,
     head_gain,
-    w_hbm,
     expert_gain,
     index_raw,
     share_raw,
-    rg_hbm,
-    ru_hbm,
-    rd_hbm,
-    cg_hbm,
-    cu_hbm,
-    cd_hbm,
-    out,
     gate_in,
     value_in,
     state_raw,
@@ -194,30 +206,44 @@
         flat = lax.rem((z * NY + y) * NC + c + step + count, count)
         return device(flat // (NY * NC), lax.rem(flat // NC, NY), lax.rem(flat, NC), x)
 
-    loads = [
-        pltpu.make_async_copy(far, near, load_sem.at[k])
-        for k, (far, near) in enumerate(
-            (
-                (value_hbm, value_in),
-                (state_hbm, state_raw),
-                (read_hbm, read_raw),
-                (gate_hbm, gate_in),
-                (w_hbm, w_out),
-                (rg_hbm, rg),
-                (ru_hbm, ru),
-                (rd_hbm, rd),
-                (cg_hbm, cg),
-                (cu_hbm, cu),
-                (cd_hbm, cd),
-            )
-        )
-    ]
-    for load in loads:
-        load.start()
     greeted = x_peers + z_peers + [peer for _, peer in plane_peers] + [along(1), along(-1)]
     barrier = pltpu.get_barrier_semaphore()
     for target in greeted:
         pl.semaphore_signal(barrier, inc=1, device_id=target, device_id_type=MESH)
+    loads = {}
+    for k, (name, far, near) in enumerate(
+        (
+            ("step", step_hbm, step_raw),
+            ("extra", extra_hbm, extra_raw),
+            ("rates", rates_hbm, rates),
+            ("value", value_hbm, value_in),
+            ("state", state_hbm, state_raw),
+            ("read", read_hbm, read_raw),
+            ("value_taps", value_taps_hbm, value_taps),
+            ("state_taps", state_taps_hbm, state_taps),
+            ("read_taps", read_taps_hbm, read_taps),
+            ("index", index_hbm, index_raw),
+            ("share", share_hbm, share_raw),
+            ("direct", direct_hbm, direct),
+            ("gate", gate_hbm, gate_in),
+            ("head_gain", head_gain_hbm, head_gain),
+            ("w", w_hbm, w_out),
+            ("residual", residual_hbm, residual),
+            ("expert_gain", expert_gain_hbm, expert_gain),
+            ("rg", rg_hbm, rg),
+            ("ru", ru_hbm, ru),
+            ("rd", rd_hbm, rd),
+            ("cg", cg_hbm, cg),
+            ("cu", cu_hbm, cu),
+            ("cd", cd_hbm, cd),
+        )
+    ):
+        loads[name] = pltpu.make_async_copy(far, near, load_sem.at[k])
+        loads[name].start()
+
+    def loaded(*wanted):
+        for name in wanted:
+            loads[name].wait()
 
     def send(src, dst, send_sem, recv_sem, target):
         copy = pltpu.make_async_remote_copy(
@@ -230,9 +256,7 @@
         )
         copy.start()
 
-    meta[...] = jnp.zeros((8, 128), F32)
-    meta[:TOPK, :ROWS] = index_raw[...].astype(F32)
-    meta[TOPK:, :ROWS] = share_raw[...]
+    loaded("step", "extra", "rates")
     sizes = jax.nn.softplus(step_raw[...])
     head_a = lax.broadcasted_iota(jnp.int32, (HEADS_HERE, HEADS_HERE), 0)
     head_b = lax.broadcasted_iota(jnp.int32, (HEADS_HERE, HEADS_HERE), 1)
@@ -270,8 +294,11 @@
         for k in range(2):
             logs[me, pl.ds(2 * g + k, 1)] = wide[:1, k * 128 : (k + 1) * 128]
 
-    for k in range(3):
-        loads[k].wait()
+    loaded("index", "share")
+    meta[...] = jnp.zeros((8, 128), F32)
+    meta[:TOPK, :ROWS] = index_raw[...].astype(F32)
+    meta[TOPK:, :ROWS] = share_raw[...]
+    loaded("value", "state", "read", "value_taps", "state_taps", "read_taps")
     pl.semaphore_wait(barrier, len(greeted))
     convs = (
         (value_in, value_rim, value_taps),
@@ -333,8 +360,10 @@
         fresh = over(state_in[:, g * STATE : (g + 1) * STATE], ending[:, at], ((0,), (0,)))
         for k in range(2):
             own_send[2 * g + k] = fresh[:, k * 128 : (k + 1) * 128].astype(BF16)
-    for index, target in plane_peers:
-        send(own_send.at[index], gathered.at[me], own_s, own_r, target)
+    parts = [pl.ds(k * (STATE // 2), STATE // 2) for k in range(2)]
+    for k, part in enumerate(parts):
+        for index, target in plane_peers:
+            send(own_send.at[index, part], gathered.at[me, part], own_s, own_r.at[k], target)
     gathered[me] = own_send[me]
 
     arrive(logs.at[pl.ds(0, PLANE - 1)], log_r)
@@ -372,19 +401,20 @@
 
     within(0)
 
-    arrive(gathered.at[pl.ds(0, PLANE - 1)], own_r)
-    carried = jnp.zeros((STATE, 128), F32)
-    for k in range(PLANE):
-        before_me[k] = carried
-        carried = carried * factors[k, pl.ds(me, 1)] + gathered[k].astype(F32)
-    planes[z] = carried.astype(BF16)
-    for d in FAR_Z:
-        send(planes.at[z], planes.at[z], slice_s, slice_r, z_peers[d - 1])
+    for h, part in enumerate(parts):
+        arrive(gathered.at[pl.ds(0, PLANE - 1), part], own_r.at[h])
+        carried = jnp.zeros((STATE // 2, 128), F32)
+        for k in range(PLANE):
+            before_me[k, part] = carried
+            carried = carried * factors[k, pl.ds(me, 1)] + gathered[k, part].astype(F32)
+        planes[z, part] = carried.astype(BF16)
+        for d in FAR_Z:
+            send(planes.at[z, part], planes.at[z, part], slice_s, slice_r.at[h], z_peers[d - 1])
 
     within(1)
     within(2)
     within(3)
-    loads[3].wait()
+    loaded("direct", "gate")
     from_start = jnp.exp(by_head)
     direct_wide = jnp.broadcast_to(as_column(direct[...]), (HEADS_HERE, 128))
     for g in range(GROUPS_HERE):
@@ -423,18 +453,22 @@
     arrive(plane_logs.at[pl.ds(0, NZ - 1)], plog_r)
     for k in range(NZ - 1):
         factors[2 * PLANE + k] = jnp.exp(plane_logs[k])
-    arrive(planes.at[pl.ds(0, NZ - 1)], slice_r)
-    carried = jnp.zeros((STATE, 128), F32)
-    for k in range(NZ - 1):
-        joined = carried * factors[2 * PLANE + k, pl.ds(me, 1)] + planes[k].astype(F32)
-        carried = jnp.where(k < z, joined, carried)
-    for k in range(PLANE):
-        incoming_send[k] = (carried * factors[PLANE + k, pl.ds(me, 1)] + before_me[k]).astype(BF16)
-    for index, target in plane_peers:
-        send(incoming_send.at[index], incoming.at[me], in_s, in_r, target)
+    for h, part in enumerate(parts):
+        arrive(planes.at[pl.ds(0, NZ - 1), part], slice_r.at[h])
+        carried = jnp.zeros((STATE // 2, 128), F32)
+        for k in range(NZ - 1):
+            joined = carried * factors[2 * PLANE + k, pl.ds(me, 1)] + planes[k, part].astype(F32)
+            carried = jnp.where(k < z, joined, carried)
+        for k in range(PLANE):
+            incoming_send[k, part] = (
+                carried * factors[PLANE + k, pl.ds(me, 1)] + before_me[k, part]
+            ).astype(BF16)
+        for index, target in plane_peers:
+            send(incoming_send.at[index, part], incoming.at[me, part], in_s, in_r.at[h], target)
     incoming[me] = incoming_send[me]
-    loads[4].wait()
-    arrive(incoming.at[pl.ds(0, PLANE - 1)], in_r)
+    loaded("head_gain", "w", "residual", "expert_gain")
+    for h, part in enumerate(parts):
+        arrive(incoming.at[pl.ds(0, PLANE - 1), part], in_r.at[h])
     for g in range(GROUPS_HERE):
         at = slice(g * WIDE, (g + 1) * WIDE)
         state = jnp.concatenate([incoming[2 * g], incoming[2 * g + 1]], axis=1)
@@ -486,62 +520,52 @@
             elif (n < 2) == up:
                 ring_arrived(3, up, n)
 
-    def dispatch(o, m):
-        for n in range(2):
-            block = stream[2 * m + n] if o == 0 else zall[o, 2 * m + n]
-            packed = over(chosen_w[o].astype(BF16), block, ((1,), (0,)))
-            send_rows[o, m, :, :, n * COLS : (n + 1) * COLS] = packed.reshape(
-                PLANE, CAP, COLS
-            ).astype(BF16)
+    def dispatch(o, n):
+        block = stream[n] if o == 0 else zall[o, n]
+        packed = over(chosen_w[o].astype(BF16), block, ((1,), (0,)))
+        send_rows[o, n] = packed.reshape(PLANE, CAP, COLS).astype(BF16)
         for index, peer in plane_peers:
-            copy = pltpu.make_async_remote_copy(
-                src_ref=send_rows.at[o, m, index],
-                dst_ref=expert_rows.at[o, m * PLANE + me],
-                send_sem=ds_sem,
-                recv_sem=dr_sem.at[o],
-                device_id=peer,
-                device_id_type=MESH,
+            send(
+                send_rows.at[o, n, index],
+                expert_rows.at[o, n * PLANE + me],
+                ds_sem,
+                dr_sem.at[o],
+                peer,
             )
-            copy.start()
-        expert_rows[o, m * PLANE + me] = send_rows[o, m, me]
+        expert_rows[o, n * PLANE + me] = send_rows[o, n, me]
 
     def run_expert(blocks):
-        halves = []
-        for m in range(2):
+        gate = lifted = None
+        for o in blocks:
+            arrive(expert_rows.at[o, pl.ds(0, PIECES * (PLANE - 1))], dr_sem.at[o])
+        for n in range(PIECES):
+            at = slice(n * COLS, (n + 1) * COLS)
             parts = []
-            gain = expert_gain[:, m * (D // 2) : (m + 1) * (D // 2)]
             for o in blocks:
-                if m == 0:
-                    arrive(expert_rows.at[o, pl.ds(0, 2 * PLANE - 2)], dr_sem.at[o])
-                wide = expert_rows[o, m * PLANE : (m + 1) * PLANE].astype(F32) * slot_scales[:, :, o : o + 1]
-                parts.append(wide.reshape(ROWS, D // 2))
-            halves.append((jnp.concatenate(parts, axis=0) * gain).astype(BF16))
-        gate = over(halves[0], rg[: D // 2], ((1,), (0,))) + over(halves[1], rg[D // 2 :], ((1,), (0,)))
-        lifted = over(halves[0], ru[: D // 2], ((1,), (0,))) + over(halves[1], ru[D // 2 :], ((1,), (0,)))
+                wide = expert_rows[o, n * PLANE : (n + 1) * PLANE].astype(F32)
+                parts.append((wide * slot_scales[:, :, o : o + 1]).reshape(ROWS, COLS))
+            piece = (jnp.concatenate(parts, axis=0) * expert_gain[:, at]).astype(BF16)
+            g, u = over(piece, rg[at], ((1,), (0,))), over(piece, ru[at], ((1,), (0,)))
+            gate, lifted = (g, u) if n == 0 else (gate + g, lifted + u)
         hidden = (jax.nn.silu(gate) * lifted).astype(BF16)
-        for m in range(2):
-            result = over(hidden, rd[:, m * (D // 2) : (m + 1) * (D // 2)], ((1,), (0,)))
+        for n in range(PIECES):
+            result = over(hidden, rd[:, n * COLS : (n + 1) * COLS], ((1,), (0,)))
             for k, o in enumerate(blocks):
-                expert_out[o, m] = (
-                    result[k * ROWS : (k + 1) * ROWS].reshape(PLANE, CAP, D // 2).astype(BF16)
+                expert_out[o, n] = (
+                    result[k * ROWS : (k + 1) * ROWS].reshape(PLANE, CAP, COLS).astype(BF16)
                 )
 
-    def give_back(o, m):
-        for index, peer in plane_peers:
-            copy = pltpu.make_async_remote_copy(
-                src_ref=expert_out.at[o, m, index],
-                dst_ref=back_rows.at[o, m, me],
-                send_sem=bs_sem,
-                recv_sem=br_sem.at[o, m],
-                device_id=peer,
-                device_id_type=MESH,
-            )
-            copy.start()
-        back_rows[o, m, me] = expert_out[o, m, me]
-
-    def combined(o, m):
-        arrive(back_rows.at[o, m, pl.ds(0, PLANE - 1)], br_sem.at[o, m])
-        returned = back_rows[o, m].astype(F32).reshape(ROWS, D // 2).astype(BF16)
+    def give_back(o):
+        for n in ((0, 2, 1, 3) if o == 4 else (2, 3, 0, 1) if o > 4 else range(PIECES)):
+            for index, peer in plane_peers:
+                send(
+                    expert_out.at[o, n, index], back_rows.at[o, n, me], bs_sem, br_sem.at[o, n], peer
+                )
+            back_rows[o, n, me] = expert_out[o, n, me]
+
+    def combined(o, n):
+        arrive(back_rows.at[o, n, pl.ds(0, PLANE - 1)], br_sem.at[o, n])
+        returned = back_rows[o, n].astype(F32).reshape(ROWS, COLS).astype(BF16)
         return over(combine_w[o].astype(BF16), returned, ((0,), (0,)))
 
     square_sums = []
@@ -560,14 +584,20 @@
         square_sums.append(jnp.sum(wide * wide, axis=-1, keepdims=True))
 
     take_piece(0)
+    dispatch(0, 0)
     take_piece(1)
-    dispatch(0, 0)
     relay(0, 0)
+    dispatch(7, 0)
+    dispatch(1, 0)
+    dispatch(0, 1)
     take_piece(2)
     relay(0, 1)
-    dispatch(7, 0)
-    dispatch(1, 0)
+    dispatch(7, 1)
+    dispatch(1, 1)
     relay(1, 0)
+    dispatch(6, 0)
+    dispatch(2, 0)
+    dispatch(0, 2)
     take_piece(3)
     squares = square_sums[0] + square_sums[1] + square_sums[2] + square_sums[3]
     scale = lax.rsqrt(squares * (1.0 / D) + EPSILON)
@@ -576,20 +606,24 @@
     scale_send[:1, :ROWS] = scale_row
     for d in FAR_Z:
         send(scale_send, scales.at[NZ - d], sc_s, sc_r, z_peers[d - 1])
-    dispatch(0, 1)
+    relay(0, 2)
+    dispatch(7, 2)
+    dispatch(1, 2)
+    relay(1, 1)
+    dispatch(6, 1)
+    dispatch(2, 1)
+    dispatch(0, 3)
     for n in range(PIECES):
         at = slice(n * COLS, (n + 1) * COLS)
         rows[:, at] = (stream[n].astype(F32) * scale * expert_gain[:, at]).astype(BF16)
     for d in FAR_X:
         send(rows, xall.at[x], xs_sem, xr_sem, x_peers[d - 1])
-    relay(0, 2)
-    relay(1, 1)
-    dispatch(6, 0)
-    dispatch(2, 0)
     relay(2, 0)
+    dispatch(5, 0)
+    dispatch(3, 0)
     relay(0, 3)
-    dispatch(7, 1)
-    dispatch(1, 1)
+    dispatch(7, 3)
+    dispatch(1, 3)
     lane = lax.broadcasted_iota(jnp.int32, (PLANE, CAP, 128), 2)
     by_slot = jnp.zeros((PLANE, CAP, 128), F32)
     arrive(scales.at[pl.ds(0, NZ - 1)], sc_r)
@@ -602,27 +636,32 @@
         send(slot_send.at[index], slot_scales.at[me], sl_s, sl_r, target)
     slot_scales[me] = slot_send[me]
     relay(1, 2)
+    dispatch(6, 2)
+    dispatch(2, 2)
     relay(2, 1)
-    dispatch(5, 0)
-    dispatch(3, 0)
+    dispatch(5, 1)
+    dispatch(3, 1)
     relay(3, 0)
+    dispatch(4, 0)
     relay(1, 3)
-    dispatch(6, 1)
-    dispatch(2, 1)
-    for k in range(5, 11):
-        loads[k].wait()
+    dispatch(6, 3)
+    dispatch(2, 3)
+    loaded("rg", "ru", "rd", "cg", "cu", "cd")
     arrive(slot_scales.at[pl.ds(0, PLANE - 1)], sl_r)
     run_expert((0,))
     relay(2, 2)
+    dispatch(5, 2)
+    dispatch(3, 2)
     relay(3, 1)
-    dispatch(4, 0)
+    dispatch(4, 1)
     relay(2, 3)
-    dispatch(5, 1)
-    dispatch(3, 1)
+    dispatch(5, 3)
     run_expert((7, 1))
     relay(3, 2)
+    dispatch(4, 2)
     relay(3, 3)
-    dispatch(4, 1)
+    dispatch(4, 3)
+    dispatch(3, 3)
     arrive(xall.at[pl.ds(0, NX - 1)], xr_sem)
     xall[x] = rows[...]
     hidden_rows = xall[...].reshape(NX * ROWS, D)
@@ -640,19 +679,20 @@
             x_peers[d - 1],
         )
     run_expert((6, 2))
+    run_expert((4,))
+    give_back(4)
     run_expert((5, 3))
-    run_expert((4,))
-    for o in (4, 3, 5, 2, 6, 1, 7, 0):
-        for m in range(2):
-            give_back(o, m)
-
-    def cell(step, up, m):
+    for o in (3, 5, 2, 6, 1, 7, 0):
+        give_back(o)
+
+    def cell(step, up, n):
         if step == 0:
-            return 12 + m
-        return (step - 1) * 4 + (0 if up else 2) + m
-
-    def pass_on(step, up, m):
-        k = cell(step, up, m)
+            return 24 + n
+        return (step - 1) * 8 + (0 if up else 4) + n
+
+    def pass_on(step, up, n, piece):
+        k = cell(step, up, n)
+        rs_send[k] = piece.astype(BF16)
         send(
             rs_send.at[k],
             rs_recv.at[k],
@@ -661,32 +701,29 @@
             device(z_at(1 if up else -1), y, c, x),
         )
 
-    def sum_arrived(step, up, m):
-        k = cell(step, up, m)
+    def sum_arrived(step, up, n):
+        k = cell(step, up, n)
         arrive(rs_recv.at[k], rsr_sem.at[k])
         return rs_recv[k].astype(F32)
 
-    for m, up in ((0, True), (1, False)):
-        rs_send[cell(0, up, m)] = combined(4, m).astype(BF16)
-        pass_on(0, up, m)
+    for n in (0, 2, 1, 3):
+        pass_on(0, n < 2, n, combined(4, n))
     for step in range(1, 4):
-        for k, up in enumerate((True, False)):
-            for m in (k, 1 - k):
-                piece = combined(4 - step if up else 4 + step, m)
-                if step > 1 or m == k:
-                    piece = piece + sum_arrived(step - 1, up, m)
-                rs_send[cell(step, up, m)] = piece.astype(BF16)
-                pass_on(step, up, m)
+        for up, order in ((True, (0, 1, 2, 3)), (False, (2, 3, 0, 1))):
+            for n in order:
+                piece = combined(4 - step if up else 4 + step, n)
+                if step > 1 or (n < 2) == up:
+                    piece = piece + sum_arrived(step - 1, up, n)
+                pass_on(step, up, n, piece)
     arrive(sh_recv, hr_sem)
-    for m in range(2):
-        at = slice(m * (D // 2), (m + 1) * (D // 2))
-        piece = jnp.concatenate([stream[2 * m], stream[2 * m + 1]], axis=1).astype(F32)
-        piece = piece + sh_send[x, :, at].astype(F32)
+    for n in (2, 3, 0, 1):
+        at = slice(n * COLS, (n + 1) * COLS)
+        piece = stream[n].astype(F32) + sh_send[x, :, at].astype(F32)
         for d in range(1, NX):
             piece = piece + sh_recv[d - 1, :, at].astype(F32)
-        piece = piece + combined(0, m)
+        piece = piece + combined(0, n)
         for up in (True, False):
-            piece = piece + sum_arrived(3, up, m)
+            piece = piece + sum_arrived(3, up, n)
         out[:, at] = piece.astype(BF16)
 
     for k, (near, _, _) in enumerate(convs):
@@ -718,9 +755,21 @@
     return pl.pallas_call(
         layer_kernel,
         out_shape=jax.ShapeDtypeStruct((ROWS, D), BF16),
-        in_specs=[vmem] + [hbm] * 4 + [vmem] * 8 + [hbm] + [vmem] * 3 + [hbm] * 6,
+        in_specs=[hbm] * 23,
         out_specs=vmem,
         scratch_shapes=[
+            pltpu.VMEM((ROWS, D), BF16),
+            pltpu.VMEM((HEADS_HERE, LENGTH), F32),
+            pltpu.VMEM((HEADS_HERE, LENGTH), F32),
+            pltpu.VMEM((CONV, INNER), BF16),
+            pltpu.VMEM((CONV, NARROW), BF16),
+            pltpu.VMEM((CONV, NARROW), BF16),
+            pltpu.VMEM((1, HEADS_HERE), F32),
+            pltpu.VMEM((1, HEADS_HERE), F32),
+            pltpu.VMEM((1, INNER), F32),
+            pltpu.VMEM((1, D), F32),
+            pltpu.VMEM((TOPK, ROWS), jnp.int32),
+            pltpu.VMEM((TOPK, ROWS), F32),
             pltpu.VMEM((LENGTH, INNER), BF16),
             pltpu.VMEM((LENGTH, INNER), BF16),
             pltpu.VMEM((LENGTH, NARROW), BF16),
@@ -762,12 +811,12 @@
             pltpu.VMEM((NZ, ROWS, ROWS), F32),
             pltpu.VMEM((NZ, 8, 128), F32),
             pltpu.VMEM((NZ, ROWS, ROWS), F32),
-            pltpu.VMEM((NZ, 2, PLANE, CAP, D // 2), BF16),
-            pltpu.VMEM((NZ, 2 * PLANE, CAP, D // 2), BF16),
-            pltpu.VMEM((NZ, 2, PLANE, CAP, D // 2), BF16),
-            pltpu.VMEM((NZ, 2, PLANE, CAP, D // 2), BF16),
-            pltpu.VMEM((14, ROWS, D // 2), BF16),
-            pltpu.VMEM((14, ROWS, D // 2), BF16),
+            pltpu.VMEM((NZ, PIECES, PLANE, CAP, COLS), BF16),
+            pltpu.VMEM((NZ, PIECES * PLANE, CAP, COLS), BF16),
+            pltpu.VMEM((NZ, PIECES, PLANE, CAP, COLS), BF16),
+            pltpu.VMEM((NZ, PIECES, PLANE, CAP, COLS), BF16),
+            pltpu.VMEM((28, ROWS, COLS), BF16),
+            pltpu.VMEM((28, ROWS, COLS), BF16),
             pltpu.VMEM((NX, ROWS, D), BF16),
             pltpu.VMEM((NX, ROWS, D), BF16),
             pltpu.VMEM((NX - 1, ROWS, D), BF16),
@@ -777,19 +826,19 @@
             pltpu.VMEM((D, 128), BF16),
             pltpu.VMEM((D, 128), BF16),
             pltpu.VMEM((D, 128), BF16),
-            dma((11,)),
+            dma((23,)),
             dma((3,)),
             dma((3,)),
             dma,
             dma,
             dma,
-            dma,
-            dma,
-            dma,
-            dma,
-            dma,
-            dma,
-            dma,
+            dma((2,)),
+            dma,
+            dma,
+            dma,
+            dma((2,)),
+            dma,
+            dma((2,)),
             dma,
             dma((PIECES,)),
             dma,
@@ -803,9 +852,9 @@
             dma,
             dma((NZ,)),
             dma,
-            dma((NZ, 2)),
-            dma,
-            dma((14,)),
+            dma((NZ, PIECES)),
+            dma,
+            dma((28,)),
             dma,
             dma,
             dma,

time: 103 us -> 100 us (0.971)
  Pallas kernels: 102 us -> 98.3 us
    pallas_call x1, Pallas kernels: 102 us -> 98.3 us  [layer(): pl.pallas_call(layer_kernel, out_shape=jax.ShapeDtypeStruct((ROWS, D), BF...]
where the time goes in v5:
time: 100 us
  Pallas kernels  98.3 us (98%)
  local copies, waits for them, and re-layouts  1.67 us (2%)
    pallas_call x1, Pallas kernels, layer(): pl.pallas_call(layer_kernel, out_shape=jax.ShapeDtypeStruct((ROWS, D), BF...  98.3 us

profile of v5, /device:TPU:1, one launch (start us, length us, event | category | flops | bytes accessed | tf_op | source)
XLA Modules:
  0.0 100.0 jit_solution(9076582795439239598)
XLA Ops:
  0.0 98.3 %shard_map.217 = bf16[64,2048]{1,0:T(8,128)(2,1)} custom-call(bf16[64,2048]{1,0:T(8,128)(2,1)} %residual_hbm.1, bf16[256,1024]{1,0:T(8,128)(2,1)} %gate_hbm.1, bf16[256,1024]{1,0:T(8,128)(2,1)} %value_hbm.1, bf16[256,512]{1,0:T(8,128)(2,1)} %state_hbm.1, bf16[256,512]{1,0:T(8,128)(2,1)} %read_hbm.1, f32[16,256]{1,0:T(8,128)} %bitcast.14, ...), custom_call_target="tpu_custom_call" | custom-call | tf_op jit(solution)/shard_map/pallas_call | solution.py:755
  98.3 1.7 %copy.25 = bf16[64,2048]{1,0:T(8,128)(2,1)} copy(bf16[64,2048]{1,0:T(8,128)(2,1)} %shard_map.217) | data formatting | bytes 524288

commit v6 on v5

--- a/solution.py
+++ b/solution.py
@@ -35,6 +35,8 @@
 RIM = 16
 COLS = 512
 PIECES = D // COLS
+FINE = 256
+PARTS = D // FINE
 
 
 def device(z, y, c, x):
@@ -116,6 +118,8 @@
     heads_out,
     own_send,
     gathered,
+    edge_send,
+    edges,
     before_me,
     planes,
     incoming_send,
@@ -125,6 +129,7 @@
     factors,
     mix_send,
     mix_recv,
+    staged,
     stream,
     rows,
     meta,
@@ -151,11 +156,14 @@
     cg,
     cu,
     cd,
+    out_sem,
     load_sem,
     rim_s,
     rim_r,
     log_s,
     log_r,
+    edge_s,
+    edge_r,
     own_s,
     own_r,
     plog_s,
@@ -176,6 +184,7 @@
     mr_sem,
     ds_sem,
     dr_sem,
+    last_r,
     bs_sem,
     br_sem,
     rss_sem,
@@ -346,8 +355,14 @@
         ending[RIM:, at] = (value * ended[RIM:]).astype(BF16)
         first_sized[:, at] = sized[:RIM]
         first_ended[:, at] = ended[:RIM]
-    for lo in range(0, NARROW, WIDE):
-        readout[RIM:, lo : lo + WIDE] = late_rows(2, lo).astype(BF16)
+        fresh = over(state_in[RIM:, g * STATE : (g + 1) * STATE], ending[RIM:, at], ((0,), (0,)))
+        for k in range(2):
+            own_send[2 * g + k] = fresh[:, k * 128 : (k + 1) * 128].astype(BF16)
+    parts = [pl.ds(k * (STATE // 2), STATE // 2) for k in range(2)]
+    for k, part in enumerate(parts):
+        for index, target in plane_peers:
+            send(own_send.at[index, part], gathered.at[me, part], own_s, own_r.at[k], target)
+    gathered[me] = own_send[me]
     arrive(state_rim, rim_r.at[1])
     for lo in range(0, NARROW, WIDE):
         state_in[:RIM, lo : lo + WIDE] = early_rows(1, lo).astype(BF16)
@@ -356,15 +371,15 @@
         at = slice(g * WIDE, (g + 1) * WIDE)
         value = early_rows(0, g * WIDE)
         values[:RIM, at] = value
-        ending[:RIM, at] = (value * first_ended[:, at]).astype(BF16)
-        fresh = over(state_in[:, g * STATE : (g + 1) * STATE], ending[:, at], ((0,), (0,)))
+        edge = (value * first_ended[:, at]).astype(BF16)
         for k in range(2):
-            own_send[2 * g + k] = fresh[:, k * 128 : (k + 1) * 128].astype(BF16)
-    parts = [pl.ds(k * (STATE // 2), STATE // 2) for k in range(2)]
-    for k, part in enumerate(parts):
-        for index, target in plane_peers:
-            send(own_send.at[index, part], gathered.at[me, part], own_s, own_r.at[k], target)
-    gathered[me] = own_send[me]
+            edge_send[2 * g + k, 0] = state_in[:RIM, g * STATE : (g + 1) * STATE]
+            edge_send[2 * g + k, 1] = edge[:, k * 128 : (k + 1) * 128]
+    for index, target in plane_peers:
+        send(edge_send.at[index], edges.at[me], edge_s, edge_r, target)
+    edges[me] = edge_send[me]
+    for lo in range(0, NARROW, WIDE):
+        readout[RIM:, lo : lo + WIDE] = late_rows(2, lo).astype(BF16)
 
     arrive(logs.at[pl.ds(0, PLANE - 1)], log_r)
     reach = jnp.zeros((PAIRS, 128), F32)
@@ -401,12 +416,16 @@
 
     within(0)
 
+    arrive(edges.at[pl.ds(0, PLANE - 1)], edge_r)
+    for k in range(PLANE):
+        before_me[k] = over(edges[k, 0], edges[k, 1], ((0,), (0,)))
     for h, part in enumerate(parts):
         arrive(gathered.at[pl.ds(0, PLANE - 1), part], own_r.at[h])
         carried = jnp.zeros((STATE // 2, 128), F32)
         for k in range(PLANE):
+            fresh = gathered[k, part].astype(F32) + before_me[k, part]
             before_me[k, part] = carried
-            carried = carried * factors[k, pl.ds(me, 1)] + gathered[k, part].astype(F32)
+            carried = carried * factors[k, pl.ds(me, 1)] + fresh
         planes[z, part] = carried.astype(BF16)
         for d in FAR_Z:
             send(planes.at[z, part], planes.at[z, part], slice_s, slice_r.at[h], z_peers[d - 1])
@@ -467,31 +486,40 @@
             send(incoming_send.at[index, part], incoming.at[me, part], in_s, in_r.at[h], target)
     incoming[me] = incoming_send[me]
     loaded("head_gain", "w", "residual", "expert_gain")
-    for h, part in enumerate(parts):
-        arrive(incoming.at[pl.ds(0, PLANE - 1), part], in_r.at[h])
+    blank = jnp.zeros((STATE // 2, WIDE), BF16)
+
+    def carried_part(g, h):
+        half = jnp.concatenate([incoming[2 * g, parts[h]], incoming[2 * g + 1, parts[h]]], axis=1)
+        state = jnp.concatenate([half, blank] if h == 0 else [blank, half], axis=0)
+        at = slice(g * WIDE, (g + 1) * WIDE)
+        return over(readout[:, g * STATE : (g + 1) * STATE], state, ((1,), (0,))) * values[:, at]
+
+    arrive(incoming.at[pl.ds(0, PLANE - 1), parts[0]], in_r.at[0])
     for g in range(GROUPS_HERE):
         at = slice(g * WIDE, (g + 1) * WIDE)
-        state = jnp.concatenate([incoming[2 * g], incoming[2 * g + 1]], axis=1)
-        carried_out = over(readout[:, g * STATE : (g + 1) * STATE], state, ((1,), (0,)))
-        gated = mixed[:, at] + carried_out * values[:, at]
-        squares = jnp.zeros((LENGTH, WIDE), F32)
-        for term in split_terms(gated * gated, 2):
-            squares = squares + over(term, same_head, ((1,), (0,)))
+        mixed[:, at] = mixed[:, at] + carried_part(g, 0)
+    arrive(incoming.at[pl.ds(0, PLANE - 1), parts[1]], in_r.at[1])
+    for g in range(GROUPS_HERE):
+        at = slice(g * WIDE, (g + 1) * WIDE)
+        gated = mixed[:, at] + carried_part(g, 1)
+        squares = over((gated * gated).astype(BF16), same_head, ((1,), (0,)))
         normed = gated * lax.rsqrt(squares * (1.0 / HEAD_DIM) + EPSILON) * head_gain[:, at]
         heads_out[:, at] = normed.astype(BF16)
 
-    for n in range(PIECES):
-        partial = over(heads_out[...], w_out[:, n * COLS : (n + 1) * COLS], ((1,), (0,)))
-        mix_send[n] = partial.astype(BF16)
-        for d in FAR_X:
-            xx = lax.rem(x + d, NX)
-            send(
-                mix_send.at[n, pl.ds(pl.multiple_of(xx * ROWS, ROWS), ROWS)],
-                mix_recv.at[n, NX - d - 1],
-                mix_s,
-                mix_r.at[n],
-                x_peers[d - 1],
-            )
+    for m in range(PIECES):
+        partial = over(heads_out[...], w_out[:, m * COLS : (m + 1) * COLS], ((1,), (0,)))
+        for n in (2 * m, 2 * m + 1):
+            lo = (n - 2 * m) * FINE
+            mix_send[n] = partial[:, lo : lo + FINE].astype(BF16)
+            for d in FAR_X:
+                xx = lax.rem(x + d, NX)
+                send(
+                    mix_send.at[n, pl.ds(pl.multiple_of(xx * ROWS, ROWS), ROWS)],
+                    mix_recv.at[n, NX - d - 1],
+                    mix_s,
+                    mix_r.at[n],
+                    x_peers[d - 1],
+                )
     def hop(step, up, n):
         here = ((NZ - step) % NZ) if up else step
         there = ((NZ - step - 1) % NZ) if up else step + 1
@@ -515,21 +543,24 @@
                 hop(step + 1, up, n)
             elif step == 2:
                 ring_arrived(step, up, n)
-                if (n < 2) == up:
+                if (n < PARTS // 2) == up:
                     hop(3, up, n)
-            elif (n < 2) == up:
+            elif (n < PARTS // 2) == up:
                 ring_arrived(3, up, n)
 
     def dispatch(o, n):
-        block = stream[n] if o == 0 else zall[o, n]
-        packed = over(chosen_w[o].astype(BF16), block, ((1,), (0,)))
-        send_rows[o, n] = packed.reshape(PLANE, CAP, COLS).astype(BF16)
+        for k in range(2):
+            block = stream[2 * n + k] if o == 0 else zall[o, 2 * n + k]
+            packed = over(chosen_w[o].astype(BF16), block, ((1,), (0,)))
+            send_rows[o, n, :, :, k * FINE : (k + 1) * FINE] = packed.reshape(
+                PLANE, CAP, FINE
+            ).astype(BF16)
         for index, peer in plane_peers:
             send(
                 send_rows.at[o, n, index],
                 expert_rows.at[o, n * PLANE + me],
                 ds_sem,
-                dr_sem.at[o],
+                last_r.at[n] if o == 4 else dr_sem.at[o],
                 peer,
             )
         expert_rows[o, n * PLANE + me] = send_rows[o, n, me]
@@ -537,8 +568,11 @@
     def run_expert(blocks):
         gate = lifted = None
         for o in blocks:
-            arrive(expert_rows.at[o, pl.ds(0, PIECES * (PLANE - 1))], dr_sem.at[o])
+            if o != 4:
+                arrive(expert_rows.at[o, pl.ds(0, PIECES * (PLANE - 1))], dr_sem.at[o])
         for n in range(PIECES):
+            if blocks == (4,):
+                arrive(expert_rows.at[4, pl.ds(n * PLANE, PLANE - 1)], last_r.at[n])
             at = slice(n * COLS, (n + 1) * COLS)
             parts = []
             for o in blocks:
@@ -548,20 +582,23 @@
             g, u = over(piece, rg[at], ((1,), (0,))), over(piece, ru[at], ((1,), (0,)))
             gate, lifted = (g, u) if n == 0 else (gate + g, lifted + u)
         hidden = (jax.nn.silu(gate) * lifted).astype(BF16)
-        for n in range(PIECES):
+        for n in (0, 2, 1, 3):
             result = over(hidden, rd[:, n * COLS : (n + 1) * COLS], ((1,), (0,)))
             for k, o in enumerate(blocks):
                 expert_out[o, n] = (
                     result[k * ROWS : (k + 1) * ROWS].reshape(PLANE, CAP, COLS).astype(BF16)
                 )
+            if blocks == (4,):
+                give_piece(4, n)
+
+    def give_piece(o, n):
+        for index, peer in plane_peers:
+            send(expert_out.at[o, n, index], back_rows.at[o, n, me], bs_sem, br_sem.at[o, n], peer)
+        back_rows[o, n, me] = expert_out[o, n, me]
 
     def give_back(o):
-        for n in ((0, 2, 1, 3) if o == 4 else (2, 3, 0, 1) if o > 4 else range(PIECES)):
-            for index, peer in plane_peers:
-                send(
-                    expert_out.at[o, n, index], back_rows.at[o, n, me], bs_sem, br_sem.at[o, n], peer
-                )
-            back_rows[o, n, me] = expert_out[o, n, me]
+        for n in (2, 3, 0, 1) if o > 4 else range(PIECES):
+            give_piece(o, n)
 
     def combined(o, n):
         arrive(back_rows.at[o, n, pl.ds(0, PLANE - 1)], br_sem.at[o, n])
@@ -571,7 +608,7 @@
     square_sums = []
 
     def take_piece(n):
-        at = slice(n * COLS, (n + 1) * COLS)
+        at = slice(n * FINE, (n + 1) * FINE)
         summed = mix_send[n, pl.ds(pl.multiple_of(x * ROWS, ROWS), ROWS)].astype(F32)
         arrive(mix_recv.at[n], mix_r.at[n])
         for d in range(1, NX):
@@ -584,44 +621,57 @@
         square_sums.append(jnp.sum(wide * wide, axis=-1, keepdims=True))
 
     take_piece(0)
+    take_piece(1)
     dispatch(0, 0)
-    take_piece(1)
+    take_piece(2)
     relay(0, 0)
+    take_piece(3)
+    dispatch(0, 1)
+    relay(0, 1)
     dispatch(7, 0)
     dispatch(1, 0)
-    dispatch(0, 1)
-    take_piece(2)
-    relay(0, 1)
+    take_piece(4)
+    relay(0, 2)
+    relay(1, 0)
+    take_piece(5)
+    dispatch(0, 2)
+    relay(0, 3)
     dispatch(7, 1)
     dispatch(1, 1)
-    relay(1, 0)
+    relay(1, 1)
     dispatch(6, 0)
     dispatch(2, 0)
-    dispatch(0, 2)
-    take_piece(3)
-    squares = square_sums[0] + square_sums[1] + square_sums[2] + square_sums[3]
+    take_piece(6)
+    relay(0, 4)
+    relay(1, 2)
+    take_piece(7)
+    dispatch(0, 3)
+    squares = sum(square_sums)
     scale = lax.rsqrt(squares * (1.0 / D) + EPSILON)
     scale_row = jnp.sum(jnp.where(token == later, scale, 0.0), axis=0, keepdims=True)
     scale_send[...] = jnp.zeros((8, 128), F32)
     scale_send[:1, :ROWS] = scale_row
     for d in FAR_Z:
         send(scale_send, scales.at[NZ - d], sc_s, sc_r, z_peers[d - 1])
-    relay(0, 2)
-    dispatch(7, 2)
-    dispatch(1, 2)
-    relay(1, 1)
-    dispatch(6, 1)
-    dispatch(2, 1)
-    dispatch(0, 3)
-    for n in range(PIECES):
-        at = slice(n * COLS, (n + 1) * COLS)
+    relay(2, 0)
+    for n in range(PARTS):
+        at = slice(n * FINE, (n + 1) * FINE)
         rows[:, at] = (stream[n].astype(F32) * scale * expert_gain[:, at]).astype(BF16)
     for d in FAR_X:
         send(rows, xall.at[x], xs_sem, xr_sem, x_peers[d - 1])
-    relay(2, 0)
+    relay(0, 5)
+    dispatch(7, 2)
+    dispatch(1, 2)
+    relay(1, 3)
+    dispatch(6, 1)
+    dispatch(2, 1)
+    relay(2, 1)
     dispatch(5, 0)
     dispatch(3, 0)
-    relay(0, 3)
+    relay(0, 6)
+    relay(1, 4)
+    relay(2, 2)
+    relay(0, 7)
     dispatch(7, 3)
     dispatch(1, 3)
     lane = lax.broadcasted_iota(jnp.int32, (PLANE, CAP, 128), 2)
@@ -635,33 +685,41 @@
     for index, target in plane_peers:
         send(slot_send.at[index], slot_scales.at[me], sl_s, sl_r, target)
     slot_scales[me] = slot_send[me]
-    relay(1, 2)
+    relay(3, 0)
+    relay(1, 5)
     dispatch(6, 2)
     dispatch(2, 2)
-    relay(2, 1)
+    relay(2, 3)
     dispatch(5, 1)
     dispatch(3, 1)
-    relay(3, 0)
+    relay(3, 1)
     dispatch(4, 0)
-    relay(1, 3)
+    relay(1, 6)
+    relay(2, 4)
+    relay(3, 2)
+    relay(1, 7)
     dispatch(6, 3)
     dispatch(2, 3)
     loaded("rg", "ru", "rd", "cg", "cu", "cd")
     arrive(slot_scales.at[pl.ds(0, PLANE - 1)], sl_r)
     run_expert((0,))
-    relay(2, 2)
+    relay(2, 5)
     dispatch(5, 2)
     dispatch(3, 2)
-    relay(3, 1)
+    relay(3, 3)
     dispatch(4, 1)
-    relay(2, 3)
+    relay(3, 4)
+    relay(2, 6)
+    relay(2, 7)
     dispatch(5, 3)
     run_expert((7, 1))
-    relay(3, 2)
+    relay(3, 5)
     dispatch(4, 2)
-    relay(3, 3)
+    relay(3, 6)
+    relay(3, 7)
     dispatch(4, 3)
     dispatch(3, 3)
+    give_back(1)
     arrive(xall.at[pl.ds(0, NX - 1)], xr_sem)
     xall[x] = rows[...]
     hidden_rows = xall[...].reshape(NX * ROWS, D)
@@ -680,9 +738,8 @@
         )
     run_expert((6, 2))
     run_expert((4,))
-    give_back(4)
     run_expert((5, 3))
-    for o in (3, 5, 2, 6, 1, 7, 0):
+    for o in (3, 5, 2, 6, 7, 0):
         give_back(o)
 
     def cell(step, up, n):
@@ -718,13 +775,15 @@
     arrive(sh_recv, hr_sem)
     for n in (2, 3, 0, 1):
         at = slice(n * COLS, (n + 1) * COLS)
-        piece = stream[n].astype(F32) + sh_send[x, :, at].astype(F32)
+        piece = jnp.concatenate([stream[2 * n], stream[2 * n + 1]], axis=1).astype(F32)
+        piece = piece + sh_send[x, :, at].astype(F32)
         for d in range(1, NX):
             piece = piece + sh_recv[d - 1, :, at].astype(F32)
         piece = piece + combined(0, n)
         for up in (True, False):
             piece = piece + sum_arrived(3, up, n)
-        out[:, at] = piece.astype(BF16)
+        staged[:, at] = piece.astype(BF16)
+        pltpu.make_async_copy(staged.at[:, at], out.at[:, at], out_sem).start()
 
     for k, (near, _, _) in enumerate(convs):
         arrive(near.at[pl.ds(0, RIM)], rim_s.at[k])
@@ -732,6 +791,7 @@
         (logs.at[pl.ds(0, PLANE - 1)], log_s),
         (metas.at[pl.ds(0, NZ - 1)], ms_sem),
         (own_send.at[pl.ds(0, PLANE - 1)], own_s),
+        (edge_send.at[pl.ds(0, PLANE - 1)], edge_s),
         (plane_logs.at[pl.ds(0, NZ - 1)], plog_s),
         (planes.at[pl.ds(0, NZ - 1)], slice_s),
         (incoming_send.at[pl.ds(0, PLANE - 1)], in_s),
@@ -746,17 +806,17 @@
         (rs_send, rss_sem),
     ):
         arrive(ref, sem)
+    pltpu.make_async_copy(staged, out, out_sem).wait()
 
 
 def layer(*arrays):
-    vmem = pl.BlockSpec(memory_space=pltpu.VMEM)
     hbm = pl.BlockSpec(memory_space=pl.ANY)
     dma = pltpu.SemaphoreType.DMA
     return pl.pallas_call(
         layer_kernel,
         out_shape=jax.ShapeDtypeStruct((ROWS, D), BF16),
         in_specs=[hbm] * 23,
-        out_specs=vmem,
+        out_specs=hbm,
         scratch_shapes=[
             pltpu.VMEM((ROWS, D), BF16),
             pltpu.VMEM((HEADS_HERE, LENGTH), F32),
@@ -791,6 +851,8 @@
             pltpu.VMEM((LENGTH, INNER), BF16),
             pltpu.VMEM((PAIRS, STATE, 128), BF16),
             pltpu.VMEM((PAIRS, STATE, 128), BF16),
+            pltpu.VMEM((PAIRS, 2, RIM, 128), BF16),
+            pltpu.VMEM((PLANE, 2, RIM, 128), BF16),
             pltpu.VMEM((PAIRS, STATE, 128), F32),
             pltpu.VMEM((NZ, STATE, 128), BF16),
             pltpu.VMEM((PAIRS, STATE, 128), BF16),
@@ -798,12 +860,13 @@
             pltpu.VMEM((PLANE, PAIRS, 128), F32),
             pltpu.VMEM((NZ, PAIRS, 128), F32),
             pltpu.VMEM((2 * PLANE + NZ, PAIRS, 128), F32),
-            pltpu.VMEM((PIECES, LENGTH, COLS), BF16),
-            pltpu.VMEM((PIECES, NX - 1, ROWS, COLS), BF16),
-            pltpu.VMEM((PIECES, ROWS, COLS), BF16),
+            pltpu.VMEM((PARTS, LENGTH, FINE), BF16),
+            pltpu.VMEM((PARTS, NX - 1, ROWS, FINE), BF16),
+            pltpu.VMEM((ROWS, D), BF16),
+            pltpu.VMEM((PARTS, ROWS, FINE), BF16),
             pltpu.VMEM((ROWS, D), BF16),
             pltpu.VMEM((8, 128), F32),
-            pltpu.VMEM((NZ, PIECES, ROWS, COLS), BF16),
+            pltpu.VMEM((NZ, PARTS, ROWS, FINE), BF16),
             pltpu.VMEM((8, 128), F32),
             pltpu.VMEM((NZ, 8, 128), F32),
             pltpu.VMEM((PLANE, CAP, 128), F32),
@@ -826,12 +889,15 @@
             pltpu.VMEM((D, 128), BF16),
             pltpu.VMEM((D, 128), BF16),
             pltpu.VMEM((D, 128), BF16),
+            dma,
             dma((23,)),
             dma((3,)),
             dma((3,)),
             dma,
             dma,
             dma,
+            dma,
+            dma,
             dma((2,)),
             dma,
             dma,
@@ -840,17 +906,18 @@
             dma,
             dma((2,)),
             dma,
+            dma((PARTS,)),
+            dma,
+            dma((2, 4, PARTS)),
+            dma,
+            dma,
+            dma,
+            dma,
+            dma,
+            dma,
+            dma,
+            dma((NZ,)),
             dma((PIECES,)),
-            dma,
-            dma((2, 4, PIECES)),
-            dma,
-            dma,
-            dma,
-            dma,
-            dma,
-            dma,
-            dma,
-            dma((NZ,)),
             dma,
             dma((NZ, PIECES)),
             dma,

time: 100 us -> 99.4 us (level)
  no operation moved by 1% of the time
where the time goes in v6:
time: 99.4 us; the launch traced here: 99.3 us
  Pallas kernels  97.6 us (98%)
  local copies, waits for them, and re-layouts  1.67 us (2%)
    pallas_call x1, Pallas kernels, layer(): pl.pallas_call(layer_kernel, out_shape=jax.ShapeDtypeStruct((ROWS, D), BF...  97.6 us

profile of v6, /device:TPU:1, one launch (start us, length us, event | category | flops | bytes accessed | tf_op | source)
XLA Modules:
  0.0 99.3 jit_solution(18361457049377882858)
XLA Ops:
  0.0 97.6 %shard_map.217 = bf16[64,2048]{1,0:T(8,128)(2,1)} custom-call(bf16[64,2048]{1,0:T(8,128)(2,1)} %residual_hbm.1, bf16[256,1024]{1,0:T(8,128)(2,1)} %gate_hbm.1, bf16[256,1024]{1,0:T(8,128)(2,1)} %value_hbm.1, bf16[256,512]{1,0:T(8,128)(2,1)} %state_hbm.1, bf16[256,512]{1,0:T(8,128)(2,1)} %read_hbm.1, f32[16,256]{1,0:T(8,128)} %bitcast.14, ...), custom_call_target="tpu_custom_call" | custom-call | tf_op jit(solution)/shard_map/pallas_call | solution.py:815
  97.6 1.7 %copy.25 = bf16[64,2048]{1,0:T(8,128)(2,1)} copy(bf16[64,2048]{1,0:T(8,128)(2,1)} %shard_map.217) | data formatting | bytes 524288
